TPU v7x, 256 devices: a whole 4x4x8 slice. The times are simulated.
256 devices in a mesh: ep: 32 (over z, x), tp: 8 (over y, core).
Axes of the slice: x: 4, y: 4, z: 8, core: 2. Of those that a mesh axis runs over, the one named last changes fastest.
Arguments:
- queries: bfloat16 [16384, 1024], P('ep', 'tp'), may hold values from -8 to 8
- keys_values: bfloat16 [16384, 1024], P('ep', 'tp'), may hold values from -60 to 60
- forget_cache: float32 [16, 16384], P('tp'), may hold values from -2460 to 0, as said below
- heads_gain: float32 [1024], replicated, may hold values from 0.1 to 1.9
- output_weight: bfloat16 [1024, 2048], replicated, may hold values from -0.1875 to 0.1875
- expert_tokens: bfloat16 [4096, 2048], P('ep'), may hold values from -600 to 600
- expert_gain: float32 [2048], replicated, may hold values from 0.1 to 1.9
- routes: int32 [4096, 4], P('ep'), may hold values from 0 to 31, all different within a row; in each aligned block of 128 rows (0 to 127, 128 to 255, ...) at most 32 rows name the same one
- route_logits: float32 [4096, 4], P('ep'), may hold values from -6 to 301
- gate_weight: bfloat16 [32, 2048, 2048], P('ep', None, 'tp'), may hold values from -0.5 to 0.5
- up_weight: bfloat16 [32, 2048, 2048], P('ep', None, 'tp'), may hold values from -0.5 to 0.5
- down_weight: bfloat16 [32, 2048, 2048], P('ep', 'tp'), may hold values from -0.015625 to 0.015625
Outputs:
- mixer_out: bfloat16 [16384, 2048], P(('ep', 'tp'))
- moe_out: bfloat16 [4096, 2048], P('ep', 'tp')
Inputs may be any that keep to these rules, and one draw needn't show every extreme that they name: `forget_cache`: each row never rises from one position to the next. `routes`: the 4 experts of a row differ. In each aligned block of 128 rows (one device's tokens) no expert is named more than 32 times, so slot is below 32; some expert is named exactly 32 times in some block.
All inputs are finite; a program needn't handle non-finite values.
Results may differ from a plain program's by a relative error of at most 0.017.
Values may be sent and summed in bfloat16 or wider, within the bound.
No kernel may reach another device: no remote copies, remote signals or barrier semaphores. Data moves between devices by JAX's collectives and lax.ppermute only.
A program may use at most 128 MiB of HBM per device.

v0:
```python
import math

import jax
import jax.numpy as jnp
from jax import lax
from jax.sharding import Mesh
from jax.sharding import PartitionSpec as P

HEAD = 64
EP = ("ep_0", "ep_1")
EP_TP = ("ep_0", "ep_1", "tp")


epsilon = 1e-06
clamp_limit = 7.0
sigmoid_slope = 1.702


def gathered_by_axis(array, axes, dim):
    whole = array
    for number in range(len(axes) - 1, -1, -1):
        whole = lax.all_gather(whole, axes[number], axis=dim, tiled=True)
    return whole


def in_blocks(array, dim, devices):
    before, after = (array.shape[:dim], array.shape[dim + 1 :])
    return jnp.moveaxis(array.reshape(*before, devices, -1, *after), dim, 0)


def sent_and_summed(array, axis, dim):
    devices = lax.axis_size(axis)
    parts = lax.all_to_all(in_blocks(array, dim, devices), axis, 0, 0, tiled=True)
    return jnp.sum(parts.astype(jnp.float32), axis=0)


def scaled_rows(values, gain_vector):
    as_float = values.astype(jnp.float32)
    inverse = lax.rsqrt(jnp.mean(as_float * as_float, axis=-1, keepdims=True) + epsilon)
    return (as_float * inverse * gain_vector).astype(jnp.bfloat16)


def assign_slots(routes, experts, capacity):
    row_count, pick_count = routes.shape
    flat_routes = routes.reshape(-1)
    onehot = (flat_routes[:, None] == jnp.arange(experts, dtype=jnp.int32)[None, :]).astype(
        jnp.int32
    )
    earlier = jnp.cumsum(onehot, axis=0) - onehot
    slot_rank = jnp.sum(earlier * onehot, axis=1)
    position = flat_routes * capacity + slot_rank
    owner_row = jnp.arange(row_count * pick_count, dtype=jnp.int32) // pick_count
    slot_token = jnp.full((experts * capacity,), row_count, jnp.int32).at[position].set(owner_row)
    return (position.reshape(row_count, pick_count), slot_token)


def body(
    queries,
    keys_values,
    forget_cache,
    heads_gain,
    output_weight,
    expert_tokens,
    expert_gain,
    routes,
    route_logits,
    gate_weight,
    up_weight,
    down_weight,
):
    row_count = queries.shape[0]
    query_count = queries.shape[1] // HEAD
    key_count = keys_values.shape[1] // (2 * HEAD)
    group_size = query_count // key_count
    offset = lax.axis_index(EP) * row_count
    score_scale = 1.0 / math.sqrt(HEAD)
    count_rows = queries.shape[0]
    segment_positions = offset + jnp.arange(count_rows, dtype=jnp.int32)
    gate_rows = lax.dynamic_slice_in_dim(forget_cache, offset, count_rows, 1)
    segment_bias = gate_rows.T.reshape(count_rows, key_count, group_size, 1)
    segments = [
        (queries.reshape(count_rows, key_count, group_size, HEAD), segment_positions, segment_bias)
    ]
    start_states = tuple(
        [
            (
                jnp.full((grouped.shape[0], key_count, group_size), -jnp.inf, jnp.float32),
                jnp.zeros((grouped.shape[0], key_count, group_size), jnp.float32),
                jnp.zeros((grouped.shape[0], key_count, group_size, HEAD), jnp.float32),
            )
            for grouped, positions, bias in segments
        ]
    )
    piece_rows = gathered_by_axis(keys_values.reshape(row_count, key_count, 2 * HEAD), EP, 0)
    count_rows = piece_rows.shape[0]
    block_width = 512
    blocks = piece_rows.reshape(count_rows // block_width, block_width, key_count, 2 * HEAD)

    def one_block(states, scan_item):
        block_rows, block_index = scan_item
        first_key = block_index * block_width
        key_block = block_rows[:, :, :HEAD]
        value_block = block_rows[:, :, HEAD:]
        key_gate = lax.dynamic_slice_in_dim(forget_cache, first_key, block_width, 1).reshape(
            1, key_count, group_size, block_width
        )
        key_pos = first_key + jnp.arange(block_width, dtype=jnp.int32)
        updated = []
        for (grouped, positions, bias), state in zip(segments, states):

            def take_block(state_in, grouped=grouped, positions=positions, bias=bias):
                running_max, running_sum, weighted = state_in
                scores = (
                    jnp.einsum(
                        "qhgd,khd->qhgk", grouped, key_block, preferred_element_type=jnp.float32
                    )
                    * score_scale
                )
                scores = scores + bias - key_gate
                visible = (key_pos[None, :] <= positions[:, None])[:, None, None, :]
                scores = jnp.where(visible, scores, -jnp.inf)
                new_max = jnp.maximum(running_max, jnp.max(scores, axis=-1))
                safe_max = jnp.where(jnp.isfinite(new_max), new_max, 0.0)
                factor = jnp.exp(running_max - safe_max)
                weights = jnp.exp(scores - safe_max[..., None])
                running_sum = running_sum * factor + jnp.sum(weights, axis=-1)
                weighted = weighted * factor[..., None] + jnp.einsum(
                    "qhgk,khd->qhgd",
                    weights.astype(jnp.bfloat16),
                    value_block,
                    preferred_element_type=jnp.float32,
                )
                return (new_max, running_sum, weighted)

            def keep_state(state_in):
                return state_in

            updated.append(lax.cond(first_key <= positions[-1], take_block, keep_state, state))
        return (tuple(updated), None)

    final_states, _ = lax.scan(
        one_block, start_states, (blocks, jnp.arange(count_rows // block_width, dtype=jnp.int32))
    )
    outputs = [
        (weighted / running_sum[..., None])
        .reshape(running_sum.shape[0], query_count * HEAD)
        .astype(jnp.bfloat16)
        for running_max, running_sum, weighted in final_states
    ]
    attended = outputs[0]
    local_rows = lax.all_to_all(attended, "tp", split_axis=0, concat_axis=1, tiled=True)
    heads_normed = scaled_rows(local_rows, heads_gain)
    mixer_out = jnp.dot(heads_normed, output_weight, preferred_element_type=jnp.float32).astype(
        jnp.bfloat16
    )
    experts_count = lax.axis_size(EP)
    expert_rows, pick_count = routes.shape
    capacity = 2 * expert_rows * pick_count // experts_count
    expert_in = scaled_rows(expert_tokens, expert_gain)
    shifted = route_logits - jnp.max(route_logits, axis=1, keepdims=True)
    raised = jnp.exp(shifted)
    route_weight = raised / jnp.sum(raised, axis=1, keepdims=True)
    position, slot_token = assign_slots(routes, experts_count, capacity)
    model_width = expert_in.shape[1]
    part_width = model_width // lax.axis_size("tp")
    gate_local = gate_weight[0]
    up_local = up_weight[0]
    down_local = down_weight[0]
    own_columns = lax.dynamic_slice_in_dim(
        expert_in, lax.axis_index("tp") * part_width, part_width, 1
    )
    padded = jnp.concatenate([own_columns, jnp.zeros((1, part_width), jnp.bfloat16)], axis=0)
    outgoing = jnp.take(padded, slot_token, axis=0).reshape(experts_count, capacity, part_width)
    arrived = lax.all_to_all(outgoing, EP, split_axis=0, concat_axis=0, tiled=True).reshape(
        experts_count * capacity, part_width
    )
    piece_rows = lax.all_gather(arrived, "tp", axis=1, tiled=True)
    gate_sum = jnp.dot(piece_rows, gate_local, preferred_element_type=jnp.float32)
    up_sum = jnp.dot(piece_rows, up_local, preferred_element_type=jnp.float32)
    gate_cut = jnp.minimum(gate_sum, clamp_limit)
    up_cut = jnp.clip(up_sum, -clamp_limit, clamp_limit)
    hidden = ((up_cut + 1.0) * gate_cut * jax.nn.sigmoid(sigmoid_slope * gate_cut)).astype(
        jnp.bfloat16
    )
    expert_out = sent_and_summed(
        lax.dot_general(
            down_local, hidden, (((0,), (1,)), ((), ())), preferred_element_type=jnp.float32
        ).astype(jnp.bfloat16),
        "tp",
        0,
    ).astype(jnp.bfloat16)
    returned = lax.all_to_all(expert_out, EP, split_axis=1, concat_axis=1, tiled=True)
    picked = jnp.take(returned, position.reshape(-1), axis=1).reshape(
        part_width, expert_rows, pick_count
    )
    moe_out = jnp.einsum("crk,rk->rc", picked.astype(jnp.float32), route_weight).astype(
        jnp.bfloat16
    )
    return (mixer_out, moe_out)


def solution(mesh):
    torus = Mesh(mesh.devices.reshape(8, 4, mesh.shape["tp"]), ("ep_0", "ep_1", "tp"))
    return jax.shard_map(
        body,
        mesh=torus,
        in_specs=(
            P(EP, "tp"),
            P(EP, "tp"),
            P("tp", None),
            P(),
            P(),
            P(EP, None),
            P(),
            P(EP, None),
            P(EP, None),
            P(EP, None, "tp"),
            P(EP, None, "tp"),
            P(EP, "tp", None),
        ),
        out_specs=(P(EP_TP, None), P(EP, "tp")),
        check_vma=False,
    )
```

profile of v0, /device:TPU:2, one launch (start us, length us, event | category | flops | bytes accessed | tf_op | source)
XLA Modules:
  0.0 385.4 jit_solution(9211881118816011675)
XLA Ops:
  7.2 1.2 convert_element_type.73
  8.4 1.2 multiply_reduce_fusion
  11.4 1.2 reduce-window.6
  13.2 2.4 scatter_custom_fusion
  16.6 3.9 %gather_fusion = bf16[1024,256]{1,0:T(8,128)(2,1)S(1)} fusion(bf16[129,256]{1,0:T(8,128)(2,1)S(1)} %concatenate.3, s32[1024]{0:T(1024)S(1)} %fusion.43), kind=kCustom, calls=%fused_computation | custom fusion | bytes 1052672 | tf_op jit(solution)/shard_map/jit(_take)/gather | solution.py:173
  20.8 28.3 %all_to_all.32 = bf16[32,32,256]{2,1,0:T(8,128)(2,1)} all-to-all(bf16[32,32,256]{2,1,0:T(8,128)(2,1)S(1)} %broadcast_select_fusion), channel_id=1, replica_groups=mesh['ep_0'=8,'ep_1'=4,'tp'=8] {'ep_0','ep_1'}, dimensions={0} | all-to-all | bytes 1048576 | tf_op jit(solution)/shard_map/all_to_all | solution.py:174
  49.2 13.8 %all-gather = bf16[2048,128]{1,0:T(8,128)(2,1)} all-gather(bf16[512,128]{1,0:T(8,128)(2,1)S(1)} %copy-done.1), channel_id=2, replica_groups=mesh['ep_0'=8,'ep_1'=4,'tp'=8] {'ep_1'}, dimensions={0}, use_global_device_ids=true | all-gather | bytes 655360 | tf_op jit(solution)/shard_map/all_gather | solution.py:22
  63.1 21.2 %all-gather.5.cloned.1.call-done = bf16[1024,2048]{1,0:T(8,128)(2,1)} async-done(((bf16[1024,256]{1,0:T(8,128)(2,1)}), bf16[1024,2048]{1,0:T(8,128)(2,1)}) %all-gather.5.cloned.1.call-update) | async-done | bytes 4194320 | tf_op jit(solution)/shard_map/all_gather | solution.py:177
  84.3 4.5 %convolution_minimum_fusion = f32[1024,256]{1,0:T(8,128)} fusion(bf16[1024,2048]{1,0:T(8,128)(2,1)} %all-gather.5.cloned.1.call-done, bf16[1,2048,256]{2,1,0:T(8,128)(2,1)S(1)} %copy-done.6), kind=kOutput, calls=%fused_computation.29 | convolution fusion | flops 1074003968 | bytes 6291456 | tf_op jit(solution)/shard_map/dot_general | solution.py:178
  88.8 8.8 %convolution_convert_fusion = bf16[1024,2048]{1,0:T(8,128)(2,1)} fusion(f32[1024,256]{1,0:T(8,128)} %convolution_minimum_fusion, bf16[1024,2048]{1,0:T(8,128)(2,1)} %all-gather.5.cloned.1.call-done, bf16[1,256,2048]{2,1,0:T(8,128)(2,1)S(1)} %copy-done, bf16[1,2048,256]{2,1,0:T(8,128)(2,1)S(1)} %copy-done.7), kind=kOutput, calls=%fused_computation.27 | convolution fusion | flops 2151940096 | bytes 11534336 | tf_op jit(solution)/shard_map/dot_general | solution.py:186
  97.7 4.6 %copy.58 = bf16[128,8,8,256]{3,2,0,1:T(8,128)(2,1)} copy(bf16[128,8,8,256]{3,2,1,0:T(8,128)(2,1)} %bitcast.128) | data formatting | bytes 8388608 | tf_op jit(solution)/shard_map/reshape | solution.py:28
  102.3 4.7 %all-to-all-start.2 = ((bf16[8,256,1024]{1,2,0:T(8,128)(2,1)}), bf16[8,256,1024]{1,2,0:T(8,128)(2,1)}, u32[]{:S(2)}, u32[]{:S(2)}) async-start(bf16[8,256,1024]{1,2,0:T(8,128)(2,1)} %bitcast.125), calls=%async_computation.2 | async-start | bytes 8388608 | tf_op jit(solution)/shard_map/all_to_all | solution.py:33
  108.0 33.8 %all-gather.7.cloned.1.call-done = bf16[16384,128]{1,0:T(8,128)(2,1)} async-done(((bf16[2048,128]{1,0:T(8,128)(2,1)}), bf16[16384,128]{1,0:T(8,128)(2,1)}) %all-gather.7.cloned.1.call-update) | async-done | bytes 4194320 | tf_op jit(solution)/shard_map/all_gather | solution.py:22
  141.8 6.5 %copy.37 = bf16[32,512,1,128]{1,3,2,0:T(8,128)(2,1)} copy(bf16[32,512,1,128]{3,1,0,2:T(8,128)(2,1)} %bitcast.127) | data formatting | bytes 8388608 | tf_op jit(solution)/shard_map/while | solution.py:141
  148.4 87.1 %while.14 = (s32[]{:T(128)}, f32[512,1,2]{0,2,1:T(2,128)S(1)}, f32[512,1,2]{0,2,1:T(2,128)S(1)}, f32[512,1,2,64]{0,3,2,1:T(8,128)S(1)}, s32[32]{0:T(128)S(1)}, /...) while((s32[]{:T(128)}, f32[512,1,2]{0,2,1:T(2,128)S(1)}, ...), condition=%wide.region_5.6_spmd, body=%wide.region_0.5_spmd.sunk | while | flops 139339264 | bytes 7965025 | solution.py:141
  150.9 3.6 conditional.2
  156.9 3.6 conditional.2
  236.6 4.3 %all-to-all-start = ((bf16[8,64,128]{2,1,0:T(8,128)(2,1)}), bf16[8,64,128]{2,1,0:T(8,128)(2,1)S(1)}, u32[]{:S(2)}, u32[]{:S(2)}) async-start(bf16[8,64,128]{2,1,0:T(8,128)(2,1)} %copy.38), calls=%async_computation | async-start | bytes 262144 | tf_op jit(solution)/shard_map/all_to_all | solution.py:151
  241.1 3.7 reduce_sum.68
  244.8 2.2 all-to-all-done
  247.0 111.8 %all-to-all-start.3 = ((bf16[256,32,32]{0,2,1:T(8,128)(2,1)}), bf16[256,32,32]{0,2,1:T(8,128)(2,1)S(1)}, u32[]{:S(2)}, u32[]{:S(2)}) async-start(bf16[256,32,32]{0,2,1:T(8,128)(2,1)} %bitcast.33), calls=%async_computation.3 | async-start | bytes 1048576 | tf_op jit(solution)/shard_map/all_to_all | solution.py:192
  359.2 3.8 convolution_convert_fusion.1
  363.0 12.5 %all-to-all-done.3 = bf16[256,32,32]{0,2,1:T(8,128)(2,1)S(1)} async-done(((bf16[256,32,32]{0,2,1:T(8,128)(2,1)}), bf16[256,32,32]{0,2,1:T(8,128)(2,1)S(1)}, u32[]{:S(2)}, u32[]{:S(2)}) %all-to-all-start.3) | async-done | bytes 524320 | tf_op jit(solution)/shard_map/all_to_all | solution.py:192
  375.5 1.9 gather_fusion.1
  (214 shorter events, 52.3 us)
Async XLA Ops:
  7.2 81.7 %copy-start = (bf16[1,256,2048]{2,1,0:T(8,128)(2,1)S(1)}, bf16[1,256,2048]{2,1,0:T(8,128)(2,1)}, u32[]{:S(2)}) copy-start(bf16[1,256,2048]{2,1,0:T(8,128)(2,1)} %param.27) | copy-start | bytes 3145732
  7.2 77.1 %all-gather.5.cloned.1.call-start = ((), (), s32[]{:S(2)}) async-start(), calls=%async_computation.4 | async-start | bytes 4718592 | tf_op jit(solution)/shard_map/all_gather | solution.py:177
  10.5 38.8 %copy-start.1 = (bf16[512,128]{1,0:T(8,128)(2,1)S(1)}, bf16[512,128]{1,0:T(8,128)(2,1)}, u32[]{:S(2)}) copy-start(bf16[512,128]{1,0:T(8,128)(2,1)} %param.17) | copy-start | bytes 393220
  16.6 67.7 %copy-start.6 = (bf16[1,2048,256]{2,1,0:T(8,128)(2,1)S(1)}, bf16[1,2048,256]{2,1,0:T(8,128)(2,1)}, u32[]{:S(2)}) copy-start(bf16[1,2048,256]{2,1,0:T(8,128)(2,1)} %param.25) | copy-start | bytes 3145732
  49.2 39.7 %copy-start.7 = (bf16[1,2048,256]{2,1,0:T(8,128)(2,1)S(1)}, bf16[1,2048,256]{2,1,0:T(8,128)(2,1)}, u32[]{:S(2)}) copy-start(bf16[1,2048,256]{2,1,0:T(8,128)(2,1)} %param.26) | copy-start | bytes 3145732
  49.2 92.7 %all-gather.7.cloned.1.call-start = ((), (), s32[]{:S(2)}) async-start(), calls=%async_computation.5 | async-start | bytes 4718592 | tf_op jit(solution)/shard_map/all_gather | solution.py:22
  102.3 4.8 %copy-start.2 = (bf16[512,128]{1,0:T(8,128)(2,1)S(1)}, bf16[512,128]{1,0:T(8,128)(2,1)}, u32[]{:S(2)}) copy-start(bf16[512,128]{1,0:T(8,128)(2,1)} %param.16) | copy-start | bytes 393220
  102.3 134.3 %all-to-all-start.2 = ((bf16[8,256,1024]{1,2,0:T(8,128)(2,1)}), bf16[8,256,1024]{1,2,0:T(8,128)(2,1)}, u32[]{:S(2)}, u32[]{:S(2)}) async-start(bf16[8,256,1024]{1,2,0:T(8,128)(2,1)} %bitcast.125), calls=%async_computation.2 | async-start | bytes 8388608 | tf_op jit(solution)/shard_map/all_to_all | solution.py:33
  148.4 92.5 %copy-start.3 = (s32[128,4]{0,1:T(4,128)S(1)}, s32[128,4]{0,1:T(4,128)}, u32[]{:S(2)}) copy-start(s32[128,4]{0,1:T(4,128)} %param.23) | copy-start | bytes 6148
  148.4 92.7 %copy-start.4 = (f32[128,4]{0,1:T(4,128)S(1)}, f32[128,4]{0,1:T(4,128)}, u32[]{:S(2)}) copy-start(f32[128,4]{0,1:T(4,128)} %param.24) | copy-start | bytes 6148
  235.5 123.6 %copy-start.5 = (f32[1024]{0:T(1024)S(1)}, f32[1024]{0:T(1024)}, u32[]{:S(2)}) copy-start(f32[1024]{0:T(1024)} %param.19) | copy-start | bytes 12292
  236.6 10.4 %all-to-all-start = ((bf16[8,64,128]{2,1,0:T(8,128)(2,1)}), bf16[8,64,128]{2,1,0:T(8,128)(2,1)S(1)}, u32[]{:S(2)}, u32[]{:S(2)}) async-start(bf16[8,64,128]{2,1,0:T(8,128)(2,1)} %copy.38), calls=%async_computation | async-start | bytes 262144 | tf_op jit(solution)/shard_map/all_to_all | solution.py:151
  247.0 128.5 %all-to-all-start.3 = ((bf16[256,32,32]{0,2,1:T(8,128)(2,1)}), bf16[256,32,32]{0,2,1:T(8,128)(2,1)S(1)}, u32[]{:S(2)}, u32[]{:S(2)}) async-start(bf16[256,32,32]{0,2,1:T(8,128)(2,1)} %bitcast.33), calls=%async_computation.3 | async-start | bytes 1048576 | tf_op jit(solution)/shard_map/all_to_all | solution.py:192
Sparse Core Ops, SparseCore 0:
  49.3 34.9 all-gather.4
  86.1 55.6 all-gather.6
where the time goes:
time: 388 us; the launch traced here: 385 us
  starting transfers between devices  121 us (31%)
  waiting for transfers between devices  69.8 us (18%)
  local copies, waits for them, and re-layouts  65.9 us (17%)
  loops' own time  42.4 us (11%)
  blocking collectives  42.2 us (11%)
  matrix products  20 us (5%)
  between operations  14.3 us (4%)
  other arithmetic  9.81 us (3%)
    all_to_all x1, starting transfers between devices, body(): lax.all_to_all(expert_out, EP, split_axis=1, concat_axis=1, tiled=True)  112 us
    another operation x1, loops' own time, body(): lax.scan(one_block, start_states, (blocks, jnp.arange(count_rows // block...  41.9 us
    all_gather x1, waiting for transfers between devices, gathered_by_axis(): whole = lax.all_gather(whole, axes[number], axis=dim, tiled=True)  33.8 us
    all_to_all x1, blocking collectives, body(): lax.all_to_all(outgoing, EP, split_axis=0, concat_axis=0, tiled=True)  28.3 us
    all_gather x1, waiting for transfers between devices, body(): piece_rows = lax.all_gather(arrived, 'tp', axis=1, tiled=True)  21.2 us
    slice x32, local copies, waits for them, and re-layouts, one_block(): positions[-1]  18.9 us
    dynamic_slice x32, local copies, waits for them, and re-layouts, body(): lax.scan(one_block, start_states, (blocks, jnp.arange(count_rows // block...  18.8 us
    all_gather x1, blocking collectives, gathered_by_axis(): whole = lax.all_gather(whole, axes[number], axis=dim, tiled=True)  13.8 us
  transfers between devices with their start and end apart: 5, of which 4 were waited for; matrix products, arithmetic and copies ran while one was open for 21% of the time, Pallas kernels for 0%

commit v1 on v0

v1 whole, which is shorter than its diff:
```python
import functools

import jax
import jax.numpy as jnp
from jax import lax
from jax.experimental import pallas as pl
from jax.experimental.pallas import tpu as pltpu
from jax.sharding import Mesh
from jax.sharding import PartitionSpec as P

EP = ("z", "x")
TP = ("y", "c")
epsilon = 1e-06
clamp_limit = 7.0
sigmoid_slope = 1.702


def scaled_rows(values, gain_vector):
    as_float = values.astype(jnp.float32)
    inverse = lax.rsqrt(jnp.mean(as_float * as_float, axis=-1, keepdims=True) + epsilon)
    return (as_float * inverse * gain_vector).astype(jnp.bfloat16)


BLK = 512
NEG = -1e30

def pieces_of(values):
    high = values.astype(jnp.bfloat16).astype(jnp.float32)
    rest = values - high
    middle = rest.astype(jnp.bfloat16).astype(jnp.float32)
    return high, middle, rest - middle

def attend_kernel(place, q_ref, kv_ref, fk_ref, fq_ref, o_ref, kaug, vaug, acc, top, knorm):
    step = pl.program_id(0)
    zed, ex = place[0], place[1]
    blocks = kv_ref.shape[0]

    @pl.when(step == 0)
    def _prepare():
        one = jnp.ones((blocks, BLK), jnp.float32)
        rows = [jnp.zeros((64, BLK), jnp.float32)]
        for h in range(2):
            rows += list(pieces_of(-fk_ref[h]))
        rows += [one, one]
        table = jnp.concatenate(rows, axis=0).T
        lane = lax.broadcasted_iota(jnp.int32, (BLK, 128), 1)
        tail = jnp.where(lax.broadcasted_iota(jnp.int32, (16, BLK), 0) == 0, 1.0, 0.0)
        most = jnp.zeros((1, BLK), jnp.float32)
        for b in range(blocks):
            block = kv_ref[b].astype(jnp.float32)
            kaug[b] = jnp.where(
                lane < 64, block, jnp.where((lane & 7) == b, table, 0.0)
            ).astype(jnp.bfloat16)
            turned = block.T
            vaug[b] = jnp.concatenate([turned[64:], tail], axis=0).astype(jnp.bfloat16)
            keys = turned[:64]
            most = jnp.maximum(most, jnp.sum(keys * keys, axis=0, keepdims=True))
        knorm[0] = jnp.max(most)

    q_turned = q_ref[0].astype(jnp.float32).T * 0.125
    q_most = jnp.maximum(
        jnp.max(jnp.sum(q_turned[:64] * q_turned[:64], axis=0, keepdims=True)),
        jnp.max(jnp.sum(q_turned[64:] * q_turned[64:], axis=0, keepdims=True)),
    )
    calm = q_most * knorm[0] <= 1600.0
    qaug = []
    for h in range(2):
        gate = fq_ref[0, h : h + 1]
        high, low, _ = pieces_of(gate)
        on, off = jnp.ones((24, BLK), jnp.float32), jnp.zeros((24, BLK), jnp.float32)
        qaug.append(
            jnp.concatenate(
                [
                    q_turned[64 * h : 64 * h + 64],
                    on if h == 0 else off,
                    on if h == 1 else off,
                    jnp.broadcast_to(high, (8, BLK)),
                    jnp.broadcast_to(low, (8, BLK)),
                ],
                axis=0,
            ).astype(jnp.bfloat16)
        )
    acc[...] = jnp.zeros_like(acc)
    full = zed + jnp.where(ex < step, 1, 0)
    half = BLK // 2

    def take(b, shifted, masked):
        for h in range(2):
            for part in range(2):
                span = slice(part * half, part * half + half)
                scores = jnp.dot(kaug[b], qaug[h][:, span], preferred_element_type=jnp.float32)
                if masked:
                    seen = lax.broadcasted_iota(jnp.int32, (BLK, half), 0) <= (
                        lax.broadcasted_iota(jnp.int32, (BLK, half), 1) + part * half
                    )
                    scores = jnp.where(seen, scores, NEG)
                if shifted:
                    old = top[h, :, span]
                    new = jnp.maximum(old, jnp.max(scores, axis=0, keepdims=True))
                    top[h, :, span] = new
                    acc[h, :, span] = acc[h, :, span] * jnp.exp(old - new)
                    scores = scores - new
                weights = jnp.exp(scores)
                if masked and shifted:
                    weights = jnp.where(seen, weights, 0.0)
                acc[h, :, span] += jnp.dot(
                    vaug[b], weights.astype(jnp.bfloat16), preferred_element_type=jnp.float32
                )

    def sweep(shifted):
        def one(b, carry):
            take(b, shifted, False)
            return carry

        lax.fori_loop(0, full, one, 0)

        @pl.when(ex == step)
        def _edge():
            take(zed, shifted, True)

    @pl.when(calm)
    def _calm():
        top[...] = jnp.zeros_like(top)
        sweep(False)

    @pl.when(jnp.logical_not(calm))
    def _wild():
        top[...] = jnp.full_like(top, NEG)
        sweep(True)

    for h in range(2):
        total = acc[h, 64:65]
        peak = top[h]
        rows = list(pieces_of(total)) + list(pieces_of(peak))
        rows.append(jnp.zeros((10, BLK), jnp.float32))
        o_ref[0, h] = jnp.concatenate([acc[h, :64]] + rows, axis=0).astype(jnp.bfloat16)

def attend(place, q4, kv8, fk, fq):
    n = kv8.shape[0]
    return pl.pallas_call(
        attend_kernel,
        grid_spec=pltpu.PrefetchScalarGridSpec(
            num_scalar_prefetch=1,
            grid=(4,),
            in_specs=[
                pl.BlockSpec((1, BLK, 128), lambda i, p: (i, 0, 0)),
                pl.BlockSpec((n, BLK, 128), lambda i, p: (0, 0, 0)),
                pl.BlockSpec((2, n, BLK), lambda i, p: (0, 0, 0)),
                pl.BlockSpec((1, 2, BLK), lambda i, p: (i, 0, 0)),
            ],
            out_specs=pl.BlockSpec((1, 2, 80, BLK), lambda i, p: (i, 0, 0, 0)),
            scratch_shapes=[
                pltpu.VMEM((n, BLK, 128), jnp.bfloat16),
                pltpu.VMEM((n, 80, BLK), jnp.bfloat16),
                pltpu.VMEM((2, 80, BLK), jnp.float32),
                pltpu.VMEM((2, 1, BLK), jnp.float32),
                pltpu.SMEM((1,), jnp.float32),
            ],
        ),
        out_shape=jax.ShapeDtypeStruct((4, 2, 80, BLK), jnp.bfloat16),
        name="attend",
    )(place, q4, kv8, fk, fq)

def merge_kernel(p_ref, o_ref):
    tops, sums, outs = [], [], []
    for h in range(2):
        peaks, totals = [], []
        for s in range(4):
            side = p_ref[s, h, 64:80].astype(jnp.float32)
            totals.append(side[0:1] + side[1:2] + side[2:3])
            peaks.append(side[3:4] + side[4:5] + side[5:6])
        peak = functools.reduce(jnp.maximum, peaks)
        factors = [jnp.exp(p - peak) for p in peaks]
        total = sum(f * t for f, t in zip(factors, totals))
        value = sum(f * p_ref[s, h, :64].astype(jnp.float32) for s, f in enumerate(factors))
        outs.append(value / total)
    o_ref[...] = jnp.concatenate(outs, axis=0).T.astype(jnp.bfloat16)

def merge(parts):
    return pl.pallas_call(
        merge_kernel,
        out_shape=jax.ShapeDtypeStruct((BLK, 128), jnp.bfloat16),
        name="merge",
    )(parts)

def shift(array, axis, by):
    count = lax.axis_size(axis)
    return lax.ppermute(array, axis, [(i, (i + by) % count) for i in range(count)])


def spread(array, axis):
    count = lax.axis_size(axis)
    return lax.all_to_all(
        jnp.broadcast_to(array[None], (count, *array.shape)), axis, 0, 0, tiled=True
    )


def hidden_kernel(order, *refs):
    pieces, (gate_ref, up_ref, out_ref) = refs[:8], refs[8:]
    gate = up = None
    for n, piece in enumerate(pieces):
        rows = pl.ds(pl.multiple_of(order[n] * 256, 256), 256)
        left = piece[...]
        g = jnp.dot(left, gate_ref[rows, :], preferred_element_type=jnp.float32)
        u = jnp.dot(left, up_ref[rows, :], preferred_element_type=jnp.float32)
        gate, up = (g, u) if n == 0 else (gate + g, up + u)
    gate = jnp.minimum(gate, clamp_limit)
    up = jnp.clip(up, -clamp_limit, clamp_limit)
    out_ref[...] = ((up + 1.0) * gate * jax.nn.sigmoid(sigmoid_slope * gate)).astype(jnp.bfloat16)


def hidden_of(order, pieces, gate_local, up_local):
    rows = pieces[0].shape[0]
    tile = 256
    return pl.pallas_call(
        hidden_kernel,
        grid_spec=pltpu.PrefetchScalarGridSpec(
            num_scalar_prefetch=1,
            grid=(rows // tile,),
            in_specs=[pl.BlockSpec((tile, 256), lambda i, o: (i, 0))] * 8
            + [pl.BlockSpec((2048, 256), lambda i, o: (0, 0))] * 2,
            out_specs=pl.BlockSpec((tile, 256), lambda i, o: (i, 0)),
        ),
        out_shape=jax.ShapeDtypeStruct((rows, 256), jnp.bfloat16),
        name="hidden",
    )(order, *pieces, gate_local, up_local)


def body(
    queries,
    keys_values,
    forget_cache,
    heads_gain,
    output_weight,
    expert_tokens,
    expert_gain,
    routes,
    route_logits,
    gate_weight,
    up_weight,
    down_weight,
):
    zed, ex = lax.axis_index("z"), lax.axis_index("x")
    why, core = lax.axis_index("y"), lax.axis_index("c")
    rank = lax.axis_index(TP)
    rows = routes.shape[0]
    experts, capacity, width = 32, 32, 256

    tokens = expert_tokens.astype(jnp.float32)
    inverse = lax.rsqrt(jnp.mean(tokens * tokens, axis=-1, keepdims=True) + epsilon)
    own = lax.dynamic_slice_in_dim(tokens, rank * width, width, 1)
    own_gain = lax.dynamic_slice_in_dim(expert_gain, rank * width, width, 0)
    own_in = (own * inverse * own_gain).astype(jnp.bfloat16)

    chosen = routes.T[None, :, :] == jnp.arange(experts, dtype=jnp.int32)[:, None, None]
    named = jnp.any(chosen, axis=1)
    number = jnp.arange(rows, dtype=jnp.int32)
    earlier = (number[:, None] < number[None, :]).astype(jnp.bfloat16)
    slot = jnp.dot(named.astype(jnp.bfloat16), earlier, preferred_element_type=jnp.float32)
    slot = jnp.where(named, slot.astype(jnp.int32), -1)
    place = slot[:, None, :] == jnp.arange(capacity, dtype=jnp.int32)[None, :, None]
    onehot = place.astype(jnp.bfloat16).reshape(experts * capacity, rows)
    outgoing = jnp.dot(onehot, own_in, preferred_element_type=jnp.float32).astype(jnp.bfloat16)
    arrived = lax.all_to_all(
        outgoing.reshape(experts, capacity, width), EP, 0, 0, tiled=True
    ).reshape(experts * capacity, width)

    kv, q, arrived = lax.optimization_barrier((keys_values, queries, arrived))
    pieces = [arrived] + [shift(arrived, "y", by) for by in (1, 3, 2)]
    places = [2 * ((why - by) % 4) for by in (0, 1, 3, 2)]
    twins = [shift(piece, "c", 1) for piece in pieces]
    order = jnp.stack([p + core for p in places] + [p + 1 - core for p in places]).astype(jnp.int32)

    kv8 = spread(kv, "z")
    q4 = spread(q, "x")
    gates = forget_cache.reshape(2, 8, 4, BLK)
    fk = lax.dynamic_index_in_dim(gates, ex, 2, keepdims=False)
    fq = lax.dynamic_index_in_dim(gates, zed, 1, keepdims=False).transpose(1, 0, 2)

    hidden = hidden_of(order, pieces + twins, gate_weight[0], up_weight[0])
    down = down_weight[0].reshape(width, 4, 2, width)

    def partial(by, side):
        part = lax.dynamic_slice(
            down, (0, (why + by) % 4, side, 0), (width, 1, 1, width)
        ).reshape(width, width)
        return jnp.dot(hidden, part, preferred_element_type=jnp.float32)

    steps = (2, 1, 3, 0)
    others = [shift(partial(by, 1 - core).astype(jnp.bfloat16), "c", 1) for by in steps]
    pairs = [
        (partial(by, core) + other.astype(jnp.float32)).astype(jnp.bfloat16)
        for by, other in zip(steps, others)
    ]
    moved = [shift(pair, "y", by) if by else pair for by, pair in zip(steps, pairs)]
    expert_out = sum(m.astype(jnp.float32) for m in moved).astype(jnp.bfloat16)

    parts = attend(jnp.stack([zed, ex]).astype(jnp.int32), q4, kv8, fk, fq)
    parts = lax.all_to_all(parts, "x", 0, 0, tiled=True)
    attended = merge(parts)
    local = lax.all_to_all(attended, TP, split_axis=0, concat_axis=1, tiled=True)

    returned = lax.all_to_all(
        expert_out.reshape(experts, capacity, width), EP, 0, 0, tiled=True
    ).reshape(experts * capacity, width)

    heads_normed = scaled_rows(local, heads_gain)
    mixer_out = jnp.dot(heads_normed, output_weight, preferred_element_type=jnp.float32).astype(
        jnp.bfloat16
    )

    shifted = route_logits - jnp.max(route_logits, axis=1, keepdims=True)
    raised = jnp.exp(shifted)
    route_weight = raised / jnp.sum(raised, axis=1, keepdims=True)
    share = jnp.sum(jnp.where(chosen, route_weight.T[None, :, :], 0.0), axis=1)
    high = share.astype(jnp.bfloat16)
    low = (share - high.astype(jnp.float32)).astype(jnp.bfloat16)
    moe = 0.0
    for piece in (high, low):
        table = jnp.where(place, piece[:, None, :], jnp.bfloat16(0)).reshape(-1, rows)
        moe = moe + lax.dot_general(
            table, returned, (((0,), (0,)), ((), ())), preferred_element_type=jnp.float32
        )
    return (mixer_out, moe.astype(jnp.bfloat16))


def solution(mesh):
    torus = Mesh(mesh.devices.reshape(8, 4, 4, 2), ("z", "x", "y", "c"))
    return jax.shard_map(
        body,
        mesh=torus,
        in_specs=(
            P(EP, TP),
            P(EP, TP),
            P(TP, None),
            P(),
            P(),
            P(EP, None),
            P(),
            P(EP, None),
            P(EP, None),
            P(EP, None, TP),
            P(EP, None, TP),
            P(EP, TP, None),
        ),
        out_specs=(P(EP + TP, None), P(EP, TP)),
        check_vma=False,
    )
```

time: 388 us -> 211 us (0.54)
  local copies, waits for them, and re-layouts: 65.9 us -> 7.29 us
  starting transfers between devices: 121 us -> 74 us
  loops' own time: 42.4 us -> 0 us
  Pallas kernels: 0 us -> 18.6 us
  blocking collectives: 42.2 us -> 28.2 us
  between operations: 14.3 us -> 0.97 us
  waiting for transfers between devices: 69.8 us -> 62.7 us
  matrix products: 20 us -> 14 us
  other arithmetic: 9.81 us -> 4.23 us
    all_to_all x3 -> x5, starting transfers between devices: 121 us -> 62.9 us  [the longest x1 45.8 us: body(): lax.all_to_all(expert_out.reshape(experts, capacity, width), EP, 0, 0, ti...]
    all_gather x2 -> x0, waiting for transfers between devices: 55.1 us -> none  [the longest x1 33.8 us: gathered_by_axis(): whole = lax.all_gather(whole, axes[number], axis=dim, tiled=True)]
    another operation x33 -> x0, loops' own time: 42.4 us -> none  [the longest x1 41.9 us: body(): lax.scan(one_block, start_states, (blocks, jnp.arange(count_rows // block...]
    all_to_all x3 -> x5, waiting for transfers between devices: 14.7 us -> 41.8 us  [the longest x2 16 us: spread(): lax.all_to_all(jnp.broadcast_to(array[None], (count, *array.shape)), axis...]
    ppermute x0 -> x14, waiting for transfers between devices: none -> 21 us  [shift(): lax.ppermute(array, axis, [(i, (i + by) % count) for i in range(count)])]
    dynamic_slice x35 -> x2, local copies, waits for them, and re-layouts: 21.1 us -> 0.8 us  [the longest x1 0.77 us: body(): own_gain = lax.dynamic_slice_in_dim(expert_gain, rank * width, width, 0)]
    slice x33 -> x0, local copies, waits for them, and re-layouts: 19.1 us -> none  [the longest x32 18.9 us: one_block(): positions[-1]]
    pallas_call x0 -> x3, Pallas kernels: none -> 18.6 us  [the longest x1 9.54 us: attend(): pl.pallas_call(attend_kernel, grid_spec=pltpu.PrefetchScalarGridSpec(num_...]
  transfers between devices with their start and end apart: 5 -> 19, of which waited for: 4 -> 7; matrix products, arithmetic and copies ran while one was open for 21% -> 8% of each run, Pallas kernels for 0% -> 9%
where the time goes in v1:
time: 211 us; the launch traced here: 210 us
  starting transfers between devices  74 us (35%)
  waiting for transfers between devices  62.7 us (30%)
  blocking collectives  28.2 us (13%)
  Pallas kernels  18.6 us (9%)
  matrix products  14 us (7%)
  local copies, waits for them, and re-layouts  7.29 us (3%)
  other arithmetic  4.23 us (2%)
    all_to_all x1, starting transfers between devices, body(): lax.all_to_all(expert_out.reshape(experts, capacity, width), EP, 0, 0, ti...  45.8 us
    all_to_all x1, blocking collectives, body(): lax.all_to_all(outgoing.reshape(experts, capacity, width), EP, 0, 0, tile...  28.2 us
    ppermute x14, waiting for transfers between devices, shift(): lax.ppermute(array, axis, [(i, (i + by) % count) for i in range(count)])  21 us
    all_to_all x2, waiting for transfers between devices, spread(): lax.all_to_all(jnp.broadcast_to(array[None], (count, *array.shape)), axis...  16 us
    all_to_all x1, waiting for transfers between devices, body(): lax.all_to_all(expert_out.reshape(experts, capacity, width), EP, 0, 0, ti...  12.7 us
    ppermute x14, starting transfers between devices, shift(): lax.ppermute(array, axis, [(i, (i + by) % count) for i in range(count)])  11.2 us
    all_to_all x1, waiting for transfers between devices, body(): parts = lax.all_to_all(parts, 'x', 0, 0, tiled=True)  9.83 us
    pallas_call x1, Pallas kernels, attend(): pl.pallas_call(attend_kernel, grid_spec=pltpu.PrefetchScalarGridSpec(num_...  9.54 us
  transfers between devices with their start and end apart: 19, of which 7 were waited for; matrix products, arithmetic and copies ran while one was open for 8% of the time, Pallas kernels for 9%

profile of v1, /device:TPU:2, one launch (start us, length us, event | category | flops | bytes accessed | tf_op | source)
XLA Modules:
  0.0 210.0 jit_solution(4290597664380940284)
XLA Ops:
  5.4 28.2 %all_to_all.38 = bf16[32,32,256]{2,1,0:T(8,128)(2,1)S(1)} all-to-all(bf16[32,32,256]{2,1,0:T(8,128)(2,1)S(1)} %bitcast.103), channel_id=1, replica_groups=mesh['z'=8,'x'=4,'y'=4,'c'=2] {'z','x'}, dimensions={0} | all-to-all | bytes 1048576 | tf_op jit(solution)/shard_map/all_to_all | solution.py:264
  33.7 1.6 collective-permute-start
  35.2 1.7 collective-permute-start.1
  36.9 2.0 collective-permute-start.2
  38.9 9.8 %collective-permute-done.refs_1_ = bf16[1024,256]{1,0:T(8,128)(2,1)} collective-permute-done((bf16[1024,256]{1,0:T(8,128)(2,1)S(1)}, bf16[1024,256]{1,0:T(8,128)(2,1)}, u32[]{:S(2)}, u32[]{:S(2)}) %collective-permute-start) | collective-permute-done | bytes 524320 | tf_op jit(solution)/shard_map/ppermute | solution.py:188
  48.7 1.5 collective-permute-done.1.refs_2_
  50.2 9.7 %collective-permute-done.2.refs_3_ = bf16[1024,256]{1,0:T(8,128)(2,1)} collective-permute-done((bf16[1024,256]{1,0:T(8,128)(2,1)S(1)}, bf16[1024,256]{1,0:T(8,128)(2,1)}, u32[]{:S(2)}, u32[]{:S(2)}) %collective-permute-start.2) | collective-permute-done | bytes 524320 | tf_op jit(solution)/shard_map/ppermute | solution.py:188
  60.7 4.7 %all-to-all-start.1 = ((bf16[4,512,128]{2,1,0:T(8,128)(2,1)}), bf16[4,512,128]{2,1,0:T(8,128)(2,1)S(1)}, u32[]{:S(2)}, u32[]{:S(2)}) async-start(bf16[4,512,128]{2,1,0:T(8,128)(2,1)} %broadcast_in_dim.35), calls=%async_computation.1 | async-start | bytes 1048576 | tf_op jit(solution)/shard_map/all_to_all | solution.py:193
  67.5 7.0 %hidden.1 = bf16[1024,256]{1,0:T(8,128)(2,1)} custom-call(s32[8]{0:T(128)} %stack.47.order, bf16[1024,256]{1,0:T(8,128)(2,1)} %bitcast.108, bf16[1024,256]{1,0:T(8,128)(2,1)} %collective-permute-done.refs_1_, bf16[1024,256]{1,0:T(8,128)(2,1)} %collective-permute-done.1.refs_2_, bf16[1024,256]{1,0:T(8,128)(2,1)} %collective-permute-done.2.refs_3_, ...), custom_call_target="tpu_custom_call" | custom-call | tf_op jit(solution)/shard_map/hidden/pallas_call | solution.py:215
  75.7 3.6 %all-to-all-start.2 = ((bf16[8,512,128]{2,1,0:T(8,128)(2,1)}), bf16[8,512,128]{2,1,0:T(8,128)(2,1)S(1)}, u32[]{:S(2)}, u32[]{:S(2)}) async-start(bf16[8,512,128]{2,1,0:T(8,128)(2,1)} %broadcast_in_dim.40), calls=%async_computation.2 | async-start | bytes 2097152 | tf_op jit(solution)/shard_map/all_to_all | solution.py:193
  79.2 1.4 convolution_convert_fusion.4
  86.5 1.9 collective-permute-start.10
  89.5 1.4 collective-permute-start.12
  92.3 16.0 %all-to-all-done.2.kv_ref = bf16[8,512,128]{2,1,0:T(8,128)(2,1)S(1)} async-done(((bf16[8,512,128]{2,1,0:T(8,128)(2,1)}), bf16[8,512,128]{2,1,0:T(8,128)(2,1)S(1)}, u32[]{:S(2)}, u32[]{:S(2)}) %all-to-all-start.2) | async-done | bytes 1048608 | tf_op jit(solution)/shard_map/all_to_all | solution.py:193
  109.3 9.5 %attend.1 = bf16[4,2,80,512]{3,2,1,0:T(8,128)(2,1)} custom-call(s32[2]{0:T(128)} %pad_add_fusion.place, bf16[4,512,128]{2,1,0:T(8,128)(2,1)} %copy-done.3, bf16[8,512,128]{2,1,0:T(8,128)(2,1)} %copy-done.1, f32[2,8,512]{2,1,0:T(8,128)} %bitcast.113, f32[4,2,512]{2,1,0:T(2,128)} %dynamic-slice_bitcast_fusion.fq_ref), custom_call_target="tpu_custom_call" | custom-call | tf_op jit(solution)/shard_map/attend/pallas_call | solution.py:140
  118.8 5.5 %all-to-all-start.3 = ((bf16[4,2,80,512]{3,2,1,0:T(8,128)(2,1)}), bf16[4,2,80,512]{3,2,1,0:T(8,128)(2,1)S(1)}, u32[]{:S(2)}, u32[]{:S(2)}) async-start(bf16[4,2,80,512]{3,2,1,0:T(8,128)(2,1)} %attend.1), calls=%async_computation.3 | async-start | bytes 1310720 | tf_op jit(solution)/shard_map/all_to_all | solution.py:299
  124.4 9.8 %all-to-all-done.3.p_ref = bf16[4,2,80,512]{3,2,1,0:T(8,128)(2,1)S(1)} async-done(((bf16[4,2,80,512]{3,2,1,0:T(8,128)(2,1)}), bf16[4,2,80,512]{3,2,1,0:T(8,128)(2,1)S(1)}, u32[]{:S(2)}, u32[]{:S(2)}) %all-to-all-start.3) | async-done | bytes 655392 | tf_op jit(solution)/shard_map/all_to_all | solution.py:299
  135.1 2.0 merge.1
  137.0 3.4 %all-to-all-start.4 = ((bf16[8,64,128]{2,1,0:T(8,128)(2,1)}), bf16[8,64,128]{2,1,0:T(8,128)(2,1)S(1)}, u32[]{:S(2)}, u32[]{:S(2)}) async-start(bf16[8,64,128]{2,1,0:T(8,128)(2,1)} %bitcast.111), calls=%async_computation.4 | async-start | bytes 262144 | tf_op jit(solution)/shard_map/all_to_all | solution.py:301
  140.5 2.7 %fusion.6 = bf16[1024,256]{1,0:T(8,128)(2,1)} fusion(bf16[1024,256]{1,0:T(8,128)(2,1)S(1)} %copy-done, bf16[1024,256]{1,0:T(8,128)(2,1)} %collective-permute-done.13, bf16[1024,256]{1,0:T(8,128)(2,1)} %collective-permute-done.12, bf16[1024,256]{1,0:T(8,128)(2,1)} %collective-permute-done.10, bf16[1024,256]{1,0:T(8,128)(2,1)} %collective-permute-done.8, ...), kind=kOutput, calls=%fused_computation.15 | convolution fusion | flops 137101312 | bytes 3276808 | tf_op jit(solution)/shard_map/dot_general | solution.py:287
  143.2 3.2 %all-to-all-done.4 = bf16[8,64,128]{2,1,0:T(8,128)(2,1)S(1)} async-done(((bf16[8,64,128]{2,1,0:T(8,128)(2,1)}), bf16[8,64,128]{2,1,0:T(8,128)(2,1)S(1)}, u32[]{:S(2)}, u32[]{:S(2)}) %all-to-all-start.4) | async-done | bytes 131104 | tf_op jit(solution)/shard_map/all_to_all | solution.py:301
  146.4 45.8 %all-to-all-start.5 = ((bf16[32,32,256]{2,1,0:T(8,128)(2,1)}), bf16[32,32,256]{2,1,0:T(8,128)(2,1)S(1)}, u32[]{:S(2)}, u32[]{:S(2)}) async-start(bf16[32,32,256]{2,1,0:T(8,128)(2,1)} %bitcast.32), calls=%async_computation.5 | async-start | bytes 1048576 | tf_op jit(solution)/shard_map/all_to_all | solution.py:303
  192.4 3.8 %convolution_convert_fusion = bf16[64,2048]{1,0:T(8,128)(2,1)} fusion(bf16[1024,2048]{1,0:T(8,128)(2,1)} %param.16, f32[1024]{0:T(1024)S(1)} %copy-done.11, f32[64]{0:T(128)S(1)} %add_rsqrt_fusion, bf16[8,64,128]{2,1,0:T(8,128)(2,1)S(1)} %all-to-all-done.4), kind=kOutput, calls=%fused_computation | convolution fusion | flops 268828672 | bytes 4591872 | tf_op jit(solution)/shard_map/dot_general | solution.py:308
  196.2 12.7 %all-to-all-done.5 = bf16[32,32,256]{2,1,0:T(8,128)(2,1)S(1)} async-done(((bf16[32,32,256]{2,1,0:T(8,128)(2,1)}), bf16[32,32,256]{2,1,0:T(8,128)(2,1)S(1)}, u32[]{:S(2)}, u32[]{:S(2)}) %all-to-all-start.5) | async-done | bytes 524320 | tf_op jit(solution)/shard_map/all_to_all | solution.py:303
  (79 shorter events, 20.3 us)
Async XLA Ops:
  0.6 59.2 %copy-start.7 = (bf16[512,128]{1,0:T(8,128)(2,1)S(1)}, bf16[512,128]{1,0:T(8,128)(2,1)}, u32[]{:S(2)}) copy-start(bf16[512,128]{1,0:T(8,128)(2,1)} %param.12) | copy-start | bytes 393220
  0.6 64.7 %copy-start.5 = (bf16[1,256,2048]{2,1,0:T(8,128)(2,1)S(1)}, bf16[1,256,2048]{2,1,0:T(8,128)(2,1)}, u32[]{:S(2)}) copy-start(bf16[1,256,2048]{2,1,0:T(8,128)(2,1)} %param.23) | copy-start | bytes 3145732
  0.6 65.3 %copy-start.6 = (f32[2,16384]{1,0:T(2,128)S(1)}, f32[2,16384]{1,0:T(2,128)}, u32[]{:S(2)}) copy-start(f32[2,16384]{1,0:T(2,128)} %param.14) | copy-start | bytes 393220
  33.7 15.0 %collective-permute-start = (bf16[1024,256]{1,0:T(8,128)(2,1)S(1)}, bf16[1024,256]{1,0:T(8,128)(2,1)}, u32[]{:S(2)}, u32[]{:S(2)}) collective-permute-start(bf16[1024,256]{1,0:T(8,128)(2,1)S(1)} %bitcast.104), channel_id=1, source_target_pairs={{0,2},{2,4},{4,6},{6,0},{1,3},{3,5},{5,7},{7,1},{8,10},{10,12},{12... | collective-permute-start | bytes 1572872 | tf_op jit(solution)/shard_map/ppermute | solution.py:188
  35.2 14.9 %collective-permute-start.1 = (bf16[1024,256]{1,0:T(8,128)(2,1)S(1)}, bf16[1024,256]{1,0:T(8,128)(2,1)}, u32[]{:S(2)}, u32[]{:S(2)}) collective-permute-start(bf16[1024,256]{1,0:T(8,128)(2,1)S(1)} %bitcast.105), channel_id=1, source_target_pairs={{0,6},{2,0},{4,2},{6,4},{1,7},{3,1},{5,3},{7,5},{8,14},{10,8},{12,... | collective-permute-start | bytes 1572872 | tf_op jit(solution)/shard_map/ppermute | solution.py:188
  36.9 22.9 %collective-permute-start.2 = (bf16[1024,256]{1,0:T(8,128)(2,1)S(1)}, bf16[1024,256]{1,0:T(8,128)(2,1)}, u32[]{:S(2)}, u32[]{:S(2)}) collective-permute-start(bf16[1024,256]{1,0:T(8,128)(2,1)S(1)} %bitcast.106), channel_id=1, source_target_pairs={{0,4},{2,6},{4,0},{6,2},{1,5},{3,7},{5,1},{7,3},{8,12},{10,14},{12... | collective-permute-start | bytes 1572872 | tf_op jit(solution)/shard_map/ppermute | solution.py:188
  38.9 28.5 %collective-permute-start.3 = (bf16[1024,256]{1,0:T(8,128)(2,1)S(1)}, bf16[1024,256]{1,0:T(8,128)(2,1)}, u32[]{:S(2)}, u32[]{:S(2)}) collective-permute-start(bf16[1024,256]{1,0:T(8,128)(2,1)S(1)} %bitcast.107), channel_id=1, source_target_pairs={{0,1},{1,0},{2,3},{3,2},{4,5},{5,4},{6,7},{7,6},{8,9},{9,8},{10,11... | collective-permute-start | bytes 1572872 | tf_op jit(solution)/shard_map/ppermute | solution.py:188
  48.7 18.8 %collective-permute-start.4 = (bf16[1024,256]{1,0:T(8,128)(2,1)}, bf16[1024,256]{1,0:T(8,128)(2,1)}, u32[]{:S(2)}, u32[]{:S(2)}) collective-permute-start(bf16[1024,256]{1,0:T(8,128)(2,1)} %collective-permute-done.refs_1_), channel_id=1, source_target_pairs={{0,1},{1,0},{2,3},{3,2},{4,5},{5,4},{6,7},{7,6},{8,9},{9,8},{10,11... | collective-permute-start | bytes 1572872 | tf_op jit(solution)/shard_map/ppermute | solution.py:188
  50.1 17.3 %collective-permute-start.5 = (bf16[1024,256]{1,0:T(8,128)(2,1)}, bf16[1024,256]{1,0:T(8,128)(2,1)}, u32[]{:S(2)}, u32[]{:S(2)}) collective-permute-start(bf16[1024,256]{1,0:T(8,128)(2,1)} %collective-permute-done.1.refs_2_), channel_id=1, source_target_pairs={{0,1},{1,0},{2,3},{3,2},{4,5},{5,4},{6,7},{7,6},{8,9},{9,8},{10,11... | collective-permute-start | bytes 1572872 | tf_op jit(solution)/shard_map/ppermute | solution.py:188
  59.8 7.6 %collective-permute-start.6 = (bf16[1024,256]{1,0:T(8,128)(2,1)}, bf16[1024,256]{1,0:T(8,128)(2,1)}, u32[]{:S(2)}, u32[]{:S(2)}) collective-permute-start(bf16[1024,256]{1,0:T(8,128)(2,1)} %collective-permute-done.2.refs_3_), channel_id=1, source_target_pairs={{0,1},{1,0},{2,3},{3,2},{4,5},{5,4},{6,7},{7,6},{8,9},{9,8},{10,11... | collective-permute-start | bytes 1572872 | tf_op jit(solution)/shard_map/ppermute | solution.py:188
  60.7 13.8 %all-to-all-start.1 = ((bf16[4,512,128]{2,1,0:T(8,128)(2,1)}), bf16[4,512,128]{2,1,0:T(8,128)(2,1)S(1)}, u32[]{:S(2)}, u32[]{:S(2)}) async-start(bf16[4,512,128]{2,1,0:T(8,128)(2,1)} %broadcast_in_dim.35), calls=%async_computation.1 | async-start | bytes 1048576 | tf_op jit(solution)/shard_map/all_to_all | solution.py:193
  75.7 32.6 %all-to-all-start.2 = ((bf16[8,512,128]{2,1,0:T(8,128)(2,1)}), bf16[8,512,128]{2,1,0:T(8,128)(2,1)S(1)}, u32[]{:S(2)}, u32[]{:S(2)}) async-start(bf16[8,512,128]{2,1,0:T(8,128)(2,1)} %broadcast_in_dim.40), calls=%async_computation.2 | async-start | bytes 2097152 | tf_op jit(solution)/shard_map/all_to_all | solution.py:193
  80.6 3.1 %collective-permute-start.7 = (bf16[1024,256]{1,0:T(8,128)(2,1)S(1)}, bf16[1024,256]{1,0:T(8,128)(2,1)S(1)}, u32[]{:S(2)}, u32[]{:S(2)}) collective-permute-start(bf16[1024,256]{1,0:T(8,128)(2,1)S(1)} %convolution_convert_fusion.4), channel_id=1, source_target_pairs={{0,1},{1,0},{2,3},{3,2},{4,5},{5,4},{6,7},{7,6},{8,9},{9,8},{10,11... | collective-permute-start | bytes 1572872 | tf_op jit(solution)/shard_map/ppermute | solution.py:188
  81.1 5.1 %collective-permute-start.9 = (bf16[1024,256]{1,0:T(8,128)(2,1)S(1)}, bf16[1024,256]{1,0:T(8,128)(2,1)S(1)}, u32[]{:S(2)}, u32[]{:S(2)}) collective-permute-start(bf16[1024,256]{1,0:T(8,128)(2,1)S(1)} %convolution_convert_fusion.3), channel_id=1, source_target_pairs={{0,1},{1,0},{2,3},{3,2},{4,5},{5,4},{6,7},{7,6},{8,9},{9,8},{10,11... | collective-permute-start | bytes 1572872 | tf_op jit(solution)/shard_map/ppermute | solution.py:188
  82.0 6.4 %collective-permute-start.11 = (bf16[1024,256]{1,0:T(8,128)(2,1)S(1)}, bf16[1024,256]{1,0:T(8,128)(2,1)S(1)}, u32[]{:S(2)}, u32[]{:S(2)}) collective-permute-start(bf16[1024,256]{1,0:T(8,128)(2,1)S(1)} %convolution_convert_fusion.2), channel_id=1, source_target_pairs={{0,1},{1,0},{2,3},{3,2},{4,5},{5,4},{6,7},{7,6},{8,9},{9,8},{10,11... | collective-permute-start | bytes 1572872 | tf_op jit(solution)/shard_map/ppermute | solution.py:188
  83.2 57.2 %collective-permute-start.13 = (bf16[1024,256]{1,0:T(8,128)(2,1)}, bf16[1024,256]{1,0:T(8,128)(2,1)}, u32[]{:S(2)}, u32[]{:S(2)}) collective-permute-start(bf16[1024,256]{1,0:T(8,128)(2,1)} %convolution_convert_fusion.1), channel_id=1, source_target_pairs={{0,1},{1,0},{2,3},{3,2},{4,5},{5,4},{6,7},{7,6},{8,9},{9,8},{10,11... | collective-permute-start | bytes 1572872 | tf_op jit(solution)/shard_map/ppermute | solution.py:188
  84.8 55.6 %collective-permute-start.8 = (bf16[1024,256]{1,0:T(8,128)(2,1)}, bf16[1024,256]{1,0:T(8,128)(2,1)}, u32[]{:S(2)}, u32[]{:S(2)}) collective-permute-start(bf16[1024,256]{1,0:T(8,128)(2,1)} %fusion), channel_id=1, source_target_pairs={{0,4},{2,6},{4,0},{6,2},{1,5},{3,7},{5,1},{7,3},{8,12},{10,14},{12... | collective-permute-start | bytes 1572872 | tf_op jit(solution)/shard_map/ppermute | solution.py:188
  86.5 53.9 %collective-permute-start.10 = (bf16[1024,256]{1,0:T(8,128)(2,1)S(1)}, bf16[1024,256]{1,0:T(8,128)(2,1)}, u32[]{:S(2)}, u32[]{:S(2)}) collective-permute-start(bf16[1024,256]{1,0:T(8,128)(2,1)S(1)} %fusion.1), channel_id=1, source_target_pairs={{0,2},{2,4},{4,6},{6,0},{1,3},{3,5},{5,7},{7,1},{8,10},{10,12},{12... | collective-permute-start | bytes 1572872 | tf_op jit(solution)/shard_map/ppermute | solution.py:188
  89.5 50.9 %collective-permute-start.12 = (bf16[1024,256]{1,0:T(8,128)(2,1)}, bf16[1024,256]{1,0:T(8,128)(2,1)}, u32[]{:S(2)}, u32[]{:S(2)}) collective-permute-start(bf16[1024,256]{1,0:T(8,128)(2,1)} %fusion.2), channel_id=1, source_target_pairs={{0,6},{2,0},{4,2},{6,4},{1,7},{3,1},{5,3},{7,5},{8,14},{10,8},{12,... | collective-permute-start | bytes 1572872 | tf_op jit(solution)/shard_map/ppermute | solution.py:188
  109.3 82.9 %copy-start.10 = (s32[128,4]{0,1:T(4,128)S(1)}, s32[128,4]{0,1:T(4,128)}, u32[]{:S(2)}) copy-start(s32[128,4]{0,1:T(4,128)} %param.19) | copy-start | bytes 6148
  109.3 83.1 %copy-start.11 = (f32[1024]{0:T(1024)S(1)}, f32[1024]{0:T(1024)}, u32[]{:S(2)}) copy-start(f32[1024]{0:T(1024)} %param.15) | copy-start | bytes 12292
  118.8 15.4 %all-to-all-start.3 = ((bf16[4,2,80,512]{3,2,1,0:T(8,128)(2,1)}), bf16[4,2,80,512]{3,2,1,0:T(8,128)(2,1)S(1)}, u32[]{:S(2)}, u32[]{:S(2)}) async-start(bf16[4,2,80,512]{3,2,1,0:T(8,128)(2,1)} %attend.1), calls=%async_computation.3 | async-start | bytes 1310720 | tf_op jit(solution)/shard_map/all_to_all | solution.py:299
  137.0 9.4 %all-to-all-start.4 = ((bf16[8,64,128]{2,1,0:T(8,128)(2,1)}), bf16[8,64,128]{2,1,0:T(8,128)(2,1)S(1)}, u32[]{:S(2)}, u32[]{:S(2)}) async-start(bf16[8,64,128]{2,1,0:T(8,128)(2,1)} %bitcast.111), calls=%async_computation.4 | async-start | bytes 262144 | tf_op jit(solution)/shard_map/all_to_all | solution.py:301
  146.4 62.4 %all-to-all-start.5 = ((bf16[32,32,256]{2,1,0:T(8,128)(2,1)}), bf16[32,32,256]{2,1,0:T(8,128)(2,1)S(1)}, u32[]{:S(2)}, u32[]{:S(2)}) async-start(bf16[32,32,256]{2,1,0:T(8,128)(2,1)} %bitcast.32), calls=%async_computation.5 | async-start | bytes 1048576 | tf_op jit(solution)/shard_map/all_to_all | solution.py:303
  (7 other events, 102.4 us)

commit v2 on v1

v2 whole, which is shorter than its diff:
```python
import functools

import jax
import jax.numpy as jnp
from jax import lax
from jax.experimental import pallas as pl
from jax.experimental.pallas import tpu as pltpu
from jax.sharding import Mesh
from jax.sharding import PartitionSpec as P


EP = ("z", "x")
TP = ("y", "c")
epsilon = 1e-06
clamp_limit = 7.0
sigmoid_slope = 1.702


BLK = 512
NEG = -1e30


def pieces_of(values):
    high = values.astype(jnp.bfloat16).astype(jnp.float32)
    rest = values - high
    middle = rest.astype(jnp.bfloat16).astype(jnp.float32)
    return high, middle, rest - middle


def attend_kernel(place, q_ref, kv_ref, fk_ref, fq_ref, o_ref, kaug, vaug, qaug, held, acc, top, knorm):
    step = pl.program_id(0)
    zed, ex = place[0], place[1]
    blocks = kv_ref.shape[0]
    half = BLK // 2

    @pl.when(step == 0)
    def _prepare():
        one = jnp.ones((blocks, BLK), jnp.float32)
        rows = [jnp.zeros((64, BLK), jnp.float32)]
        for h in range(2):
            rows += list(pieces_of(-fk_ref[h]))
        rows += [one, one]
        table = jnp.concatenate(rows, axis=0).T
        lane = lax.broadcasted_iota(jnp.int32, (BLK, 128), 1)
        tail = jnp.where(lax.broadcasted_iota(jnp.int32, (16, BLK), 0) == 0, 1.0, 0.0)
        most = jnp.zeros((1, BLK), jnp.float32)
        for b in range(blocks):
            block = kv_ref[b].astype(jnp.float32)
            kaug[b] = jnp.where(
                lane < 64, block, jnp.where((lane & 7) == b, table, 0.0)
            ).astype(jnp.bfloat16)
            turned = block.T
            vaug[b] = jnp.concatenate([turned[64:], tail], axis=0).astype(jnp.bfloat16)
            keys = turned[:64]
            most = jnp.maximum(most, jnp.sum(keys * keys, axis=0, keepdims=True))
        knorm[0] = jnp.max(most)

    q_turned = q_ref[0].astype(jnp.float32).T * 0.125
    q_most = jnp.maximum(
        jnp.max(jnp.sum(q_turned[:64] * q_turned[:64], axis=0, keepdims=True)),
        jnp.max(jnp.sum(q_turned[64:] * q_turned[64:], axis=0, keepdims=True)),
    )
    calm = q_most * knorm[0] <= 1600.0
    for h in range(2):
        gate = fq_ref[0, h : h + 1]
        high, low, _ = pieces_of(gate)
        on, off = jnp.ones((24, BLK), jnp.float32), jnp.zeros((24, BLK), jnp.float32)
        whole = jnp.concatenate(
            [
                q_turned[64 * h : 64 * h + 64],
                on if h == 0 else off,
                on if h == 1 else off,
                jnp.broadcast_to(high, (8, BLK)),
                jnp.broadcast_to(low, (8, BLK)),
            ],
            axis=0,
        ).astype(jnp.bfloat16)
        for part in range(2):
            qaug[part, h] = whole[:, part * half : part * half + half]
    acc[...] = jnp.zeros_like(acc)
    home = (ex - step) & 3
    after = jnp.where(ex < home, 1, 0)
    low_count = zed + after
    count = blocks - 1 + 2 * after

    def unit(i):
        first = i < low_count
        return jnp.where(first, 0, 1), jnp.where(first, i, i - low_count)

    def scores_of(part, b, h):
        return jnp.dot(kaug[b], qaug[part, h], preferred_element_type=jnp.float32)

    def add(part, b, h, weights):
        acc[part, h] += jnp.dot(
            vaug[b], weights.astype(jnp.bfloat16), preferred_element_type=jnp.float32
        )

    def shifted_add(part, b, h, scores, seen):
        old = top[part, h]
        new = jnp.maximum(old, jnp.max(scores, axis=0, keepdims=True))
        top[part, h] = new
        acc[part, h] = acc[part, h] * jnp.exp(old - new)
        weights = jnp.exp(scores - new)
        add(part, b, h, weights if seen is None else jnp.where(seen, weights, 0.0))

    def seen_of(part):
        return lax.broadcasted_iota(jnp.int32, (BLK, half), 0) <= (
            lax.broadcasted_iota(jnp.int32, (BLK, half), 1) + part * half
        )

    @pl.when(calm)
    def _calm():
        top[...] = jnp.zeros_like(top)
        part, b = unit(0)
        for h in range(2):
            held[h] = scores_of(part, b, h)

        def one(i, carry):
            part, b = unit(i)
            next_part, next_b = unit(jnp.minimum(i + 1, count - 1))
            for h in range(2):
                weights = jnp.exp(held[h])
                held[h] = scores_of(next_part, next_b, h)
                add(part, b, h, weights)
            return carry

        lax.fori_loop(0, count, one, 0)

        @pl.when(step == 0)
        def _edge():
            for part, b in ((0, zed), (1, blocks - 1 - zed)):
                for h in range(2):
                    add(part, b, h, jnp.exp(jnp.where(seen_of(part), scores_of(part, b, h), NEG)))

    @pl.when(jnp.logical_not(calm))
    def _wild():
        top[...] = jnp.full_like(top, NEG)

        def one(i, carry):
            part, b = unit(i)
            for h in range(2):
                shifted_add(part, b, h, scores_of(part, b, h), None)
            return carry

        lax.fori_loop(0, count, one, 0)

        @pl.when(step == 0)
        def _edge():
            for part, b in ((0, zed), (1, blocks - 1 - zed)):
                for h in range(2):
                    seen = seen_of(part)
                    scores = jnp.where(seen, scores_of(part, b, h), NEG)
                    shifted_add(part, b, h, scores, seen)

    for h in range(2):
        for part in range(2):
            rows = list(pieces_of(acc[part, h, 64:65])) + list(pieces_of(top[part, h]))
            rows.append(jnp.zeros((10, half), jnp.float32))
            o_ref[0, h, :, part * half : part * half + half] = jnp.concatenate(
                [acc[part, h, :64]] + rows, axis=0
            ).astype(jnp.bfloat16)


def attend(place, q4, kv8, fk, fq):
    n = kv8.shape[0]
    half = BLK // 2
    return pl.pallas_call(
        attend_kernel,
        grid_spec=pltpu.PrefetchScalarGridSpec(
            num_scalar_prefetch=1,
            grid=(4,),
            in_specs=[
                pl.BlockSpec((1, BLK, 128), lambda i, p: (i, 0, 0)),
                pl.BlockSpec((n, BLK, 128), lambda i, p: (0, 0, 0)),
                pl.BlockSpec((2, n, BLK), lambda i, p: (0, 0, 0)),
                pl.BlockSpec((1, 2, BLK), lambda i, p: ((p[1] - i) & 3, 0, 0)),
            ],
            out_specs=pl.BlockSpec((1, 2, 80, BLK), lambda i, p: (i, 0, 0, 0)),
            scratch_shapes=[
                pltpu.VMEM((n, BLK, 128), jnp.bfloat16),
                pltpu.VMEM((n, 80, BLK), jnp.bfloat16),
                pltpu.VMEM((2, 2, 128, half), jnp.bfloat16),
                pltpu.VMEM((2, BLK, half), jnp.float32),
                pltpu.VMEM((2, 2, 80, half), jnp.float32),
                pltpu.VMEM((2, 2, 1, half), jnp.float32),
                pltpu.SMEM((1,), jnp.float32),
            ],
        ),
        out_shape=jax.ShapeDtypeStruct((4, 2, 80, BLK), jnp.bfloat16),
        name="attend",
    )(place, q4, kv8, fk, fq)


def merge_kernel(*refs):
    parts, o_ref = refs[:4], refs[4]
    outs = []
    for h in range(2):
        peaks, totals = [], []
        for part in parts:
            side = part[h, 64:80].astype(jnp.float32)
            totals.append(side[0:1] + side[1:2] + side[2:3])
            peaks.append(side[3:4] + side[4:5] + side[5:6])
        peak = functools.reduce(jnp.maximum, peaks)
        factors = [jnp.exp(p - peak) for p in peaks]
        total = sum(f * t for f, t in zip(factors, totals))
        value = sum(f * part[h, :64].astype(jnp.float32) for part, f in zip(parts, factors))
        outs.append(value / total)
    o_ref[...] = jnp.concatenate(outs, axis=0).T.astype(jnp.bfloat16)


def merge(parts):
    return pl.pallas_call(
        merge_kernel,
        out_shape=jax.ShapeDtypeStruct((BLK, 128), jnp.bfloat16),
        name="merge",
    )(*parts)


def project_kernel(order, *refs):
    pieces, (gain_ref, weight_ref, out_ref) = refs[:4], refs[4:]
    lefts = [piece[s].astype(jnp.float32) for piece in pieces for s in range(2)]
    squares = sum(jnp.sum(left * left, axis=1, keepdims=True) for left in lefts)
    inverse = lax.rsqrt(squares * (1.0 / 1024.0) + epsilon)
    total = None
    for n, left in enumerate(lefts):
        normed = (left * inverse * gain_ref[pl.ds(order[n], 1), :]).astype(jnp.bfloat16)
        rows = pl.ds(pl.multiple_of(order[n] * 128, 128), 128)
        term = jnp.dot(normed, weight_ref[rows, :], preferred_element_type=jnp.float32)
        total = term if n == 0 else total + term
    out_ref[...] = total.astype(jnp.bfloat16)


def project(order, pieces, gain, weight):
    vmem = pl.BlockSpec(memory_space=pltpu.VMEM)
    return pl.pallas_call(
        project_kernel,
        in_specs=[pl.BlockSpec(memory_space=pltpu.SMEM)] + [vmem] * 6,
        out_specs=vmem,
        out_shape=jax.ShapeDtypeStruct((64, 2048), jnp.bfloat16),
        name="project",
    )(order, *pieces, gain.reshape(8, 128), weight)


def shift(array, axis, by):
    count = lax.axis_size(axis)
    return lax.ppermute(array, axis, [(i, (i + by) % count) for i in range(count)])


def mirror(array):
    count = lax.axis_size("z")
    return lax.ppermute(array, "z", [(i, count - 1 - i) for i in range(count)])


def spread(array, axis):
    count = lax.axis_size(axis)
    return lax.all_to_all(
        jnp.broadcast_to(array[None], (count, *array.shape)), axis, 0, 0, tiled=True
    )


def hidden_kernel(order, *refs):
    pieces, (gate_ref, up_ref, out_ref) = refs[:10], refs[10:]
    upper = pl.program_id(0) < pl.num_programs(0) // 2
    lefts = [piece[...] for piece in pieces[:6]]
    lefts += [jnp.where(upper, a[...], b[...]) for a, b in (pieces[6:8], pieces[8:])]
    gate = up = None
    for n, left in enumerate(lefts):
        rows = pl.ds(pl.multiple_of(order[n] * 256, 256), 256)
        g = jnp.dot(left, gate_ref[rows, :], preferred_element_type=jnp.float32)
        u = jnp.dot(left, up_ref[rows, :], preferred_element_type=jnp.float32)
        gate, up = (g, u) if n == 0 else (gate + g, up + u)
    gate = jnp.minimum(gate, clamp_limit)
    up = jnp.clip(up, -clamp_limit, clamp_limit)
    out_ref[...] = ((up + 1.0) * gate * jax.nn.sigmoid(sigmoid_slope * gate)).astype(jnp.bfloat16)


def hidden_of(order, pieces, gate_local, up_local):
    rows = pieces[0].shape[0]
    tile = 256
    half = rows // tile // 2
    whole = pl.BlockSpec((tile, 256), lambda i, o: (i, 0))
    upper = pl.BlockSpec((tile, 256), lambda i, o: (jnp.minimum(i, half - 1), 0))
    lower = pl.BlockSpec((tile, 256), lambda i, o: (jnp.maximum(i - half, 0), 0))
    return pl.pallas_call(
        hidden_kernel,
        grid_spec=pltpu.PrefetchScalarGridSpec(
            num_scalar_prefetch=1,
            grid=(rows // tile,),
            in_specs=[whole] * 6
            + [upper, lower] * 2
            + [pl.BlockSpec((2048, 256), lambda i, o: (0, 0))] * 2,
            out_specs=whole,
        ),
        out_shape=jax.ShapeDtypeStruct((rows, 256), jnp.bfloat16),
        name="hidden",
    )(order, *pieces, gate_local, up_local)


def body(
    queries,
    keys_values,
    forget_cache,
    heads_gain,
    output_weight,
    expert_tokens,
    expert_gain,
    routes,
    route_logits,
    gate_weight,
    up_weight,
    down_weight,
):
    zed, ex = lax.axis_index("z"), lax.axis_index("x")
    why, core = lax.axis_index("y"), lax.axis_index("c")
    rank = lax.axis_index(TP)
    rows = routes.shape[0]
    experts, capacity, width = 32, 32, 256

    middle = BLK // 2
    q = jnp.concatenate([queries[:middle], mirror(queries[middle:])], axis=0)
    q4 = jnp.stack([q] + [shift(q, "x", by) for by in (1, 2, 3)])

    tokens = expert_tokens.astype(jnp.float32)
    inverse = lax.rsqrt(jnp.mean(tokens * tokens, axis=-1, keepdims=True) + epsilon)
    own = lax.dynamic_slice_in_dim(tokens, rank * width, width, 1)
    own_gain = lax.dynamic_slice_in_dim(expert_gain, rank * width, width, 0)
    own_in = (own * inverse * own_gain).astype(jnp.bfloat16)

    chosen = routes.T[None, :, :] == jnp.arange(experts, dtype=jnp.int32)[:, None, None]
    named = jnp.any(chosen, axis=1)
    number = jnp.arange(rows, dtype=jnp.int32)
    earlier = (number[:, None] < number[None, :]).astype(jnp.bfloat16)
    slot = jnp.dot(named.astype(jnp.bfloat16), earlier, preferred_element_type=jnp.float32)
    slot = jnp.where(named, slot.astype(jnp.int32), -1)
    place = slot[:, None, :] == jnp.arange(capacity, dtype=jnp.int32)[None, :, None]
    onehot = place.astype(jnp.bfloat16).reshape(experts * capacity, rows)
    outgoing = jnp.dot(onehot, own_in, preferred_element_type=jnp.float32).astype(jnp.bfloat16)
    arrived = lax.all_to_all(
        outgoing.reshape(experts, capacity, width), EP, 0, 0, tiled=True
    ).reshape(experts * capacity, width)

    kv, arrived = lax.optimization_barrier((keys_values, arrived))
    near = experts * capacity // 2
    left, right = shift(arrived, "y", 1), shift(arrived, "y", 3)
    far = [shift(left[:near], "y", 1), shift(right[near:], "y", 3)]
    pieces = [arrived, left, right]
    pieces += [shift(piece, "c", 1) for piece in pieces]
    pieces += far + [shift(piece, "c", 1) for piece in far]
    places = [2 * ((why - by) % 4) for by in (0, 1, 3)]
    order = [p + core for p in places] + [p + 1 - core for p in places]
    last = 2 * ((why + 2) % 4)
    order = jnp.stack(order + [last + core, last + 1 - core]).astype(jnp.int32)

    kv8 = spread(kv, "z")
    gates = forget_cache.reshape(2, 8, 4, BLK)
    fk = lax.dynamic_index_in_dim(gates, ex, 2, keepdims=False)
    fq = jnp.concatenate(
        [
            lax.dynamic_index_in_dim(gates, zed, 1, keepdims=False)[:, :, :middle],
            lax.dynamic_index_in_dim(gates, 7 - zed, 1, keepdims=False)[:, :, middle:],
        ],
        axis=2,
    ).transpose(1, 0, 2)

    hidden = hidden_of(order, pieces, gate_weight[0], up_weight[0])
    down = down_weight[0].reshape(width, 4, 2, width)

    def partial(by, side):
        part = lax.dynamic_slice(
            down, (0, (why + by) % 4, side, 0), (width, 1, 1, width)
        ).reshape(width, width)
        return jnp.dot(hidden, part, preferred_element_type=jnp.float32)

    steps = (2, 1, 3, 0)
    others = [shift(partial(by, 1 - core).astype(jnp.bfloat16), "c", 1) for by in steps]
    pairs = [
        (partial(by, core) + other.astype(jnp.float32)).astype(jnp.bfloat16)
        for by, other in zip(steps, others)
    ]
    far, after, before, kept = [pair for pair in pairs]
    first, second = shift(far[:near], "y", 1), shift(far[near:], "y", 3)

    def joined(pair, extra, top):
        total = (pair[:near] if top else pair[near:]).astype(jnp.float32) + extra.astype(jnp.float32)
        total = total.astype(jnp.bfloat16)
        return jnp.concatenate([total, pair[near:]] if top else [pair[:near], total], axis=0)

    moved = [kept, shift(joined(after, first, True), "y", 1)]
    moved.append(shift(joined(before, second, False), "y", 3))
    expert_out = sum(m.astype(jnp.float32) for m in moved).astype(jnp.bfloat16)

    parts = attend(jnp.stack([zed, ex]).astype(jnp.int32), q4, kv8, fk, fq)
    parts = [parts[0]] + [shift(parts[by], "x", 4 - by) for by in (1, 2, 3)]
    returned = lax.all_to_all(
        expert_out.reshape(experts, capacity, width), EP, 0, 0, tiled=True
    ).reshape(experts * capacity, width)
    attended = merge(parts)
    attended = jnp.concatenate([attended[:middle], mirror(attended[middle:])], axis=0)
    attended = attended.reshape(4, 2, 64, 128)
    twin = shift(lax.dynamic_index_in_dim(attended, 1 - core, 1, keepdims=False), "c", 1)
    mine = lax.dynamic_index_in_dim(attended, core, 1, keepdims=False)
    both = jnp.stack([mine, twin], axis=1)
    slices = []
    for by in range(4):
        piece = lax.dynamic_index_in_dim(both, (why + by) % 4, 0, keepdims=False)
        slices.append(shift(piece, "y", by) if by else piece)
    heads = [2 * ((why - by) % 4) + side for by in range(4) for side in (core, 1 - core)]
    mixer_out = project(jnp.stack(heads).astype(jnp.int32), slices, heads_gain, output_weight)

    shifted = route_logits - jnp.max(route_logits, axis=1, keepdims=True)
    raised = jnp.exp(shifted)
    route_weight = raised / jnp.sum(raised, axis=1, keepdims=True)
    share = jnp.sum(jnp.where(chosen, route_weight.T[None, :, :], 0.0), axis=1)
    high = share.astype(jnp.bfloat16)
    low = (share - high.astype(jnp.float32)).astype(jnp.bfloat16)
    moe = 0.0
    for piece in (high, low):
        table = jnp.where(place, piece[:, None, :], jnp.bfloat16(0)).reshape(-1, rows)
        moe = moe + lax.dot_general(
            table, returned, (((0,), (0,)), ((), ())), preferred_element_type=jnp.float32
        )
    return (mixer_out, moe.astype(jnp.bfloat16))


def solution(mesh):
    torus = Mesh(mesh.devices.reshape(8, 4, 4, 2), ("z", "x", "y", "c"))
    return jax.shard_map(
        body,
        mesh=torus,
        in_specs=(
            P(EP, TP),
            P(EP, TP),
            P(TP, None),
            P(),
            P(),
            P(EP, None),
            P(),
            P(EP, None),
            P(EP, None),
            P(EP, None, TP),
            P(EP, None, TP),
            P(EP, TP, None),
        ),
        out_specs=(P(EP + TP, None), P(EP, TP)),
        check_vma=False,
    )
```

time: 211 us -> 194 us (0.919)
  starting transfers between devices: 74 us -> 43.1 us
  Pallas kernels: 18.6 us -> 47.8 us
  waiting for transfers between devices: 62.7 us -> 37.8 us
  local copies, waits for them, and re-layouts: 7.29 us -> 14.4 us
  other arithmetic: 4.23 us -> 9.03 us
  matrix products: 14 us -> 11.5 us
    all_to_all x1, starting transfers between devices: 45.8 us -> 10.2 us  [body(): lax.all_to_all(expert_out.reshape(experts, capacity, width), EP, 0, 0, ti...]
    pallas_call x1, Pallas kernels: 9.54 us -> 34.8 us  [attend(): pl.pallas_call(attend_kernel, grid_spec=pltpu.PrefetchScalarGridSpec(num_...]
    all_to_all x2 -> x1, waiting for transfers between devices: 16 us -> 0.01 us  [spread(): lax.all_to_all(jnp.broadcast_to(array[None], (count, *array.shape)), axis...]
    ppermute x14 -> x27, starting transfers between devices: 11.2 us -> 26.3 us  [shift(): lax.ppermute(array, axis, [(i, (i + by) % count) for i in range(count)])]
    ppermute x0 -> x2, waiting for transfers between devices: none -> 14.2 us  [mirror(): return lax.ppermute(array, 'z', [(i, count - 1 - i) for i in range(count)])]
    all_to_all x2 -> x0, waiting for transfers between devices: 13.1 us -> none  [the longest x1 9.83 us: body(): parts = lax.all_to_all(parts, 'x', 0, 0, tiled=True)]
    all_to_all x1, waiting for transfers between devices: 12.7 us -> 0.01 us  [body(): lax.all_to_all(expert_out.reshape(experts, capacity, width), EP, 0, 0, ti...]
    all_to_all x2 -> x0, starting transfers between devices: 8.86 us -> none  [the longest x1 5.49 us: body(): parts = lax.all_to_all(parts, 'x', 0, 0, tiled=True)]
  transfers between devices with their start and end apart: 19 -> 31, of which waited for: 7 -> 11; matrix products, arithmetic and copies ran while one was open for 8% -> 13% of each run, Pallas kernels for 9% -> 25%
where the time goes in v2:
time: 194 us; the launch traced here: 193 us
  Pallas kernels  47.8 us (25%)
  starting transfers between devices  43.1 us (22%)
  waiting for transfers between devices  37.8 us (19%)
  blocking collectives  28.2 us (15%)
  local copies, waits for them, and re-layouts  14.4 us (7%)
  matrix products  11.5 us (6%)
  other arithmetic  9.03 us (5%)
    pallas_call x1, Pallas kernels, attend(): pl.pallas_call(attend_kernel, grid_spec=pltpu.PrefetchScalarGridSpec(num_...  34.8 us
    all_to_all x1, blocking collectives, body(): lax.all_to_all(outgoing.reshape(experts, capacity, width), EP, 0, 0, tile...  28.2 us
    ppermute x27, starting transfers between devices, shift(): lax.ppermute(array, axis, [(i, (i + by) % count) for i in range(count)])  26.3 us
    ppermute x27, waiting for transfers between devices, shift(): lax.ppermute(array, axis, [(i, (i + by) % count) for i in range(count)])  23.6 us
    ppermute x2, waiting for transfers between devices, mirror(): return lax.ppermute(array, 'z', [(i, count - 1 - i) for i in range(count)])  14.2 us
    all_to_all x1, starting transfers between devices, body(): lax.all_to_all(expert_out.reshape(experts, capacity, width), EP, 0, 0, ti...  10.2 us
    dot_general x8, matrix products, partial(): return jnp.dot(hidden, part, preferred_element_type=jnp.float32)  9.79 us
    pallas_call x1, Pallas kernels, hidden_of(): pl.pallas_call(hidden_kernel, grid_spec=pltpu.PrefetchScalarGridSpec(num_...  7.15 us
  transfers between devices with their start and end apart: 31, of which 11 were waited for; matrix products, arithmetic and copies ran while one was open for 13% of the time, Pallas kernels for 25%

profile of v2, /device:TPU:2, one launch (start us, length us, event | category | flops | bytes accessed | tf_op | source)
XLA Modules:
  0.0 192.9 jit_solution(10801511740210853101)
XLA Ops:
  5.4 28.2 %all_to_all.15 = bf16[32,32,256]{2,1,0:T(8,128)(2,1)S(1)} all-to-all(bf16[32,32,256]{2,1,0:T(8,128)(2,1)S(1)} %bitcast.123), channel_id=1, replica_groups=mesh['z'=8,'x'=4,'y'=4,'c'=2] {'z','x'}, dimensions={0} | all-to-all | bytes 1048576 | tf_op jit(solution)/shard_map/all_to_all | solution.py:338
  37.0 5.5 %collective-permute-done = bf16[256,128]{1,0:T(8,128)(2,1)S(1)} collective-permute-done((bf16[256,128]{1,0:T(8,128)(2,1)S(1)}, bf16[256,128]{1,0:T(8,128)(2,1)S(1)}, u32[]{:S(2)}, u32[]{:S(2)}) %collective-permute-start) | collective-permute-done | bytes 65568 | tf_op jit(solution)/shard_map/ppermute | solution.py:251
  48.7 3.0 %collective-permute-start.18 = (bf16[512,256]{1,0:T(8,128)(2,1)S(1)}, bf16[512,256]{1,0:T(8,128)(2,1)}, u32[]{:S(2)}, u32[]{:S(2)}) collective-permute-start(bf16[512,256]{1,0:T(8,128)(2,1)S(1)} %slice.81), channel_id=1, source_target_pairs={{0,6},{2,0},{4,2},{6,4},{1,7},{3,1},{5,3},{7,5},{8,14},{10,8},{12,... | collective-permute-start | bytes 786440 | tf_op jit(solution)/shard_map/ppermute | solution.py:246
  60.1 1.9 pad_maximum_fusion.q_ref
  62.0 2.1 %broadcast_in_dim.54 = bf16[8,512,128]{2,1,0:T(8,128)(2,1)} broadcast(bf16[512,128]{1,0:T(8,128)(2,1)} %param.13), dimensions={1,2} | broadcast | bytes 1179648 | tf_op jit(solution)/shard_map/broadcast_in_dim | solution.py:257
  64.0 3.7 %all-to-all-start.1 = ((bf16[8,512,128]{2,1,0:T(8,128)(2,1)}), bf16[8,512,128]{2,1,0:T(8,128)(2,1)S(1)}, u32[]{:S(2)}, u32[]{:S(2)}) async-start(bf16[8,512,128]{2,1,0:T(8,128)(2,1)} %broadcast_in_dim.54), calls=%async_computation.1 | async-start | bytes 2097152 | tf_op jit(solution)/shard_map/all_to_all | solution.py:256
  67.7 7.1 %hidden.1 = bf16[1024,256]{1,0:T(8,128)(2,1)} custom-call(s32[8]{0:T(128)} %stack.103.order, bf16[1024,256]{1,0:T(8,128)(2,1)} %bitcast.127, bf16[1024,256]{1,0:T(8,128)(2,1)} %copy-done.3, bf16[1024,256]{1,0:T(8,128)(2,1)} %collective-permute-done.13.refs_2_, bf16[1024,256]{1,0:T(8,128)(2,1)} %collective-permute-done.14.refs_3_, ...), custom_call_target="tpu_custom_call" | custom-call | tf_op jit(solution)/shard_map/hidden/pallas_call | solution.py:284
  80.4 2.2 %convolution_convert_fusion.3 = bf16[1024,256]{1,0:T(8,128)(2,1)} fusion(bf16[1024,256]{1,0:T(8,128)(2,1)} %hidden.1, bf16[256,4,2,256]{0,3,2,1:T(8,128)(2,1)S(1)} %bitcast.118, s32[]{:T(128)S(6)} %select_n.142, s32[]{:T(128)S(6)} %select_n.141), kind=kOutput, calls=%fused_computation.7 | convolution fusion | flops 134479872 | bytes 1179656 | tf_op jit(solution)/shard_map/dot_general | solution.py:372
  84.9 2.6 %collective-permute-start.27 = (bf16[512,256]{1,0:T(8,128)(2,1)S(1)}, bf16[512,256]{1,0:T(8,128)(2,1)S(1)}, u32[]{:S(2)}, u32[]{:S(2)}) collective-permute-start(bf16[512,256]{1,0:T(8,128)(2,1)S(1)} %get-tuple-element.13), channel_id=1, source_target_pairs={{0,6},{2,0},{4,2},{6,4},{1,7},{3,1},{5,3},{7,5},{8,14},{10,8},{12,... | collective-permute-start | bytes 786440 | tf_op jit(solution)/shard_map/ppermute | solution.py:246
  87.9 6.0 %collective-permute-done.24 = bf16[512,256]{1,0:T(8,128)(2,1)S(1)} collective-permute-done((bf16[512,256]{1,0:T(8,128)(2,1)S(1)}, bf16[512,256]{1,0:T(8,128)(2,1)S(1)}, u32[]{:S(2)}, u32[]{:S(2)}) %collective-permute-start.24) | collective-permute-done | bytes 262176 | tf_op jit(solution)/shard_map/ppermute | solution.py:246
  95.7 3.2 %collective-permute-start.28 = (bf16[1024,256]{1,0:T(8,128)(2,1)}, bf16[1024,256]{1,0:T(8,128)(2,1)}, u32[]{:S(2)}, u32[]{:S(2)}) collective-permute-start(bf16[1024,256]{1,0:T(8,128)(2,1)} %pad_maximum_fusion.2), channel_id=1, source_target_pairs={{0,6},{2,0},{4,2},{6,4},{1,7},{3,1},{5,3},{7,5},{8,14},{10,8},{12,... | collective-permute-start | bytes 1572872 | tf_op jit(solution)/shard_map/ppermute | solution.py:246
  100.0 34.8 %attend.1 = bf16[4,2,80,512]{3,2,1,0:T(8,128)(2,1)} custom-call(s32[2]{0:T(128)} %pad_add_fusion.place, bf16[4,512,128]{2,1,0:T(8,128)(2,1)} %pad_maximum_fusion.q_ref, bf16[8,512,128]{2,1,0:T(8,128)(2,1)} %copy-done.1, f32[2,8,512]{2,1,0:T(8,128)} %bitcast.132, f32[4,2,512]{2,1,0:T(2,128)} %maximum_bitcast_fusion.fq_ref), custom_call_target="tpu_custom_call" | custom-call | tf_op jit(solution)/shard_map/attend/pallas_call | solution.py:167
  136.6 3.3 %collective-permute-start.4 = (bf16[2,80,512]{2,1,0:T(8,128)(2,1)S(1)}, bf16[2,80,512]{2,1,0:T(8,128)(2,1)S(1)}, u32[]{:S(2)}, u32[]{:S(2)}) collective-permute-start(bf16[2,80,512]{2,1,0:T(8,128)(2,1)S(1)} %get-tuple-element.10), channel_id=1, source_target_pairs={{0,24},{8,0},{16,8},{24,16},{1,25},{9,1},{17,9},{25,17},{2,26},{10... | collective-permute-start | bytes 491528 | tf_op jit(solution)/shard_map/ppermute | solution.py:246
  139.9 4.5 %collective-permute-done.4.refs_1_ = bf16[2,80,512]{2,1,0:T(8,128)(2,1)S(1)} collective-permute-done((bf16[2,80,512]{2,1,0:T(8,128)(2,1)S(1)}, bf16[2,80,512]{2,1,0:T(8,128)(2,1)S(1)}, u32[]{:S(2)}, u32[]{:S(2)}) %collective-permute-start.4) | collective-permute-done | bytes 163872 | tf_op jit(solution)/shard_map/ppermute | solution.py:246
  144.4 2.3 %collective-permute-done.5.refs_2_ = bf16[2,80,512]{2,1,0:T(8,128)(2,1)S(1)} collective-permute-done((bf16[2,80,512]{2,1,0:T(8,128)(2,1)S(1)}, bf16[2,80,512]{2,1,0:T(8,128)(2,1)S(1)}, u32[]{:S(2)}, u32[]{:S(2)}) %collective-permute-start.5) | collective-permute-done | bytes 163872 | tf_op jit(solution)/shard_map/ppermute | solution.py:246
  146.7 3.4 %collective-permute-done.6.refs_3_ = bf16[2,80,512]{2,1,0:T(8,128)(2,1)S(1)} collective-permute-done((bf16[2,80,512]{2,1,0:T(8,128)(2,1)S(1)}, bf16[2,80,512]{2,1,0:T(8,128)(2,1)S(1)}, u32[]{:S(2)}, u32[]{:S(2)}) %collective-permute-start.6) | collective-permute-done | bytes 163872 | tf_op jit(solution)/shard_map/ppermute | solution.py:246
  150.8 2.1 %merge.1 = bf16[512,128]{1,0:T(8,128)(2,1)} custom-call(bf16[2,80,512]{2,1,0:T(8,128)(2,1)} %get-tuple-element.11.refs_0_, bf16[2,80,512]{2,1,0:T(8,128)(2,1)} %copy-done.7, bf16[2,80,512]{2,1,0:T(8,128)(2,1)} %copy-done.8, bf16[2,80,512]{2,1,0:T(8,128)(2,1)} %copy-done.9), custom_call_target="tpu_custom_call" | custom-call | tf_op jit(solution)/shard_map/merge/pallas_call | solution.py:212
  152.9 2.4 %fusion.4 = bf16[1024,256]{1,0:T(8,128)(2,1)} fusion(bf16[1024,256]{1,0:T(8,128)(2,1)S(1)} %copy-done, bf16[1024,256]{1,0:T(8,128)(2,1)} %collective-permute-done.28, bf16[1024,256]{1,0:T(8,128)(2,1)} %collective-permute-done.25, bf16[1024,256]{1,0:T(8,128)(2,1)S(1)} %collective-permute-done.21, bf16[256,4,2,256]{0,3,2,1:T(8,128)(2,1)S(1)} %bitcast.122, ...), kind=kOutput, calls=%fused_computation.12 | convolution fusion | flops 136577024 | bytes 2752520 | tf_op jit(solution)/shard_map/dot_general | solution.py:372
  155.4 10.2 %all-to-all-start.2 = ((bf16[32,32,256]{2,1,0:T(8,128)(2,1)}), bf16[32,32,256]{2,1,0:T(8,128)(2,1)S(1)}, u32[]{:S(2)}, u32[]{:S(2)}) async-start(bf16[32,32,256]{2,1,0:T(8,128)(2,1)} %bitcast.53), calls=%async_computation.2 | async-start | bytes 1048576 | tf_op jit(solution)/shard_map/all_to_all | solution.py:394
  166.4 2.8 %collective-permute-start.7 = (bf16[256,128]{1,0:T(8,128)(2,1)S(1)}, bf16[256,128]{1,0:T(8,128)(2,1)S(1)}, u32[]{:S(2)}, u32[]{:S(2)}) collective-permute-start(bf16[256,128]{1,0:T(8,128)(2,1)S(1)} %get-tuple-element.21), channel_id=1, source_target_pairs={{0,224},{32,192},{64,160},{96,128},{128,96},{160,64},{192,32},{224... | collective-permute-start | bytes 196616 | tf_op jit(solution)/shard_map/ppermute | solution.py:251
  169.3 8.7 %collective-permute-done.7 = bf16[256,128]{1,0:T(8,128)(2,1)S(1)} collective-permute-done((bf16[256,128]{1,0:T(8,128)(2,1)S(1)}, bf16[256,128]{1,0:T(8,128)(2,1)S(1)}, u32[]{:S(2)}, u32[]{:S(2)}) %collective-permute-start.7) | collective-permute-done | bytes 65568 | tf_op jit(solution)/shard_map/ppermute | solution.py:251
  180.0 2.2 %collective-permute-start.11 = (bf16[2,64,128]{2,1,0:T(8,128)(2,1)S(1)}, bf16[2,64,128]{2,1,0:T(8,128)(2,1)S(1)}, u32[]{:S(2)}, u32[]{:S(2)}) collective-permute-start(bf16[2,64,128]{2,1,0:T(8,128)(2,1)S(1)} %get-tuple-element.14), channel_id=1, source_target_pairs={{0,6},{2,0},{4,2},{6,4},{1,7},{3,1},{5,3},{7,5},{8,14},{10,8},{12,... | collective-permute-start | bytes 98312 | tf_op jit(solution)/shard_map/ppermute | solution.py:246
  182.9 2.5 %collective-permute-done.10.refs_2_ = bf16[2,64,128]{2,1,0:T(8,128)(2,1)S(1)} collective-permute-done((bf16[2,64,128]{2,1,0:T(8,128)(2,1)S(1)}, bf16[2,64,128]{2,1,0:T(8,128)(2,1)S(1)}, u32[]{:S(2)}, u32[]{:S(2)}) %collective-permute-start.10) | collective-permute-done | bytes 32800 | tf_op jit(solution)/shard_map/ppermute | solution.py:246
  187.9 3.8 %project.1 = bf16[64,2048]{1,0:T(8,128)(2,1)} custom-call(s32[8]{0:T(128)} %stack.87.order, bf16[2,64,128]{2,1,0:T(8,128)(2,1)} %get-tuple-element.15.refs_0_, bf16[2,64,128]{2,1,0:T(8,128)(2,1)} %copy-done.14, bf16[2,64,128]{2,1,0:T(8,128)(2,1)} %copy-done.12, bf16[2,64,128]{2,1,0:T(8,128)(2,1)} %copy-done.13, f32[8,128]{1,0:T(8,128)} %bitcast.137, ...), custom_call_target="tpu_custom_call" | custom-call | tf_op jit(solution)/shard_map/project/pallas_call | solution.py:235
  (135 shorter events, 43.5 us)
Async XLA Ops:
  33.7 13.6 %collective-permute-start.12 = (bf16[1024,256]{1,0:T(8,128)(2,1)S(1)}, bf16[1024,256]{1,0:T(8,128)(2,1)S(1)}, u32[]{:S(2)}, u32[]{:S(2)}) collective-permute-start(bf16[1024,256]{1,0:T(8,128)(2,1)S(1)} %bitcast.124), channel_id=1, source_target_pairs={{0,2},{2,4},{4,6},{6,0},{1,3},{3,5},{5,7},{7,1},{8,10},{10,12},{12... | collective-permute-start | bytes 1572872 | tf_op jit(solution)/shard_map/ppermute | solution.py:246
  35.3 12.5 %collective-permute-start.13 = (bf16[1024,256]{1,0:T(8,128)(2,1)S(1)}, bf16[1024,256]{1,0:T(8,128)(2,1)}, u32[]{:S(2)}, u32[]{:S(2)}) collective-permute-start(bf16[1024,256]{1,0:T(8,128)(2,1)S(1)} %bitcast.125), channel_id=1, source_target_pairs={{0,6},{2,0},{4,2},{6,4},{1,7},{3,1},{5,3},{7,5},{8,14},{10,8},{12,... | collective-permute-start | bytes 1572872 | tf_op jit(solution)/shard_map/ppermute | solution.py:246
  42.5 9.3 %collective-permute-start.1 = (bf16[512,128]{1,0:T(8,128)(2,1)S(1)}, bf16[512,128]{1,0:T(8,128)(2,1)S(1)}, u32[]{:S(2)}, u32[]{:S(2)}) collective-permute-start(bf16[512,128]{1,0:T(8,128)(2,1)S(1)} %get-tuple-element.25), channel_id=1, source_target_pairs={{0,8},{8,16},{16,24},{24,0},{1,9},{9,17},{17,25},{25,1},{2,10},{10... | collective-permute-start | bytes 393224 | tf_op jit(solution)/shard_map/ppermute | solution.py:246
  44.1 7.9 %collective-permute-start.2 = (bf16[512,128]{1,0:T(8,128)(2,1)S(1)}, bf16[512,128]{1,0:T(8,128)(2,1)}, u32[]{:S(2)}, u32[]{:S(2)}) collective-permute-start(bf16[512,128]{1,0:T(8,128)(2,1)S(1)} %get-tuple-element.25), channel_id=1, source_target_pairs={{0,16},{8,24},{16,0},{24,8},{1,17},{9,25},{17,1},{25,9},{2,18},{10... | collective-permute-start | bytes 393224 | tf_op jit(solution)/shard_map/ppermute | solution.py:246
  45.8 6.6 %collective-permute-start.3 = (bf16[512,128]{1,0:T(8,128)(2,1)S(1)}, bf16[512,128]{1,0:T(8,128)(2,1)}, u32[]{:S(2)}, u32[]{:S(2)}) collective-permute-start(bf16[512,128]{1,0:T(8,128)(2,1)S(1)} %get-tuple-element.25), channel_id=1, source_target_pairs={{0,24},{8,0},{16,8},{24,16},{1,25},{9,1},{17,9},{25,17},{2,26},{10... | collective-permute-start | bytes 393224 | tf_op jit(solution)/shard_map/ppermute | solution.py:246
  47.3 7.7 %collective-permute-start.17 = (bf16[512,256]{1,0:T(8,128)(2,1)S(1)}, bf16[512,256]{1,0:T(8,128)(2,1)S(1)}, u32[]{:S(2)}, u32[]{:S(2)}) collective-permute-start(bf16[512,256]{1,0:T(8,128)(2,1)S(1)} %slice.80), channel_id=1, source_target_pairs={{0,2},{2,4},{4,6},{6,0},{1,3},{3,5},{5,7},{7,1},{8,10},{10,12},{12... | collective-permute-start | bytes 786440 | tf_op jit(solution)/shard_map/ppermute | solution.py:246
  48.7 6.8 %collective-permute-start.18 = (bf16[512,256]{1,0:T(8,128)(2,1)S(1)}, bf16[512,256]{1,0:T(8,128)(2,1)}, u32[]{:S(2)}, u32[]{:S(2)}) collective-permute-start(bf16[512,256]{1,0:T(8,128)(2,1)S(1)} %slice.81), channel_id=1, source_target_pairs={{0,6},{2,0},{4,2},{6,4},{1,7},{3,1},{5,3},{7,5},{8,14},{10,8},{12,... | collective-permute-start | bytes 786440 | tf_op jit(solution)/shard_map/ppermute | solution.py:246
  51.9 15.8 %collective-permute-start.14 = (bf16[1024,256]{1,0:T(8,128)(2,1)S(1)}, bf16[1024,256]{1,0:T(8,128)(2,1)}, u32[]{:S(2)}, u32[]{:S(2)}) collective-permute-start(bf16[1024,256]{1,0:T(8,128)(2,1)S(1)} %bitcast.126), channel_id=1, source_target_pairs={{0,1},{1,0},{2,3},{3,2},{4,5},{5,4},{6,7},{7,6},{8,9},{9,8},{10,11... | collective-permute-start | bytes 1572872 | tf_op jit(solution)/shard_map/ppermute | solution.py:246
  52.0 15.7 %collective-permute-start.15 = (bf16[1024,256]{1,0:T(8,128)(2,1)S(1)}, bf16[1024,256]{1,0:T(8,128)(2,1)}, u32[]{:S(2)}, u32[]{:S(2)}) collective-permute-start(bf16[1024,256]{1,0:T(8,128)(2,1)S(1)} %collective-permute-done.12.refs_1_), channel_id=1, source_target_pairs={{0,1},{1,0},{2,3},{3,2},{4,5},{5,4},{6,7},{7,6},{8,9},{9,8},{10,11... | collective-permute-start | bytes 1572872 | tf_op jit(solution)/shard_map/ppermute | solution.py:246
  52.5 15.3 %collective-permute-start.16 = (bf16[1024,256]{1,0:T(8,128)(2,1)}, bf16[1024,256]{1,0:T(8,128)(2,1)}, u32[]{:S(2)}, u32[]{:S(2)}) collective-permute-start(bf16[1024,256]{1,0:T(8,128)(2,1)} %collective-permute-done.13.refs_2_), channel_id=1, source_target_pairs={{0,1},{1,0},{2,3},{3,2},{4,5},{5,4},{6,7},{7,6},{8,9},{9,8},{10,11... | collective-permute-start | bytes 1572872 | tf_op jit(solution)/shard_map/ppermute | solution.py:246
  55.0 12.7 %collective-permute-start.19 = (bf16[512,256]{1,0:T(8,128)(2,1)S(1)}, bf16[512,256]{1,0:T(8,128)(2,1)}, u32[]{:S(2)}, u32[]{:S(2)}) collective-permute-start(bf16[512,256]{1,0:T(8,128)(2,1)S(1)} %collective-permute-done.17.refs_6_), channel_id=1, source_target_pairs={{0,1},{1,0},{2,3},{3,2},{4,5},{5,4},{6,7},{7,6},{8,9},{9,8},{10,11... | collective-permute-start | bytes 786440 | tf_op jit(solution)/shard_map/ppermute | solution.py:246
  55.6 12.1 %collective-permute-start.20 = (bf16[512,256]{1,0:T(8,128)(2,1)}, bf16[512,256]{1,0:T(8,128)(2,1)}, u32[]{:S(2)}, u32[]{:S(2)}) collective-permute-start(bf16[512,256]{1,0:T(8,128)(2,1)} %collective-permute-done.18.refs_7_), channel_id=1, source_target_pairs={{0,1},{1,0},{2,3},{3,2},{4,5},{5,4},{6,7},{7,6},{8,9},{9,8},{10,11... | collective-permute-start | bytes 786440 | tf_op jit(solution)/shard_map/ppermute | solution.py:246
  64.0 34.9 %all-to-all-start.1 = ((bf16[8,512,128]{2,1,0:T(8,128)(2,1)}), bf16[8,512,128]{2,1,0:T(8,128)(2,1)S(1)}, u32[]{:S(2)}, u32[]{:S(2)}) async-start(bf16[8,512,128]{2,1,0:T(8,128)(2,1)} %broadcast_in_dim.54), calls=%async_computation.1 | async-start | bytes 2097152 | tf_op jit(solution)/shard_map/all_to_all | solution.py:256
  76.3 6.4 %collective-permute-start.23 = (bf16[1024,256]{1,0:T(8,128)(2,1)S(1)}, bf16[1024,256]{1,0:T(8,128)(2,1)S(1)}, u32[]{:S(2)}, u32[]{:S(2)}) collective-permute-start(bf16[1024,256]{1,0:T(8,128)(2,1)S(1)} %convolution_convert_fusion.1), channel_id=1, source_target_pairs={{0,1},{1,0},{2,3},{3,2},{4,5},{5,4},{6,7},{7,6},{8,9},{9,8},{10,11... | collective-permute-start | bytes 1572872 | tf_op jit(solution)/shard_map/ppermute | solution.py:246
  80.0 7.5 %collective-permute-start.26 = (bf16[1024,256]{1,0:T(8,128)(2,1)S(1)}, bf16[1024,256]{1,0:T(8,128)(2,1)S(1)}, u32[]{:S(2)}, u32[]{:S(2)}) collective-permute-start(bf16[1024,256]{1,0:T(8,128)(2,1)S(1)} %convolution_convert_fusion), channel_id=1, source_target_pairs={{0,1},{1,0},{2,3},{3,2},{4,5},{5,4},{6,7},{7,6},{8,9},{9,8},{10,11... | collective-permute-start | bytes 1572872 | tf_op jit(solution)/shard_map/ppermute | solution.py:246
  82.6 70.3 %collective-permute-start.21 = (bf16[1024,256]{1,0:T(8,128)(2,1)}, bf16[1024,256]{1,0:T(8,128)(2,1)S(1)}, u32[]{:S(2)}, u32[]{:S(2)}) collective-permute-start(bf16[1024,256]{1,0:T(8,128)(2,1)} %convolution_convert_fusion.3), channel_id=1, source_target_pairs={{0,1},{1,0},{2,3},{3,2},{4,5},{5,4},{6,7},{7,6},{8,9},{9,8},{10,11... | collective-permute-start | bytes 1572872 | tf_op jit(solution)/shard_map/ppermute | solution.py:246
  83.1 10.8 %collective-permute-start.24 = (bf16[512,256]{1,0:T(8,128)(2,1)S(1)}, bf16[512,256]{1,0:T(8,128)(2,1)S(1)}, u32[]{:S(2)}, u32[]{:S(2)}) collective-permute-start(bf16[512,256]{1,0:T(8,128)(2,1)S(1)} %get-tuple-element.12), channel_id=1, source_target_pairs={{0,2},{2,4},{4,6},{6,0},{1,3},{3,5},{5,7},{7,1},{8,10},{10,12},{12... | collective-permute-start | bytes 786440 | tf_op jit(solution)/shard_map/ppermute | solution.py:246
  84.9 9.9 %collective-permute-start.27 = (bf16[512,256]{1,0:T(8,128)(2,1)S(1)}, bf16[512,256]{1,0:T(8,128)(2,1)S(1)}, u32[]{:S(2)}, u32[]{:S(2)}) collective-permute-start(bf16[512,256]{1,0:T(8,128)(2,1)S(1)} %get-tuple-element.13), channel_id=1, source_target_pairs={{0,6},{2,0},{4,2},{6,4},{1,7},{3,1},{5,3},{7,5},{8,14},{10,8},{12,... | collective-permute-start | bytes 786440 | tf_op jit(solution)/shard_map/ppermute | solution.py:246
  94.8 58.1 %collective-permute-start.25 = (bf16[1024,256]{1,0:T(8,128)(2,1)}, bf16[1024,256]{1,0:T(8,128)(2,1)}, u32[]{:S(2)}, u32[]{:S(2)}) collective-permute-start(bf16[1024,256]{1,0:T(8,128)(2,1)} %pad_maximum_fusion.1), channel_id=1, source_target_pairs={{0,2},{2,4},{4,6},{6,0},{1,3},{3,5},{5,7},{7,1},{8,10},{10,12},{12... | collective-permute-start | bytes 1572872 | tf_op jit(solution)/shard_map/ppermute | solution.py:246
  95.7 57.2 %collective-permute-start.28 = (bf16[1024,256]{1,0:T(8,128)(2,1)}, bf16[1024,256]{1,0:T(8,128)(2,1)}, u32[]{:S(2)}, u32[]{:S(2)}) collective-permute-start(bf16[1024,256]{1,0:T(8,128)(2,1)} %pad_maximum_fusion.2), channel_id=1, source_target_pairs={{0,6},{2,0},{4,2},{6,4},{1,7},{3,1},{5,3},{7,5},{8,14},{10,8},{12,... | collective-permute-start | bytes 1572872 | tf_op jit(solution)/shard_map/ppermute | solution.py:246
  136.6 7.7 %collective-permute-start.4 = (bf16[2,80,512]{2,1,0:T(8,128)(2,1)S(1)}, bf16[2,80,512]{2,1,0:T(8,128)(2,1)S(1)}, u32[]{:S(2)}, u32[]{:S(2)}) collective-permute-start(bf16[2,80,512]{2,1,0:T(8,128)(2,1)S(1)} %get-tuple-element.10), channel_id=1, source_target_pairs={{0,24},{8,0},{16,8},{24,16},{1,25},{9,1},{17,9},{25,17},{2,26},{10... | collective-permute-start | bytes 491528 | tf_op jit(solution)/shard_map/ppermute | solution.py:246
  139.9 6.8 %collective-permute-start.5 = (bf16[2,80,512]{2,1,0:T(8,128)(2,1)S(1)}, bf16[2,80,512]{2,1,0:T(8,128)(2,1)S(1)}, u32[]{:S(2)}, u32[]{:S(2)}) collective-permute-start(bf16[2,80,512]{2,1,0:T(8,128)(2,1)S(1)} %get-tuple-element.9), channel_id=1, source_target_pairs={{0,16},{8,24},{16,0},{24,8},{1,17},{9,25},{17,1},{25,9},{2,18},{10... | collective-permute-start | bytes 491528 | tf_op jit(solution)/shard_map/ppermute | solution.py:246
  155.4 36.4 %all-to-all-start.2 = ((bf16[32,32,256]{2,1,0:T(8,128)(2,1)}), bf16[32,32,256]{2,1,0:T(8,128)(2,1)S(1)}, u32[]{:S(2)}, u32[]{:S(2)}) async-start(bf16[32,32,256]{2,1,0:T(8,128)(2,1)} %bitcast.53), calls=%async_computation.2 | async-start | bytes 1048576 | tf_op jit(solution)/shard_map/all_to_all | solution.py:394
  166.4 11.6 %collective-permute-start.7 = (bf16[256,128]{1,0:T(8,128)(2,1)S(1)}, bf16[256,128]{1,0:T(8,128)(2,1)S(1)}, u32[]{:S(2)}, u32[]{:S(2)}) collective-permute-start(bf16[256,128]{1,0:T(8,128)(2,1)S(1)} %get-tuple-element.21), channel_id=1, source_target_pairs={{0,224},{32,192},{64,160},{96,128},{128,96},{160,64},{192,32},{224... | collective-permute-start | bytes 196616 | tf_op jit(solution)/shard_map/ppermute | solution.py:251
  (26 other events, 473.5 us)

commit v3 on v2

--- a/solution.py
+++ b/solution.py
@@ -18,6 +18,7 @@
 
 BLK = 512
 NEG = -1e30
+KEYS_FROM = (0, 7, 1, 6, 2, 5, 3, 4)
 
 
 def pieces_of(values):
@@ -27,25 +28,29 @@
     return high, middle, rest - middle
 
 
-def attend_kernel(place, q_ref, kv_ref, fk_ref, fq_ref, o_ref, kaug, vaug, qaug, held, acc, top, knorm):
-    step = pl.program_id(0)
+def attend_kernel(first, place, *refs):
+    q_refs, kv_refs = refs[:2], refs[2:10]
+    fk_ref, low_ref, high_ref, o_ref, kaug, vaug, qaug, held, acc, top, knorm = refs[10:]
+    turn = pl.program_id(0)
+    step = turn + first
     zed, ex = place[0], place[1]
-    blocks = kv_ref.shape[0]
+    blocks = len(kv_refs)
     half = BLK // 2
 
-    @pl.when(step == 0)
+    @pl.when(turn == 0)
     def _prepare():
         one = jnp.ones((blocks, BLK), jnp.float32)
         rows = [jnp.zeros((64, BLK), jnp.float32)]
         for h in range(2):
-            rows += list(pieces_of(-fk_ref[h]))
+            rows += list(pieces_of(-fk_ref[h, :, 0, 0, :]))
         rows += [one, one]
         table = jnp.concatenate(rows, axis=0).T
         lane = lax.broadcasted_iota(jnp.int32, (BLK, 128), 1)
         tail = jnp.where(lax.broadcasted_iota(jnp.int32, (16, BLK), 0) == 0, 1.0, 0.0)
         most = jnp.zeros((1, BLK), jnp.float32)
-        for b in range(blocks):
-            block = kv_ref[b].astype(jnp.float32)
+        for kv_ref, away in zip(kv_refs, KEYS_FROM):
+            b = (zed + away) & 7
+            block = kv_ref[...].astype(jnp.float32)
             kaug[b] = jnp.where(
                 lane < 64, block, jnp.where((lane & 7) == b, table, 0.0)
             ).astype(jnp.bfloat16)
@@ -55,14 +60,17 @@
             most = jnp.maximum(most, jnp.sum(keys * keys, axis=0, keepdims=True))
         knorm[0] = jnp.max(most)
 
-    q_turned = q_ref[0].astype(jnp.float32).T * 0.125
+    q_now = jnp.where(turn == 0, q_refs[0][...], q_refs[1][...])
+    q_turned = q_now.astype(jnp.float32).T * 0.125
     q_most = jnp.maximum(
         jnp.max(jnp.sum(q_turned[:64] * q_turned[:64], axis=0, keepdims=True)),
         jnp.max(jnp.sum(q_turned[64:] * q_turned[64:], axis=0, keepdims=True)),
     )
     calm = q_most * knorm[0] <= 1600.0
     for h in range(2):
-        gate = fq_ref[0, h : h + 1]
+        gate = jnp.concatenate(
+            [low_ref[h, 0, 0, :, :half], high_ref[h, 0, 0, :, half:]], axis=1
+        )
         high, low, _ = pieces_of(gate)
         on, off = jnp.ones((24, BLK), jnp.float32), jnp.zeros((24, BLK), jnp.float32)
         whole = jnp.concatenate(
@@ -95,14 +103,6 @@
             vaug[b], weights.astype(jnp.bfloat16), preferred_element_type=jnp.float32
         )
 
-    def shifted_add(part, b, h, scores, seen):
-        old = top[part, h]
-        new = jnp.maximum(old, jnp.max(scores, axis=0, keepdims=True))
-        top[part, h] = new
-        acc[part, h] = acc[part, h] * jnp.exp(old - new)
-        weights = jnp.exp(scores - new)
-        add(part, b, h, weights if seen is None else jnp.where(seen, weights, 0.0))
-
     def seen_of(part):
         return lax.broadcasted_iota(jnp.int32, (BLK, half), 0) <= (
             lax.broadcasted_iota(jnp.int32, (BLK, half), 1) + part * half
@@ -126,31 +126,34 @@
 
         lax.fori_loop(0, count, one, 0)
 
-        @pl.when(step == 0)
-        def _edge():
-            for part, b in ((0, zed), (1, blocks - 1 - zed)):
-                for h in range(2):
-                    add(part, b, h, jnp.exp(jnp.where(seen_of(part), scores_of(part, b, h), NEG)))
+        def edge(part):
+            b = jnp.where(part == 0, zed, blocks - 1 - zed)
+            for h in range(2):
+                add(part, b, h, jnp.exp(jnp.where(seen_of(part), scores_of(part, b, h), NEG)))
+
+        if first == 0:
+            lax.fori_loop(0, jnp.where(turn == 0, 2, 0), lambda part, c: (edge(part), c)[1], 0)
 
     @pl.when(jnp.logical_not(calm))
     def _wild():
         top[...] = jnp.full_like(top, NEG)
+        low_all = zed + jnp.where(ex <= home, 1, 0)
 
         def one(i, carry):
-            part, b = unit(i)
-            for h in range(2):
-                shifted_add(part, b, h, scores_of(part, b, h), None)
+            h, n = i & 1, i >> 1
+            part = jnp.where(n < low_all, 0, 1)
+            b = n - part * low_all
+            edge = (step == 0) & (b == jnp.where(part == 0, zed, blocks - 1 - zed))
+            seen = seen_of(part + jnp.where(edge, 0, 4))
+            scores = jnp.where(seen, scores_of(part, b, h), NEG)
+            old = top[part, h]
+            new = jnp.maximum(old, jnp.max(scores, axis=0, keepdims=True))
+            top[part, h] = new
+            acc[part, h] = acc[part, h] * jnp.exp(old - new)
+            add(part, b, h, jnp.where(seen, jnp.exp(scores - new), 0.0))
             return carry
 
-        lax.fori_loop(0, count, one, 0)
-
-        @pl.when(step == 0)
-        def _edge():
-            for part, b in ((0, zed), (1, blocks - 1 - zed)):
-                for h in range(2):
-                    seen = seen_of(part)
-                    scores = jnp.where(seen, scores_of(part, b, h), NEG)
-                    shifted_add(part, b, h, scores, seen)
+        lax.fori_loop(0, 2 * (blocks - 1 + 2 * jnp.where(ex <= home, 1, 0)), one, 0)
 
     for h in range(2):
         for part in range(2):
@@ -161,19 +164,21 @@
             ).astype(jnp.bfloat16)
 
 
-def attend(place, q4, kv8, fk, fq):
-    n = kv8.shape[0]
+def attend(first, place, q_pair, kv_list, gates):
+    n = len(kv_list)
     half = BLK // 2
+    whole = pl.BlockSpec((BLK, 128), lambda i, p: (0, 0))
+    one_gate = (2, 1, 1, 1, BLK)
     return pl.pallas_call(
-        attend_kernel,
+        functools.partial(attend_kernel, first),
         grid_spec=pltpu.PrefetchScalarGridSpec(
             num_scalar_prefetch=1,
-            grid=(4,),
-            in_specs=[
-                pl.BlockSpec((1, BLK, 128), lambda i, p: (i, 0, 0)),
-                pl.BlockSpec((n, BLK, 128), lambda i, p: (0, 0, 0)),
-                pl.BlockSpec((2, n, BLK), lambda i, p: (0, 0, 0)),
-                pl.BlockSpec((1, 2, BLK), lambda i, p: ((p[1] - i) & 3, 0, 0)),
+            grid=(2,),
+            in_specs=[whole] * (2 + n)
+            + [
+                pl.BlockSpec((2, n, 1, 1, BLK), lambda i, p: (0, 0, p[1], 0, 0)),
+                pl.BlockSpec(one_gate, lambda i, p: (0, p[0], (p[1] - i - first) & 3, 0, 0)),
+                pl.BlockSpec(one_gate, lambda i, p: (0, 7 - p[0], (p[1] - i - first) & 3, 0, 0)),
             ],
             out_specs=pl.BlockSpec((1, 2, 80, BLK), lambda i, p: (i, 0, 0, 0)),
             scratch_shapes=[
@@ -186,9 +191,9 @@
                 pltpu.SMEM((1,), jnp.float32),
             ],
         ),
-        out_shape=jax.ShapeDtypeStruct((4, 2, 80, BLK), jnp.bfloat16),
+        out_shape=jax.ShapeDtypeStruct((2, 2, 80, BLK), jnp.bfloat16),
         name="attend",
-    )(place, q4, kv8, fk, fq)
+    )(place, *q_pair, *kv_list, gates, gates, gates)
 
 
 def merge_kernel(*refs):
@@ -249,13 +254,6 @@
 def mirror(array):
     count = lax.axis_size("z")
     return lax.ppermute(array, "z", [(i, count - 1 - i) for i in range(count)])
-
-
-def spread(array, axis):
-    count = lax.axis_size(axis)
-    return lax.all_to_all(
-        jnp.broadcast_to(array[None], (count, *array.shape)), axis, 0, 0, tiled=True
-    )
 
 
 def hidden_kernel(order, *refs):
@@ -317,12 +315,19 @@
     experts, capacity, width = 32, 32, 256
 
     middle = BLK // 2
-    q = jnp.concatenate([queries[:middle], mirror(queries[middle:])], axis=0)
-    q4 = jnp.stack([q] + [shift(q, "x", by) for by in (1, 2, 3)])
+    turned = mirror(queries[middle:])
+    q = jnp.concatenate([queries[:middle], turned], axis=0)
+    q_list = [q] + [shift(q, "x", by) for by in (1, 2, 3)]
+    ups, downs = [keys_values], [keys_values]
+    for _ in range(3):
+        ups.append(shift(ups[-1], "z", 1))
+    for _ in range(4):
+        downs.append(shift(downs[-1], "z", 7))
+    kv_list = [keys_values, ups[1], downs[1], ups[2], downs[2], ups[3], downs[3], downs[4]]
 
     tokens = expert_tokens.astype(jnp.float32)
     inverse = lax.rsqrt(jnp.mean(tokens * tokens, axis=-1, keepdims=True) + epsilon)
-    own = lax.dynamic_slice_in_dim(tokens, rank * width, width, 1)
+    own = lax.dynamic_slice_in_dim(expert_tokens, rank * width, width, 1).astype(jnp.float32)
     own_gain = lax.dynamic_slice_in_dim(expert_gain, rank * width, width, 0)
     own_in = (own * inverse * own_gain).astype(jnp.bfloat16)
 
@@ -338,36 +343,22 @@
     arrived = lax.all_to_all(
         outgoing.reshape(experts, capacity, width), EP, 0, 0, tiled=True
     ).reshape(experts * capacity, width)
-
-    kv, arrived = lax.optimization_barrier((keys_values, arrived))
     near = experts * capacity // 2
     left, right = shift(arrived, "y", 1), shift(arrived, "y", 3)
     far = [shift(left[:near], "y", 1), shift(right[near:], "y", 3)]
     pieces = [arrived, left, right]
     pieces += [shift(piece, "c", 1) for piece in pieces]
     pieces += far + [shift(piece, "c", 1) for piece in far]
-    places = [2 * ((why - by) % 4) for by in (0, 1, 3)]
-    order = [p + core for p in places] + [p + 1 - core for p in places]
-    last = 2 * ((why + 2) % 4)
-    order = jnp.stack(order + [last + core, last + 1 - core]).astype(jnp.int32)
-
-    kv8 = spread(kv, "z")
-    gates = forget_cache.reshape(2, 8, 4, BLK)
-    fk = lax.dynamic_index_in_dim(gates, ex, 2, keepdims=False)
-    fq = jnp.concatenate(
-        [
-            lax.dynamic_index_in_dim(gates, zed, 1, keepdims=False)[:, :, :middle],
-            lax.dynamic_index_in_dim(gates, 7 - zed, 1, keepdims=False)[:, :, middle:],
-        ],
-        axis=2,
-    ).transpose(1, 0, 2)
+    ways = jnp.array([0, 1, 3, 0, 1, 3, 2, 2], jnp.int32)
+    sides = jnp.array([0, 0, 0, 1, 1, 1, 0, 1], jnp.int32)
+    order = 2 * ((why - ways) & 3) + (core ^ sides)
 
     hidden = hidden_of(order, pieces, gate_weight[0], up_weight[0])
     down = down_weight[0].reshape(width, 4, 2, width)
 
     def partial(by, side):
         part = lax.dynamic_slice(
-            down, (0, (why + by) % 4, side, 0), (width, 1, 1, width)
+            down, (0, (why + by) & 3, side, 0), (width, 1, 1, width)
         ).reshape(width, width)
         return jnp.dot(hidden, part, preferred_element_type=jnp.float32)
 
@@ -389,23 +380,30 @@
     moved.append(shift(joined(before, second, False), "y", 3))
     expert_out = sum(m.astype(jnp.float32) for m in moved).astype(jnp.bfloat16)
 
-    parts = attend(jnp.stack([zed, ex]).astype(jnp.int32), q4, kv8, fk, fq)
-    parts = [parts[0]] + [shift(parts[by], "x", 4 - by) for by in (1, 2, 3)]
+    gates = forget_cache.reshape(2, 8, 4, 1, BLK)
+    spot = jnp.stack([zed, ex]).astype(jnp.int32)
+    parts = attend(0, spot, q_list[:2], kv_list, gates)
+    parts = [parts[0], shift(parts[1], "x", 3)]
+    rest = attend(2, spot, q_list[2:], kv_list, gates)
+    parts += [shift(rest[0], "x", 2), shift(rest[1], "x", 1)]
     returned = lax.all_to_all(
         expert_out.reshape(experts, capacity, width), EP, 0, 0, tiled=True
     ).reshape(experts * capacity, width)
     attended = merge(parts)
-    attended = jnp.concatenate([attended[:middle], mirror(attended[middle:])], axis=0)
+    turned = mirror(attended[middle:])
+    attended = jnp.concatenate([attended[:middle], turned], axis=0)
     attended = attended.reshape(4, 2, 64, 128)
     twin = shift(lax.dynamic_index_in_dim(attended, 1 - core, 1, keepdims=False), "c", 1)
     mine = lax.dynamic_index_in_dim(attended, core, 1, keepdims=False)
     both = jnp.stack([mine, twin], axis=1)
     slices = []
     for by in range(4):
-        piece = lax.dynamic_index_in_dim(both, (why + by) % 4, 0, keepdims=False)
+        piece = lax.dynamic_index_in_dim(both, (why + by) & 3, 0, keepdims=False)
         slices.append(shift(piece, "y", by) if by else piece)
-    heads = [2 * ((why - by) % 4) + side for by in range(4) for side in (core, 1 - core)]
-    mixer_out = project(jnp.stack(heads).astype(jnp.int32), slices, heads_gain, output_weight)
+    ways = jnp.array([0, 0, 1, 1, 2, 2, 3, 3], jnp.int32)
+    sides = jnp.array([0, 1, 0, 1, 0, 1, 0, 1], jnp.int32)
+    heads = 2 * ((why - ways) & 3) + (core ^ sides)
+    mixer_out = project(heads, slices, heads_gain, output_weight)
 
     shifted = route_logits - jnp.max(route_logits, axis=1, keepdims=True)
     raised = jnp.exp(shifted)

time: 194 us -> 195 us (level)
  blocking collectives: 28.2 us -> 0 us
  starting transfers between devices: 43.1 us -> 64.8 us
  Pallas kernels: 47.8 us -> 55.6 us
  local copies, waits for them, and re-layouts: 14.4 us -> 9.7 us
  waiting for transfers between devices: 37.8 us -> 40.9 us
    all_to_all x1 -> x0, blocking collectives: 28.2 us -> none  [body(): lax.all_to_all(outgoing.reshape(experts, capacity, width), EP, 0, 0, tile...]
    ppermute x27 -> x34, starting transfers between devices: 26.3 us -> 43.7 us  [shift(): lax.ppermute(array, axis, [(i, (i + by) % count) for i in range(count)])]
    all_to_all x1, waiting for transfers between devices: 0.01 us -> 14 us  [body(): lax.all_to_all(outgoing.reshape(experts, capacity, width), EP, 0, 0, tile...]
    ppermute x27 -> x34, waiting for transfers between devices: 23.6 us -> 14.5 us  [shift(): lax.ppermute(array, axis, [(i, (i + by) % count) for i in range(count)])]
    all_to_all x1, starting transfers between devices: 3.66 us -> 11.6 us  [body(): lax.all_to_all(outgoing.reshape(experts, capacity, width), EP, 0, 0, tile...]
    pallas_call x1 -> x2, Pallas kernels: 34.8 us -> 42.6 us  [attend(): pl.pallas_call(functools.partial(attend_kernel, first), grid_spec=pltpu.P...]
    all_to_all x1, starting transfers between devices: 10.2 us -> 6.44 us  [body(): lax.all_to_all(expert_out.reshape(experts, capacity, width), EP, 0, 0, ti...]
    broadcast_in_dim x1 -> x0, local copies, waits for them, and re-layouts: 2.05 us -> none  [spread(): jnp.broadcast_to(array[None], (count, *array.shape))]
  transfers between devices with their start and end apart: 31 -> 38, of which waited for: 11 -> 11; matrix products, arithmetic and copies ran while one was open for 13% -> 11% of each run, Pallas kernels for 25% -> 29%
where the time goes in v3:
time: 195 us; the launch traced here: 194 us
  starting transfers between devices  64.8 us (33%)
  Pallas kernels  55.6 us (29%)
  waiting for transfers between devices  40.9 us (21%)
  matrix products  13 us (7%)
  local copies, waits for them, and re-layouts  9.7 us (5%)
  other arithmetic  9.06 us (5%)
    ppermute x34, starting transfers between devices, shift(): lax.ppermute(array, axis, [(i, (i + by) % count) for i in range(count)])  43.7 us
    pallas_call x2, Pallas kernels, attend(): pl.pallas_call(functools.partial(attend_kernel, first), grid_spec=pltpu.P...  42.6 us
    ppermute x34, waiting for transfers between devices, shift(): lax.ppermute(array, axis, [(i, (i + by) % count) for i in range(count)])  14.5 us
    all_to_all x1, waiting for transfers between devices, body(): lax.all_to_all(outgoing.reshape(experts, capacity, width), EP, 0, 0, tile...  14 us
    ppermute x2, waiting for transfers between devices, mirror(): return lax.ppermute(array, 'z', [(i, count - 1 - i) for i in range(count)])  12.4 us
    all_to_all x1, starting transfers between devices, body(): lax.all_to_all(outgoing.reshape(experts, capacity, width), EP, 0, 0, tile...  11.6 us
    dot_general x8, matrix products, partial(): return jnp.dot(hidden, part, preferred_element_type=jnp.float32)  9.68 us
    pallas_call x1, Pallas kernels, hidden_of(): pl.pallas_call(hidden_kernel, grid_spec=pltpu.PrefetchScalarGridSpec(num_...  7.15 us
  transfers between devices with their start and end apart: 38, of which 11 were waited for; matrix products, arithmetic and copies ran while one was open for 11% of the time, Pallas kernels for 29%

profile of v3, /device:TPU:2, one launch (start us, length us, event | category | flops | bytes accessed | tf_op | source)
XLA Modules:
  0.0 194.2 jit_solution(12139502200965970384)
XLA Ops:
  3.8 2.0 %convolution_convert_fusion.4 = bf16[1024,256]{1,0:T(8,128)(2,1)} fusion(pred[1024,128]{1,0:T(32,128)(4,1)S(1)} %bitcast_compare_fusion, f32[256]{0:T(256)S(1)} %dynamic_slice.57, f32[128]{0:T(128)S(1)} %add_rsqrt_fusion, bf16[128,2048]{1,0:T(8,128)(2,1)} %param.21, s32[]{:T(128)S(6)} %select_n.64), kind=kOutput, calls=%fused_computation.16 | convolution fusion | flops 67502080 | bytes 722436 | tf_op jit(solution)/shard_map/dot_general | solution.py:342
  5.8 11.6 %all-to-all-start = ((bf16[32,32,256]{2,1,0:T(8,128)(2,1)}), bf16[32,32,256]{2,1,0:T(8,128)(2,1)S(1)}, u32[]{:S(2)}, u32[]{:S(2)}) async-start(bf16[32,32,256]{2,1,0:T(8,128)(2,1)} %bitcast.17), calls=%async_computation | async-start | bytes 1048576 | tf_op jit(solution)/shard_map/all_to_all | solution.py:343
  17.4 2.8 %collective-permute-start.3 = (bf16[512,128]{1,0:T(8,128)(2,1)}, bf16[512,128]{1,0:T(8,128)(2,1)S(1)}, u32[]{:S(2)}, u32[]{:S(2)}) collective-permute-start(bf16[512,128]{1,0:T(8,128)(2,1)} %refs_2_.3), channel_id=1, source_target_pairs={{0,224},{32,0},{64,32},{96,64},{128,96},{160,128},{192,160},{224,1... | collective-permute-start | bytes 393224 | tf_op jit(solution)/shard_map/ppermute | solution.py:251
  20.2 14.0 %all-to-all-done = bf16[32,32,256]{2,1,0:T(8,128)(2,1)S(1)} async-done(((bf16[32,32,256]{2,1,0:T(8,128)(2,1)}), bf16[32,32,256]{2,1,0:T(8,128)(2,1)S(1)}, u32[]{:S(2)}, u32[]{:S(2)}) %all-to-all-start) | async-done | bytes 524320 | tf_op jit(solution)/shard_map/all_to_all | solution.py:343
  42.8 3.4 %collective-permute-start.7 = (bf16[512,128]{1,0:T(8,128)(2,1)S(1)}, bf16[512,128]{1,0:T(8,128)(2,1)S(1)}, u32[]{:S(2)}, u32[]{:S(2)}) collective-permute-start(bf16[512,128]{1,0:T(8,128)(2,1)S(1)} %collective-permute-done.5.refs_6_), channel_id=1, source_target_pairs={{0,224},{32,0},{64,32},{96,64},{128,96},{160,128},{192,160},{224,1... | collective-permute-start | bytes 393224 | tf_op jit(solution)/shard_map/ppermute | solution.py:251
  47.9 2.2 %collective-permute-start.10 = (bf16[512,128]{1,0:T(8,128)(2,1)S(1)}, bf16[512,128]{1,0:T(8,128)(2,1)S(1)}, u32[]{:S(2)}, u32[]{:S(2)}) collective-permute-start(bf16[512,128]{1,0:T(8,128)(2,1)S(1)} %pad_maximum_fusion.2.refs_0_), channel_id=1, source_target_pairs={{0,16},{8,24},{16,0},{24,8},{1,17},{9,25},{17,1},{25,9},{2,18},{10... | collective-permute-start | bytes 393224 | tf_op jit(solution)/shard_map/ppermute | solution.py:251
  56.2 2.0 %collective-permute-start.25 = (bf16[512,256]{1,0:T(8,128)(2,1)S(1)}, bf16[512,256]{1,0:T(8,128)(2,1)}, u32[]{:S(2)}, u32[]{:S(2)}) collective-permute-start(bf16[512,256]{1,0:T(8,128)(2,1)S(1)} %slice.71), channel_id=1, source_target_pairs={{0,6},{2,0},{4,2},{6,4},{1,7},{3,1},{5,3},{7,5},{8,14},{10,8},{12,... | collective-permute-start | bytes 786440 | tf_op jit(solution)/shard_map/ppermute | solution.py:251
  68.3 22.2 %attend.3 = bf16[2,2,80,512]{3,2,1,0:T(8,128)(2,1)} custom-call(s32[2]{0:T(128)} %pad_add_fusion.place, bf16[512,128]{1,0:T(8,128)(2,1)} %copy-done.16, bf16[512,128]{1,0:T(8,128)(2,1)} %copy-done.17, bf16[512,128]{1,0:T(8,128)(2,1)} %refs_2_.3, bf16[512,128]{1,0:T(8,128)(2,1)} %copy-done.6, bf16[512,128]{1,0:T(8,128)(2,1)} %copy-done.5, ...), custom_call_target="tpu_custom_call" | custom-call | tf_op jit(solution)/shard_map/attend/pallas_call | solution.py:172
  90.7 7.1 %hidden.1 = bf16[1024,256]{1,0:T(8,128)(2,1)} custom-call(s32[8]{0:T(128)} %fusion.60.order, bf16[1024,256]{1,0:T(8,128)(2,1)} %bitcast.97, bf16[1024,256]{1,0:T(8,128)(2,1)} %copy-done.3, bf16[1024,256]{1,0:T(8,128)(2,1)} %copy-done.4, bf16[1024,256]{1,0:T(8,128)(2,1)} %collective-permute-done.21.refs_3_, ...), custom_call_target="tpu_custom_call" | custom-call | tf_op jit(solution)/shard_map/hidden/pallas_call | solution.py:282
  103.0 2.2 %convolution_convert_fusion.3 = bf16[1024,256]{1,0:T(8,128)(2,1)} fusion(bf16[1024,256]{1,0:T(8,128)(2,1)} %hidden.1, bf16[256,4,2,256]{0,3,2,1:T(8,128)(2,1)S(1)} %bitcast.89, s32[]{:T(128)S(6)} %select_n.57, s32[]{:T(128)S(6)} %select_n.56), kind=kOutput, calls=%fused_computation.7 | convolution fusion | flops 134479872 | bytes 1179656 | tf_op jit(solution)/shard_map/dot_general | solution.py:363
  107.0 2.7 %collective-permute-start.34 = (bf16[512,256]{1,0:T(8,128)(2,1)S(1)}, bf16[512,256]{1,0:T(8,128)(2,1)S(1)}, u32[]{:S(2)}, u32[]{:S(2)}) collective-permute-start(bf16[512,256]{1,0:T(8,128)(2,1)S(1)} %get-tuple-element.5), channel_id=1, source_target_pairs={{0,6},{2,0},{4,2},{6,4},{1,7},{3,1},{5,3},{7,5},{8,14},{10,8},{12,... | collective-permute-start | bytes 786440 | tf_op jit(solution)/shard_map/ppermute | solution.py:251
  110.1 5.7 %collective-permute-done.31 = bf16[512,256]{1,0:T(8,128)(2,1)S(1)} collective-permute-done((bf16[512,256]{1,0:T(8,128)(2,1)S(1)}, bf16[512,256]{1,0:T(8,128)(2,1)S(1)}, u32[]{:S(2)}, u32[]{:S(2)}) %collective-permute-start.31) | collective-permute-done | bytes 262176 | tf_op jit(solution)/shard_map/ppermute | solution.py:251
  117.7 3.2 %collective-permute-start.35 = (bf16[1024,256]{1,0:T(8,128)(2,1)}, bf16[1024,256]{1,0:T(8,128)(2,1)S(1)}, u32[]{:S(2)}, u32[]{:S(2)}) collective-permute-start(bf16[1024,256]{1,0:T(8,128)(2,1)} %pad_maximum_fusion.1), channel_id=1, source_target_pairs={{0,6},{2,0},{4,2},{6,4},{1,7},{3,1},{5,3},{7,5},{8,14},{10,8},{12,... | collective-permute-start | bytes 1572872 | tf_op jit(solution)/shard_map/ppermute | solution.py:251
  120.9 3.9 %collective-permute-start.12 = (bf16[2,80,512]{2,1,0:T(8,128)(2,1)S(1)}, bf16[2,80,512]{2,1,0:T(8,128)(2,1)S(1)}, u32[]{:S(2)}, u32[]{:S(2)}) collective-permute-start(bf16[2,80,512]{2,1,0:T(8,128)(2,1)S(1)} %get-tuple-element.7), channel_id=1, source_target_pairs={{0,16},{8,24},{16,0},{24,8},{1,17},{9,25},{17,1},{25,9},{2,18},{10... | collective-permute-start | bytes 491528 | tf_op jit(solution)/shard_map/ppermute | solution.py:251
  125.5 20.4 %attend.2 = bf16[2,2,80,512]{3,2,1,0:T(8,128)(2,1)} custom-call(s32[2]{0:T(128)} %pad_add_fusion.place, bf16[512,128]{1,0:T(8,128)(2,1)} %copy-done.12, bf16[512,128]{1,0:T(8,128)(2,1)} %copy-done.18, bf16[512,128]{1,0:T(8,128)(2,1)} %refs_2_.3, bf16[512,128]{1,0:T(8,128)(2,1)} %copy-done.6, bf16[512,128]{1,0:T(8,128)(2,1)} %copy-done.5, ...), custom_call_target="tpu_custom_call" | custom-call | tf_op jit(solution)/shard_map/attend/pallas_call | solution.py:172
  147.5 3.9 %collective-permute-start.9 = (bf16[2,80,512]{2,1,0:T(8,128)(2,1)S(1)}, bf16[2,80,512]{2,1,0:T(8,128)(2,1)S(1)}, u32[]{:S(2)}, u32[]{:S(2)}) collective-permute-start(bf16[2,80,512]{2,1,0:T(8,128)(2,1)S(1)} %get-tuple-element.8), channel_id=1, source_target_pairs={{0,24},{8,0},{16,8},{24,16},{1,25},{9,1},{17,9},{25,17},{2,26},{10... | collective-permute-start | bytes 491528 | tf_op jit(solution)/shard_map/ppermute | solution.py:251
  151.5 2.8 %collective-permute-done.9.refs_1_ = bf16[2,80,512]{2,1,0:T(8,128)(2,1)S(1)} collective-permute-done((bf16[2,80,512]{2,1,0:T(8,128)(2,1)S(1)}, bf16[2,80,512]{2,1,0:T(8,128)(2,1)S(1)}, u32[]{:S(2)}, u32[]{:S(2)}) %collective-permute-start.9) | collective-permute-done | bytes 163872 | tf_op jit(solution)/shard_map/ppermute | solution.py:251
  154.9 2.0 %merge.1 = bf16[512,128]{1,0:T(8,128)(2,1)} custom-call(bf16[2,80,512]{2,1,0:T(8,128)(2,1)} %get-tuple-element.9.refs_0_, bf16[2,80,512]{2,1,0:T(8,128)(2,1)} %copy-done.15, bf16[2,80,512]{2,1,0:T(8,128)(2,1)} %copy-done.13, bf16[2,80,512]{2,1,0:T(8,128)(2,1)} %copy-done.14), custom_call_target="tpu_custom_call" | custom-call | tf_op jit(solution)/shard_map/merge/pallas_call | solution.py:217
  157.0 2.3 %fusion.4 = bf16[1024,256]{1,0:T(8,128)(2,1)} fusion(bf16[1024,256]{1,0:T(8,128)(2,1)S(1)} %copy-done, bf16[1024,256]{1,0:T(8,128)(2,1)S(1)} %collective-permute-done.35, bf16[1024,256]{1,0:T(8,128)(2,1)} %collective-permute-done.32, bf16[1024,256]{1,0:T(8,128)(2,1)S(1)} %collective-permute-done.28, bf16[256,4,2,256]{0,3,2,1:T(8,128)(2,1)S(1)} %bitcast.93, ...), kind=kOutput, calls=%fused_computation.12 | convolution fusion | flops 136577024 | bytes 2752520 | tf_op jit(solution)/shard_map/dot_general | solution.py:363
  159.3 6.4 %all-to-all-start.1 = ((bf16[32,32,256]{2,1,0:T(8,128)(2,1)}), bf16[32,32,256]{2,1,0:T(8,128)(2,1)S(1)}, u32[]{:S(2)}, u32[]{:S(2)}) async-start(bf16[32,32,256]{2,1,0:T(8,128)(2,1)} %bitcast.30), calls=%async_computation.1 | async-start | bytes 1048576 | tf_op jit(solution)/shard_map/all_to_all | solution.py:389
  166.6 2.8 %collective-permute-start.14 = (bf16[256,128]{1,0:T(8,128)(2,1)S(1)}, bf16[256,128]{1,0:T(8,128)(2,1)S(1)}, u32[]{:S(2)}, u32[]{:S(2)}) collective-permute-start(bf16[256,128]{1,0:T(8,128)(2,1)S(1)} %get-tuple-element.17), channel_id=1, source_target_pairs={{0,224},{32,192},{64,160},{96,128},{128,96},{160,64},{192,32},{224... | collective-permute-start | bytes 196616 | tf_op jit(solution)/shard_map/ppermute | solution.py:256
  169.5 10.7 %collective-permute-done.14 = bf16[256,128]{1,0:T(8,128)(2,1)S(1)} collective-permute-done((bf16[256,128]{1,0:T(8,128)(2,1)S(1)}, bf16[256,128]{1,0:T(8,128)(2,1)S(1)}, u32[]{:S(2)}, u32[]{:S(2)}) %collective-permute-start.14) | collective-permute-done | bytes 65568 | tf_op jit(solution)/shard_map/ppermute | solution.py:256
  182.2 2.1 %collective-permute-start.17 = (bf16[2,64,128]{2,1,0:T(8,128)(2,1)S(1)}, bf16[2,64,128]{2,1,0:T(8,128)(2,1)S(1)}, u32[]{:S(2)}, u32[]{:S(2)}) collective-permute-start(bf16[2,64,128]{2,1,0:T(8,128)(2,1)S(1)} %get-tuple-element.13), channel_id=1, source_target_pairs={{0,4},{2,6},{4,0},{6,2},{1,5},{3,7},{5,1},{7,3},{8,12},{10,14},{12... | collective-permute-start | bytes 98312 | tf_op jit(solution)/shard_map/ppermute | solution.py:251
  189.2 3.8 %project.1 = bf16[64,2048]{1,0:T(8,128)(2,1)} custom-call(s32[8]{0:T(128)} %fusion.62.order, bf16[2,64,128]{2,1,0:T(8,128)(2,1)} %get-tuple-element.11.refs_0_, bf16[2,64,128]{2,1,0:T(8,128)(2,1)} %copy-done.19, bf16[2,64,128]{2,1,0:T(8,128)(2,1)} %copy-done.20, bf16[2,64,128]{2,1,0:T(8,128)(2,1)} %copy-done.21, f32[8,128]{1,0:T(8,128)} %bitcast.104, ...), custom_call_target="tpu_custom_call" | custom-call | tf_op jit(solution)/shard_map/project/pallas_call | solution.py:240
  (161 shorter events, 50.7 us)
Async XLA Ops:
  5.8 28.5 %all-to-all-start = ((bf16[32,32,256]{2,1,0:T(8,128)(2,1)}), bf16[32,32,256]{2,1,0:T(8,128)(2,1)S(1)}, u32[]{:S(2)}, u32[]{:S(2)}) async-start(bf16[32,32,256]{2,1,0:T(8,128)(2,1)} %bitcast.17), calls=%async_computation | async-start | bytes 1048576 | tf_op jit(solution)/shard_map/all_to_all | solution.py:343
  17.4 19.9 %collective-permute-start.3 = (bf16[512,128]{1,0:T(8,128)(2,1)}, bf16[512,128]{1,0:T(8,128)(2,1)S(1)}, u32[]{:S(2)}, u32[]{:S(2)}) collective-permute-start(bf16[512,128]{1,0:T(8,128)(2,1)} %refs_2_.3), channel_id=1, source_target_pairs={{0,224},{32,0},{64,32},{96,64},{128,96},{160,128},{192,160},{224,1... | collective-permute-start | bytes 393224 | tf_op jit(solution)/shard_map/ppermute | solution.py:251
  34.3 18.7 %collective-permute-start.19 = (bf16[1024,256]{1,0:T(8,128)(2,1)S(1)}, bf16[1024,256]{1,0:T(8,128)(2,1)S(1)}, u32[]{:S(2)}, u32[]{:S(2)}) collective-permute-start(bf16[1024,256]{1,0:T(8,128)(2,1)S(1)} %bitcast.94), channel_id=1, source_target_pairs={{0,2},{2,4},{4,6},{6,0},{1,3},{3,5},{5,7},{7,1},{8,10},{10,12},{12... | collective-permute-start | bytes 1572872 | tf_op jit(solution)/shard_map/ppermute | solution.py:251
  39.1 15.7 %collective-permute-start.20 = (bf16[1024,256]{1,0:T(8,128)(2,1)S(1)}, bf16[1024,256]{1,0:T(8,128)(2,1)S(1)}, u32[]{:S(2)}, u32[]{:S(2)}) collective-permute-start(bf16[1024,256]{1,0:T(8,128)(2,1)S(1)} %bitcast.95), channel_id=1, source_target_pairs={{0,6},{2,0},{4,2},{6,4},{1,7},{3,1},{5,3},{7,5},{8,14},{10,8},{12,... | collective-permute-start | bytes 1572872 | tf_op jit(solution)/shard_map/ppermute | solution.py:251
  42.2 7.8 %collective-permute-start.4 = (bf16[512,128]{1,0:T(8,128)(2,1)S(1)}, bf16[512,128]{1,0:T(8,128)(2,1)S(1)}, u32[]{:S(2)}, u32[]{:S(2)}) collective-permute-start(bf16[512,128]{1,0:T(8,128)(2,1)S(1)} %collective-permute-done.2.refs_3_), channel_id=1, source_target_pairs={{0,32},{32,64},{64,96},{96,128},{128,160},{160,192},{192,224},{224... | collective-permute-start | bytes 393224 | tf_op jit(solution)/shard_map/ppermute | solution.py:251
  42.8 8.7 %collective-permute-start.7 = (bf16[512,128]{1,0:T(8,128)(2,1)S(1)}, bf16[512,128]{1,0:T(8,128)(2,1)S(1)}, u32[]{:S(2)}, u32[]{:S(2)}) collective-permute-start(bf16[512,128]{1,0:T(8,128)(2,1)S(1)} %collective-permute-done.5.refs_6_), channel_id=1, source_target_pairs={{0,224},{32,0},{64,32},{96,64},{128,96},{160,128},{192,160},{224,1... | collective-permute-start | bytes 393224 | tf_op jit(solution)/shard_map/ppermute | solution.py:251
  47.9 8.3 %collective-permute-start.10 = (bf16[512,128]{1,0:T(8,128)(2,1)S(1)}, bf16[512,128]{1,0:T(8,128)(2,1)S(1)}, u32[]{:S(2)}, u32[]{:S(2)}) collective-permute-start(bf16[512,128]{1,0:T(8,128)(2,1)S(1)} %pad_maximum_fusion.2.refs_0_), channel_id=1, source_target_pairs={{0,16},{8,24},{16,0},{24,8},{1,17},{9,25},{17,1},{25,9},{2,18},{10... | collective-permute-start | bytes 393224 | tf_op jit(solution)/shard_map/ppermute | solution.py:251
  50.1 8.2 %collective-permute-start.11 = (bf16[512,128]{1,0:T(8,128)(2,1)S(1)}, bf16[512,128]{1,0:T(8,128)(2,1)S(1)}, u32[]{:S(2)}, u32[]{:S(2)}) collective-permute-start(bf16[512,128]{1,0:T(8,128)(2,1)S(1)} %pad_maximum_fusion.2.refs_0_), channel_id=1, source_target_pairs={{0,24},{8,0},{16,8},{24,16},{1,25},{9,1},{17,9},{25,17},{2,26},{10... | collective-permute-start | bytes 393224 | tf_op jit(solution)/shard_map/ppermute | solution.py:251
  54.8 7.8 %collective-permute-start.24 = (bf16[512,256]{1,0:T(8,128)(2,1)S(1)}, bf16[512,256]{1,0:T(8,128)(2,1)}, u32[]{:S(2)}, u32[]{:S(2)}) collective-permute-start(bf16[512,256]{1,0:T(8,128)(2,1)S(1)} %slice.70), channel_id=1, source_target_pairs={{0,2},{2,4},{4,6},{6,0},{1,3},{3,5},{5,7},{7,1},{8,10},{10,12},{12... | collective-permute-start | bytes 786440 | tf_op jit(solution)/shard_map/ppermute | solution.py:251
  58.3 32.2 %collective-permute-start.21 = (bf16[1024,256]{1,0:T(8,128)(2,1)S(1)}, bf16[1024,256]{1,0:T(8,128)(2,1)}, u32[]{:S(2)}, u32[]{:S(2)}) collective-permute-start(bf16[1024,256]{1,0:T(8,128)(2,1)S(1)} %bitcast.96), channel_id=1, source_target_pairs={{0,1},{1,0},{2,3},{3,2},{4,5},{5,4},{6,7},{7,6},{8,9},{9,8},{10,11... | collective-permute-start | bytes 1572872 | tf_op jit(solution)/shard_map/ppermute | solution.py:251
  58.3 32.3 %collective-permute-start.22 = (bf16[1024,256]{1,0:T(8,128)(2,1)S(1)}, bf16[1024,256]{1,0:T(8,128)(2,1)}, u32[]{:S(2)}, u32[]{:S(2)}) collective-permute-start(bf16[1024,256]{1,0:T(8,128)(2,1)S(1)} %collective-permute-done.19.refs_1_), channel_id=1, source_target_pairs={{0,1},{1,0},{2,3},{3,2},{4,5},{5,4},{6,7},{7,6},{8,9},{9,8},{10,11... | collective-permute-start | bytes 1572872 | tf_op jit(solution)/shard_map/ppermute | solution.py:251
  58.8 31.8 %collective-permute-start.23 = (bf16[1024,256]{1,0:T(8,128)(2,1)S(1)}, bf16[1024,256]{1,0:T(8,128)(2,1)}, u32[]{:S(2)}, u32[]{:S(2)}) collective-permute-start(bf16[1024,256]{1,0:T(8,128)(2,1)S(1)} %collective-permute-done.20.refs_2_), channel_id=1, source_target_pairs={{0,1},{1,0},{2,3},{3,2},{4,5},{5,4},{6,7},{7,6},{8,9},{9,8},{10,11... | collective-permute-start | bytes 1572872 | tf_op jit(solution)/shard_map/ppermute | solution.py:251
  62.6 28.0 %collective-permute-start.26 = (bf16[512,256]{1,0:T(8,128)(2,1)}, bf16[512,256]{1,0:T(8,128)(2,1)}, u32[]{:S(2)}, u32[]{:S(2)}) collective-permute-start(bf16[512,256]{1,0:T(8,128)(2,1)} %collective-permute-done.24.refs_6_), channel_id=1, source_target_pairs={{0,1},{1,0},{2,3},{3,2},{4,5},{5,4},{6,7},{7,6},{8,9},{9,8},{10,11... | collective-permute-start | bytes 786440 | tf_op jit(solution)/shard_map/ppermute | solution.py:251
  62.8 27.8 %collective-permute-start.27 = (bf16[512,256]{1,0:T(8,128)(2,1)}, bf16[512,256]{1,0:T(8,128)(2,1)}, u32[]{:S(2)}, u32[]{:S(2)}) collective-permute-start(bf16[512,256]{1,0:T(8,128)(2,1)} %collective-permute-done.25.refs_7_), channel_id=1, source_target_pairs={{0,1},{1,0},{2,3},{3,2},{4,5},{5,4},{6,7},{7,6},{8,9},{9,8},{10,11... | collective-permute-start | bytes 786440 | tf_op jit(solution)/shard_map/ppermute | solution.py:251
  90.5 34.3 %collective-permute-start.1 = (bf16[512,128]{1,0:T(8,128)(2,1)}, bf16[512,128]{1,0:T(8,128)(2,1)S(1)}, u32[]{:S(2)}, u32[]{:S(2)}) collective-permute-start(bf16[512,128]{1,0:T(8,128)(2,1)} %copy-done.12), channel_id=1, source_target_pairs={{0,8},{8,16},{16,24},{24,0},{1,9},{9,17},{17,25},{25,1},{2,10},{10... | collective-permute-start | bytes 393224 | tf_op jit(solution)/shard_map/ppermute | solution.py:251
  105.2 51.8 %collective-permute-start.28 = (bf16[1024,256]{1,0:T(8,128)(2,1)}, bf16[1024,256]{1,0:T(8,128)(2,1)S(1)}, u32[]{:S(2)}, u32[]{:S(2)}) collective-permute-start(bf16[1024,256]{1,0:T(8,128)(2,1)} %convolution_convert_fusion.3), channel_id=1, source_target_pairs={{0,1},{1,0},{2,3},{3,2},{4,5},{5,4},{6,7},{7,6},{8,9},{9,8},{10,11... | collective-permute-start | bytes 1572872 | tf_op jit(solution)/shard_map/ppermute | solution.py:251
  105.9 9.9 %collective-permute-start.31 = (bf16[512,256]{1,0:T(8,128)(2,1)S(1)}, bf16[512,256]{1,0:T(8,128)(2,1)S(1)}, u32[]{:S(2)}, u32[]{:S(2)}) collective-permute-start(bf16[512,256]{1,0:T(8,128)(2,1)S(1)} %get-tuple-element.4), channel_id=1, source_target_pairs={{0,2},{2,4},{4,6},{6,0},{1,3},{3,5},{5,7},{7,1},{8,10},{10,12},{12... | collective-permute-start | bytes 786440 | tf_op jit(solution)/shard_map/ppermute | solution.py:251
  107.0 9.7 %collective-permute-start.34 = (bf16[512,256]{1,0:T(8,128)(2,1)S(1)}, bf16[512,256]{1,0:T(8,128)(2,1)S(1)}, u32[]{:S(2)}, u32[]{:S(2)}) collective-permute-start(bf16[512,256]{1,0:T(8,128)(2,1)S(1)} %get-tuple-element.5), channel_id=1, source_target_pairs={{0,6},{2,0},{4,2},{6,4},{1,7},{3,1},{5,3},{7,5},{8,14},{10,8},{12,... | collective-permute-start | bytes 786440 | tf_op jit(solution)/shard_map/ppermute | solution.py:251
  116.7 40.2 %collective-permute-start.32 = (bf16[1024,256]{1,0:T(8,128)(2,1)}, bf16[1024,256]{1,0:T(8,128)(2,1)}, u32[]{:S(2)}, u32[]{:S(2)}) collective-permute-start(bf16[1024,256]{1,0:T(8,128)(2,1)} %pad_maximum_fusion), channel_id=1, source_target_pairs={{0,2},{2,4},{4,6},{6,0},{1,3},{3,5},{5,7},{7,1},{8,10},{10,12},{12... | collective-permute-start | bytes 1572872 | tf_op jit(solution)/shard_map/ppermute | solution.py:251
  117.7 39.3 %collective-permute-start.35 = (bf16[1024,256]{1,0:T(8,128)(2,1)}, bf16[1024,256]{1,0:T(8,128)(2,1)S(1)}, u32[]{:S(2)}, u32[]{:S(2)}) collective-permute-start(bf16[1024,256]{1,0:T(8,128)(2,1)} %pad_maximum_fusion.1), channel_id=1, source_target_pairs={{0,6},{2,0},{4,2},{6,4},{1,7},{3,1},{5,3},{7,5},{8,14},{10,8},{12,... | collective-permute-start | bytes 1572872 | tf_op jit(solution)/shard_map/ppermute | solution.py:251
  120.9 26.6 %collective-permute-start.12 = (bf16[2,80,512]{2,1,0:T(8,128)(2,1)S(1)}, bf16[2,80,512]{2,1,0:T(8,128)(2,1)S(1)}, u32[]{:S(2)}, u32[]{:S(2)}) collective-permute-start(bf16[2,80,512]{2,1,0:T(8,128)(2,1)S(1)} %get-tuple-element.7), channel_id=1, source_target_pairs={{0,16},{8,24},{16,0},{24,8},{1,17},{9,25},{17,1},{25,9},{2,18},{10... | collective-permute-start | bytes 491528 | tf_op jit(solution)/shard_map/ppermute | solution.py:251
  125.5 25.9 %collective-permute-start.13 = (bf16[2,80,512]{2,1,0:T(8,128)(2,1)S(1)}, bf16[2,80,512]{2,1,0:T(8,128)(2,1)S(1)}, u32[]{:S(2)}, u32[]{:S(2)}) collective-permute-start(bf16[2,80,512]{2,1,0:T(8,128)(2,1)S(1)} %get-tuple-element.6), channel_id=1, source_target_pairs={{0,8},{8,16},{16,24},{24,0},{1,9},{9,17},{17,25},{25,1},{2,10},{10... | collective-permute-start | bytes 491528 | tf_op jit(solution)/shard_map/ppermute | solution.py:251
  159.3 33.7 %all-to-all-start.1 = ((bf16[32,32,256]{2,1,0:T(8,128)(2,1)}), bf16[32,32,256]{2,1,0:T(8,128)(2,1)S(1)}, u32[]{:S(2)}, u32[]{:S(2)}) async-start(bf16[32,32,256]{2,1,0:T(8,128)(2,1)} %bitcast.30), calls=%async_computation.1 | async-start | bytes 1048576 | tf_op jit(solution)/shard_map/all_to_all | solution.py:389
  166.6 13.6 %collective-permute-start.14 = (bf16[256,128]{1,0:T(8,128)(2,1)S(1)}, bf16[256,128]{1,0:T(8,128)(2,1)S(1)}, u32[]{:S(2)}, u32[]{:S(2)}) collective-permute-start(bf16[256,128]{1,0:T(8,128)(2,1)S(1)} %get-tuple-element.17), channel_id=1, source_target_pairs={{0,224},{32,192},{64,160},{96,128},{128,96},{160,64},{192,32},{224... | collective-permute-start | bytes 196616 | tf_op jit(solution)/shard_map/ppermute | solution.py:256
  (43 other events, 710.7 us)

commit v4 on v3

v4 whole, which is shorter than its diff:
```python
import functools

import jax
import jax.numpy as jnp
from jax import lax
from jax.experimental import pallas as pl
from jax.experimental.pallas import tpu as pltpu
from jax.sharding import Mesh
from jax.sharding import PartitionSpec as P


EP = ("z", "x")
TP = ("y", "c")
epsilon = 1e-06
clamp_limit = 7.0
sigmoid_slope = 1.702


BLK = 512
NEG = -1e30
SMEM = pl.BlockSpec(memory_space=pltpu.SMEM)
VMEM = pl.BlockSpec(memory_space=pltpu.VMEM)
KEYS_FROM = (0, 7, 1, 6, 2, 5, 3, 4)


def pieces_of(values):
    high = values.astype(jnp.bfloat16).astype(jnp.float32)
    rest = values - high
    middle = rest.astype(jnp.bfloat16).astype(jnp.float32)
    return high, middle, rest - middle


def attend_kernel(first, place, *refs):
    q_refs, kv_refs = refs[:2], refs[2:10]
    gate_ref, near_ref, next_ref, kaug, vaug, qaug, held, acc, top, knorm = refs[10:]
    turn = pl.program_id(0)
    step = turn + first
    zed, ex = place[0], place[1]
    blocks = len(kv_refs)
    home = (ex - step) & 3
    half = BLK // 2

    @pl.when(turn == 0)
    def _prepare():
        one = jnp.ones((blocks, BLK), jnp.float32)
        rows = [jnp.zeros((64, BLK), jnp.float32)]
        spans = [
            gate_ref[:, pl.ds(pl.multiple_of((4 * b + ex) * BLK, BLK), BLK)] for b in range(blocks)
        ]
        for h in range(2):
            rows += list(pieces_of(-jnp.concatenate([span[h : h + 1] for span in spans], axis=0)))
        rows += [one, one]
        table = jnp.concatenate(rows, axis=0).T
        lane = lax.broadcasted_iota(jnp.int32, (BLK, 128), 1)
        tail = jnp.where(lax.broadcasted_iota(jnp.int32, (16, BLK), 0) == 0, 1.0, 0.0)
        most = jnp.zeros((1, BLK), jnp.float32)
        for kv_ref, away in zip(kv_refs, KEYS_FROM):
            b = (zed + away) & 7
            block = kv_ref[...].astype(jnp.float32)
            kaug[b] = jnp.where(
                lane < 64, block, jnp.where((lane & 7) == b, table, 0.0)
            ).astype(jnp.bfloat16)
            turned = block.T
            vaug[b] = jnp.concatenate([turned[64:], tail], axis=0).astype(jnp.bfloat16)
            keys = turned[:64]
            most = jnp.maximum(most, jnp.sum(keys * keys, axis=0, keepdims=True))
        knorm[0] = jnp.max(most)

    q_now = jnp.where(turn == 0, q_refs[0][...], q_refs[1][...])
    q_turned = q_now.astype(jnp.float32).T * 0.125
    q_most = jnp.maximum(
        jnp.max(jnp.sum(q_turned[:64] * q_turned[:64], axis=0, keepdims=True)),
        jnp.max(jnp.sum(q_turned[64:] * q_turned[64:], axis=0, keepdims=True)),
    )
    calm = q_most * knorm[0] <= 1600.0
    low_at = (4 * zed + home) * BLK
    high_at = (4 * (blocks - 1 - zed) + home) * BLK + half
    gates = jnp.concatenate(
        [gate_ref[:, pl.ds(pl.multiple_of(at, half), half)] for at in (low_at, high_at)], axis=1
    )
    for h in range(2):
        gate = gates[h : h + 1]
        high, low, _ = pieces_of(gate)
        on, off = jnp.ones((24, BLK), jnp.float32), jnp.zeros((24, BLK), jnp.float32)
        whole = jnp.concatenate(
            [
                q_turned[64 * h : 64 * h + 64],
                on if h == 0 else off,
                on if h == 1 else off,
                jnp.broadcast_to(high, (8, BLK)),
                jnp.broadcast_to(low, (8, BLK)),
            ],
            axis=0,
        ).astype(jnp.bfloat16)
        for part in range(2):
            qaug[part, h] = whole[:, part * half : part * half + half]
    acc[...] = jnp.zeros_like(acc)
    after = jnp.where(ex < home, 1, 0)
    low_count = zed + after
    count = blocks - 1 + 2 * after

    def unit(i):
        first = i < low_count
        return jnp.where(first, 0, 1), jnp.where(first, i, i - low_count)

    def scores_of(part, b, h):
        return jnp.dot(kaug[b], qaug[part, h], preferred_element_type=jnp.float32)

    def add(part, b, h, weights):
        acc[part, h] += jnp.dot(
            vaug[b], weights.astype(jnp.bfloat16), preferred_element_type=jnp.float32
        )

    def seen_of(part):
        return lax.broadcasted_iota(jnp.int32, (BLK, half), 0) <= (
            lax.broadcasted_iota(jnp.int32, (BLK, half), 1) + part * half
        )

    @pl.when(calm)
    def _calm():
        top[...] = jnp.zeros_like(top)
        part, b = unit(0)
        for h in range(2):
            held[h] = scores_of(part, b, h)

        def one(i, carry):
            part, b = unit(i)
            next_part, next_b = unit(jnp.minimum(i + 1, count - 1))
            for h in range(2):
                weights = jnp.exp(held[h])
                held[h] = scores_of(next_part, next_b, h)
                add(part, b, h, weights)
            return carry

        lax.fori_loop(0, count, one, 0)

        def edge(part):
            b = jnp.where(part == 0, zed, blocks - 1 - zed)
            for h in range(2):
                add(part, b, h, jnp.exp(jnp.where(seen_of(part), scores_of(part, b, h), NEG)))

        if first == 0:
            lax.fori_loop(0, jnp.where(turn == 0, 2, 0), lambda part, c: (edge(part), c)[1], 0)

    @pl.when(jnp.logical_not(calm))
    def _wild():
        top[...] = jnp.full_like(top, NEG)
        low_all = zed + jnp.where(ex <= home, 1, 0)

        def one(i, carry):
            h, n = i & 1, i >> 1
            part = jnp.where(n < low_all, 0, 1)
            b = n - part * low_all
            edge = (step == 0) & (b == jnp.where(part == 0, zed, blocks - 1 - zed))
            seen = seen_of(part + jnp.where(edge, 0, 4))
            scores = jnp.where(seen, scores_of(part, b, h), NEG)
            old = top[part, h]
            new = jnp.maximum(old, jnp.max(scores, axis=0, keepdims=True))
            top[part, h] = new
            acc[part, h] = acc[part, h] * jnp.exp(old - new)
            add(part, b, h, jnp.where(seen, jnp.exp(scores - new), 0.0))
            return carry

        lax.fori_loop(0, 2 * (blocks - 1 + 2 * jnp.where(ex <= home, 1, 0)), one, 0)

    for n, o_ref in enumerate((near_ref, next_ref)):

        @pl.when(turn == n)
        def _store(o_ref=o_ref):
            for h in range(2):
                for part in range(2):
                    rows = list(pieces_of(acc[part, h, 64:65])) + list(pieces_of(top[part, h]))
                    rows.append(jnp.zeros((10, half), jnp.float32))
                    o_ref[h, :, part * half : part * half + half] = jnp.concatenate(
                        [acc[part, h, :64]] + rows, axis=0
                    ).astype(jnp.bfloat16)


def attend(first, place, q_pair, kv_list, gates):
    n = len(kv_list)
    half = BLK // 2
    return pl.pallas_call(
        functools.partial(attend_kernel, first),
        grid_spec=pltpu.PrefetchScalarGridSpec(
            num_scalar_prefetch=1,
            grid=(2,),
            in_specs=[VMEM] * (3 + n),
            out_specs=[VMEM] * 2,
            scratch_shapes=[
                pltpu.VMEM((n, BLK, 128), jnp.bfloat16),
                pltpu.VMEM((n, 80, BLK), jnp.bfloat16),
                pltpu.VMEM((2, 2, 128, half), jnp.bfloat16),
                pltpu.VMEM((2, BLK, half), jnp.float32),
                pltpu.VMEM((2, 2, 80, half), jnp.float32),
                pltpu.VMEM((2, 2, 1, half), jnp.float32),
                pltpu.SMEM((1,), jnp.float32),
            ],
        ),
        out_shape=[jax.ShapeDtypeStruct((2, 80, BLK), jnp.bfloat16)] * 2,
        name="attend",
    )(place, *q_pair, *kv_list, gates)


def merge_kernel(*refs):
    parts, o_ref = refs[:4], refs[4]
    outs = []
    for h in range(2):
        peaks, totals = [], []
        for part in parts:
            side = part[h, 64:80].astype(jnp.float32)
            totals.append(side[0:1] + side[1:2] + side[2:3])
            peaks.append(side[3:4] + side[4:5] + side[5:6])
        peak = functools.reduce(jnp.maximum, peaks)
        factors = [jnp.exp(p - peak) for p in peaks]
        total = sum(f * t for f, t in zip(factors, totals))
        value = sum(f * part[h, :64].astype(jnp.float32) for part, f in zip(parts, factors))
        outs.append(value / total)
    o_ref[...] = jnp.concatenate(outs, axis=0).T.astype(jnp.bfloat16)


def merge(parts):
    return pl.pallas_call(
        merge_kernel,
        in_specs=[VMEM] * 4,
        out_specs=VMEM,
        out_shape=jax.ShapeDtypeStruct((BLK, 128), jnp.bfloat16),
        name="merge",
    )(*parts)


def project_kernel(place, *refs):
    pieces, (gain_ref, weight_ref, out_ref) = refs[:4], refs[4:]
    lefts = [piece[s].astype(jnp.float32) for piece in pieces for s in range(2)]
    order = [
        2 * ((place[2] - by) & 3) + (place[3] if s == 0 else 1 - place[3])
        for by in range(4)
        for s in range(2)
    ]
    squares = sum(jnp.sum(left * left, axis=1, keepdims=True) for left in lefts)
    inverse = lax.rsqrt(squares * (1.0 / 1024.0) + epsilon)
    total = None
    for j, left in zip(order, lefts):
        normed = (left * inverse * gain_ref[pl.ds(j, 1), :]).astype(jnp.bfloat16)
        rows = pl.ds(pl.multiple_of(j * 128, 128), 128)
        term = jnp.dot(normed, weight_ref[rows, :], preferred_element_type=jnp.float32)
        total = term if total is None else total + term
    out_ref[...] = total.astype(jnp.bfloat16)


def project(place, pieces, gain, weight):
    return pl.pallas_call(
        project_kernel,
        in_specs=[SMEM] + [VMEM] * 6,
        out_specs=VMEM,
        out_shape=jax.ShapeDtypeStruct((64, 2048), jnp.bfloat16),
        name="project",
    )(place, *pieces, gain.reshape(8, 128), weight)


def prepare_kernel(place, token_ref, gain_ref, route_ref, logit_ref, out_ref, table_ref):
    why, core = place[2], place[3]
    tokens = token_ref[...].astype(jnp.float32)
    rows, width = tokens.shape
    mean = jnp.sum(tokens * tokens, axis=1, keepdims=True) * (1.0 / width)
    columns = pl.ds(pl.multiple_of(why * 512, 512), 512)
    own = token_ref[:, columns].astype(jnp.float32)
    own = (own * lax.rsqrt(mean + epsilon) * gain_ref[:, columns]).astype(jnp.bfloat16)

    routes, logits = route_ref[...], logit_ref[...]
    raised = jnp.exp(logits - jnp.max(logits, axis=1, keepdims=True))
    weights = raised / jnp.sum(raised, axis=1, keepdims=True)
    number = lax.broadcasted_iota(jnp.int32, (rows, 32), 1)
    named = jnp.zeros((rows, 32), jnp.float32)
    share = jnp.zeros((rows, 32), jnp.float32)
    for k in range(4):
        same = routes[:, k : k + 1] == number
        named = jnp.where(same, 1.0, named)
        share = jnp.where(same, weights[:, k : k + 1], share)
    earlier = lax.broadcasted_iota(jnp.int32, (rows, rows), 0) > lax.broadcasted_iota(
        jnp.int32, (rows, rows), 1
    )
    slot = jnp.dot(
        jnp.where(earlier, 1.0, 0.0).astype(jnp.bfloat16),
        named.astype(jnp.bfloat16),
        preferred_element_type=jnp.float32,
    )
    position = lax.broadcasted_iota(jnp.int32, (32, 512), 1)
    widen = jnp.where(
        (position >> 4) == lax.broadcasted_iota(jnp.int32, (32, 512), 0), 1.0, 0.0
    ).astype(jnp.bfloat16)

    def widened(values):
        return jnp.dot(values.astype(jnp.bfloat16), widen, preferred_element_type=jnp.float32)

    wanted = (lax.broadcasted_iota(jnp.int32, (rows, 512), 1) & 15) + 16 * core + 1
    hit = widened(named * (slot + 1.0)) == wanted.astype(jnp.float32)
    onehot = jnp.where(hit, 1.0, 0.0)
    out_ref[...] = jnp.dot(
        onehot.T.astype(jnp.bfloat16), own, preferred_element_type=jnp.float32
    ).astype(jnp.bfloat16)
    high, low, _ = pieces_of(share)
    for n, piece in enumerate((high, low)):
        table_ref[n] = jnp.where(hit, widened(piece), 0.0).astype(jnp.bfloat16)


def prepare(place, tokens, gain, routes, logits):
    return pl.pallas_call(
        prepare_kernel,
        in_specs=[SMEM] + [VMEM] * 4,
        out_specs=[VMEM] * 2,
        out_shape=[
            jax.ShapeDtypeStruct((512, 512), jnp.bfloat16),
            jax.ShapeDtypeStruct((2, 128, 512), jnp.bfloat16),
        ],
        name="prepare",
    )(place, tokens, gain.reshape(1, -1), routes, logits)


def combine_kernel(place, table_ref, value_ref, keep_ref, send_ref):
    values = value_ref[...]
    total = sum(
        jnp.dot(table_ref[n], values, preferred_element_type=jnp.float32) for n in range(2)
    )
    first = place[3] == 0
    keep_ref[...] = jnp.where(first, total[:, :256], total[:, 256:])
    send_ref[...] = jnp.where(first, total[:, 256:], total[:, :256])


def combine(place, table, values):
    return pl.pallas_call(
        combine_kernel,
        in_specs=[SMEM] + [VMEM] * 2,
        out_specs=[VMEM] * 2,
        out_shape=[jax.ShapeDtypeStruct((128, 256), jnp.float32)] * 2,
        name="combine",
    )(place, table, values)


def experts_kernel(place, *refs):
    near, (top_ref, bottom_ref), weights = refs[:3], refs[3:5], refs[5:11]
    gates, ups, downs = weights[:2], weights[2:4], weights[4:]
    far_top, far_bottom, after_ref, before_ref, kept_ref = refs[11:]
    turn = pl.program_id(0)
    why = place[2]
    tile = pl.ds(pl.multiple_of(turn * 256, 256), 256)
    lefts = [piece[tile, :] for piece in near]
    lefts.append(jnp.where(turn == 0, top_ref[...], bottom_ref[...]))
    rows = [pl.ds(pl.multiple_of(((why - by) & 3) * 512, 512), 512) for by in (0, 1, 3, 2)]
    hidden = []
    for gate_ref, up_ref in zip(gates, ups):
        gate, up = (
            sum(
                jnp.dot(left, ref[row, :], preferred_element_type=jnp.float32)
                for left, row in zip(lefts, rows)
            )
            for ref in (gate_ref, up_ref)
        )
        gate = jnp.minimum(gate, clamp_limit)
        up = jnp.clip(up, -clamp_limit, clamp_limit)
        hidden.append(
            ((up + 1.0) * gate * jax.nn.sigmoid(sigmoid_slope * gate)).astype(jnp.bfloat16)
        )

    def partial(by):
        columns = pl.ds(pl.multiple_of(((why + by) & 3) * 512, 512), 512)
        return sum(
            jnp.dot(part, ref[:, columns], preferred_element_type=jnp.float32)
            for part, ref in zip(hidden, downs)
        ).astype(jnp.bfloat16)

    distant = partial(2)

    @pl.when(turn == 0)
    def _top():
        far_top[...] = distant

    @pl.when(turn == 1)
    def _bottom():
        far_bottom[...] = distant

    after_ref[tile, :] = partial(1)
    before_ref[tile, :] = partial(3)
    kept_ref[tile, :] = partial(0)


def experts(place, near, far, weights):
    shapes = [jax.ShapeDtypeStruct((n, 512), jnp.bfloat16) for n in (256, 256, 512, 512, 512)]
    return pl.pallas_call(
        experts_kernel,
        grid_spec=pltpu.PrefetchScalarGridSpec(
            num_scalar_prefetch=1,
            grid=(2,),
            in_specs=[VMEM] * 11,
            out_specs=[VMEM] * 5,
        ),
        out_shape=shapes,
        name="experts",
    )(place, *near, *far, *weights)


def shift(array, axis, by):
    count = lax.axis_size(axis)
    return lax.ppermute(array, axis, [(i, (i + by) % count) for i in range(count)])


def mirror(array):
    count = lax.axis_size("z")
    return lax.ppermute(array, "z", [(i, count - 1 - i) for i in range(count)])


def body(
    queries,
    keys_values,
    forget_cache,
    heads_gain,
    output_weight,
    expert_tokens,
    expert_gain,
    routes,
    route_logits,
    gate_weight,
    up_weight,
    down_weight,
):
    why, core = lax.axis_index("y"), lax.axis_index("c")
    place = jnp.stack([lax.axis_index("z"), lax.axis_index("x"), why, core]).astype(jnp.int32)
    middle = BLK // 2

    turned = mirror(queries[middle:])
    q = jnp.concatenate([queries[:middle], turned], axis=0)
    q_list = [q] + [shift(q, "x", by) for by in (1, 2, 3)]
    ups, downs = [keys_values], [keys_values]
    for _ in range(3):
        ups.append(shift(ups[-1], "z", 1))
    for _ in range(4):
        downs.append(shift(downs[-1], "z", 7))
    kv_list = [keys_values, ups[1], downs[1], ups[2], downs[2], ups[3], downs[3], downs[4]]

    outgoing, table = prepare(place, expert_tokens, expert_gain, routes, route_logits)
    arrived = lax.all_to_all(outgoing.reshape(32, 16, 512), EP, 0, 0, tiled=True)
    arrived = arrived.reshape(512, 512)
    weights = []
    for weight in (gate_weight[0], up_weight[0], down_weight[0]):
        weights += [weight, shift(weight, "c", 1)]
    left, right = shift(arrived, "y", 1), shift(arrived, "y", 3)
    far = [shift(left[:middle], "y", 1), shift(right[middle:], "y", 3)]
    top, bottom, after, before, kept = experts(place, [arrived, left, right], far, weights)
    first, second = shift(top, "y", 1), shift(bottom, "y", 3)

    def joined(a, b):
        return (a.astype(jnp.float32) + b.astype(jnp.float32)).astype(jnp.bfloat16)

    after = jnp.concatenate([joined(after[:middle], first), after[middle:]], axis=0)
    before = jnp.concatenate([before[:middle], joined(before[middle:], second)], axis=0)
    moved = [kept, shift(after, "y", 1)]
    moved.append(shift(before, "y", 3))
    expert_out = sum(m.astype(jnp.float32) for m in moved).astype(jnp.bfloat16)

    parts = attend(0, place, q_list[:2], kv_list, forget_cache)
    parts = [parts[0], shift(parts[1], "x", 3)]
    rest = attend(2, place, q_list[2:], kv_list, forget_cache)
    parts += [shift(rest[0], "x", 2), shift(rest[1], "x", 1)]
    returned = lax.all_to_all(expert_out.reshape(32, 16, 512), EP, 0, 0, tiled=True)
    attended = merge(parts)
    turned = mirror(attended[middle:])
    attended = jnp.concatenate([attended[:middle], turned], axis=0)
    attended = attended.reshape(4, 2, 64, 128)
    twin = shift(lax.dynamic_index_in_dim(attended, 1 - core, 1, keepdims=False), "c", 1)
    mine = lax.dynamic_index_in_dim(attended, core, 1, keepdims=False)
    both = jnp.stack([mine, twin], axis=1)
    slices = []
    for by in range(4):
        piece = lax.dynamic_index_in_dim(both, (why + by) & 3, 0, keepdims=False)
        slices.append(shift(piece, "y", by) if by else piece)
    mixer_out = project(place, slices, heads_gain, output_weight)

    keep, send = combine(place, table, returned.reshape(512, 512))
    moe_out = (keep + shift(send, "c", 1)).astype(jnp.bfloat16)
    return (mixer_out, moe_out)


def solution(mesh):
    torus = Mesh(mesh.devices.reshape(8, 4, 4, 2), ("z", "x", "y", "c"))
    return jax.shard_map(
        body,
        mesh=torus,
        in_specs=(
            P(EP, TP),
            P(EP, TP),
            P(TP, None),
            P(),
            P(),
            P(EP, None),
            P(),
            P(EP, None),
            P(EP, None),
            P(EP, None, TP),
            P(EP, None, TP),
            P(EP, TP, None),
        ),
        out_specs=(P(EP + TP, None), P(EP, TP)),
        check_vma=False,
    )
```

time: 195 us -> 197 us (1.010); the launches traced: 194 us -> 193 us
  matrix products: 13 us -> 0 us
  waiting for transfers between devices: 40.9 us -> 51.4 us
  Pallas kernels: 55.6 us -> 62.2 us
  other arithmetic: 9.06 us -> 5.06 us
  starting transfers between devices: 64.8 us -> 62.7 us
    ppermute x34 -> x29, waiting for transfers between devices: 14.5 us -> 32.8 us  [shift(): lax.ppermute(array, axis, [(i, (i + by) % count) for i in range(count)])]
    dot_general x12 -> x0, matrix products: 13 us -> none  [the longest x8 9.68 us: partial(): return jnp.dot(hidden, part, preferred_element_type=jnp.float32)]
    ppermute x2, waiting for transfers between devices: 12.4 us -> 2.5 us  [mirror(): return lax.ppermute(array, 'z', [(i, count - 1 - i) for i in range(count)])]
    pallas_call x3 -> x5, Pallas kernels: 13 us -> 19.9 us  [the longest x1 9.22 us: experts(): pl.pallas_call(experts_kernel, grid_spec=pltpu.PrefetchScalarGridSpec(num...]
    ppermute x34 -> x29, starting transfers between devices: 43.7 us -> 37 us  [shift(): lax.ppermute(array, axis, [(i, (i + by) % count) for i in range(count)])]
    unnamed x59 -> x58, local copies, waits for them, and re-layouts: 3.52 us -> 7.6 us
    convert_element_type x3 -> x4, other arithmetic: 0.14 us -> 3.69 us  [the longest x2 2.03 us: joined(): return (a.astype(jnp.float32) + b.astype(jnp.float32)).astype(jnp.bfloat16)]
    all_to_all x2, starting transfers between devices: 18.1 us -> 21.3 us  [the longest x1 11.6 us: body(): lax.all_to_all(outgoing.reshape(32, 16, 512), EP, 0, 0, tiled=True)]
  transfers between devices with their start and end apart: 38 -> 33, of which waited for: 11 -> 12; matrix products, arithmetic and copies ran while one was open for 11% -> 3% of each run, Pallas kernels for 29% -> 26%
where the time goes in v4:
time: 197 us; the launch traced here: 193 us
  starting transfers between devices  62.7 us (32%)
  Pallas kernels  62.2 us (32%)
  waiting for transfers between devices  51.4 us (26%)
  local copies, waits for them, and re-layouts  10.6 us (5%)
  other arithmetic  5.06 us (3%)
    pallas_call x2, Pallas kernels, attend(): pl.pallas_call(functools.partial(attend_kernel, first), grid_spec=pltpu.P...  42.3 us
    ppermute x29, starting transfers between devices, shift(): lax.ppermute(array, axis, [(i, (i + by) % count) for i in range(count)])  37 us
    ppermute x29, waiting for transfers between devices, shift(): lax.ppermute(array, axis, [(i, (i + by) % count) for i in range(count)])  32.8 us
    all_to_all x1, waiting for transfers between devices, body(): lax.all_to_all(outgoing.reshape(32, 16, 512), EP, 0, 0, tiled=True)  16.1 us
    all_to_all x1, starting transfers between devices, body(): lax.all_to_all(outgoing.reshape(32, 16, 512), EP, 0, 0, tiled=True)  11.6 us
    all_to_all x1, starting transfers between devices, body(): lax.all_to_all(expert_out.reshape(32, 16, 512), EP, 0, 0, tiled=True)  9.73 us
    pallas_call x1, Pallas kernels, experts(): pl.pallas_call(experts_kernel, grid_spec=pltpu.PrefetchScalarGridSpec(num...  9.22 us
    unnamed x58, local copies, waits for them, and re-layouts  7.6 us
  transfers between devices with their start and end apart: 33, of which 12 were waited for; matrix products, arithmetic and copies ran while one was open for 3% of the time, Pallas kernels for 26%

profile of v4, /device:TPU:2, one launch (start us, length us, event | category | flops | bytes accessed | tf_op | source)
XLA Modules:
  0.0 193.0 jit_solution(16878525046209418314)
XLA Ops:
  4.1 2.8 %prepare.1 = (bf16[512,512]{1,0:T(8,128)(2,1)}, bf16[2,128,512]{2,1,0:T(8,128)(2,1)}) custom-call(s32[4]{0:T(128)} %pad_add_fusion.place, bf16[128,2048]{1,0:T(8,128)(2,1)} %token_ref.1, f32[1,2048]{1,0:T(1,128)} %bitcast.38, s32[128,4]{1,0:T(8,128)} %copy.14.route_ref, f32[128,4]{1,0:T(8,128)} %copy.15.logit_ref), custom_call_target="tpu_custom_call" | custom-call | tf_op jit(solution)/shard_map/prepare/pallas_call | solution.py:307
  6.9 11.6 %all-to-all-start = ((bf16[32,16,512]{2,1,0:T(8,128)(2,1)}), bf16[32,16,512]{2,1,0:T(8,128)(2,1)S(1)}, u32[]{:S(2)}, u32[]{:S(2)}) async-start(bf16[32,16,512]{2,1,0:T(8,128)(2,1)} %bitcast.35), calls=%async_computation | async-start | bytes 1048576 | tf_op jit(solution)/shard_map/all_to_all | solution.py:440
  19.2 16.1 %all-to-all-done = bf16[32,16,512]{2,1,0:T(8,128)(2,1)S(1)} async-done(((bf16[32,16,512]{2,1,0:T(8,128)(2,1)}), bf16[32,16,512]{2,1,0:T(8,128)(2,1)S(1)}, u32[]{:S(2)}, u32[]{:S(2)}) %all-to-all-start) | async-done | bytes 524320 | tf_op jit(solution)/shard_map/all_to_all | solution.py:440
  38.6 10.4 %collective-permute-done.19.refs_1_ = bf16[512,512]{1,0:T(8,128)(2,1)S(1)} collective-permute-done((bf16[512,512]{1,0:T(8,128)(2,1)S(1)}, bf16[512,512]{1,0:T(8,128)(2,1)S(1)}, u32[]{:S(2)}, u32[]{:S(2)}) %collective-permute-start.19) | collective-permute-done | bytes 524320 | tf_op jit(solution)/shard_map/ppermute | solution.py:403
  49.4 3.0 %collective-permute-start.22 = (bf16[256,512]{1,0:T(8,128)(2,1)S(1)}, bf16[256,512]{1,0:T(8,128)(2,1)S(1)}, u32[]{:S(2)}, u32[]{:S(2)}) collective-permute-start(bf16[256,512]{1,0:T(8,128)(2,1)S(1)} %slice.43), channel_id=1, source_target_pairs={{0,6},{2,0},{4,2},{6,4},{1,7},{3,1},{5,3},{7,5},{8,14},{10,8},{12,... | collective-permute-start | bytes 786440 | tf_op jit(solution)/shard_map/ppermute | solution.py:403
  52.4 4.2 %collective-permute-done.21.refs_3_ = bf16[256,512]{1,0:T(8,128)(2,1)S(1)} collective-permute-done((bf16[256,512]{1,0:T(8,128)(2,1)S(1)}, bf16[256,512]{1,0:T(8,128)(2,1)S(1)}, u32[]{:S(2)}, u32[]{:S(2)}) %collective-permute-start.21) | collective-permute-done | bytes 262176 | tf_op jit(solution)/shard_map/ppermute | solution.py:403
  58.0 9.2 %experts.1 = (bf16[256,512]{1,0:T(8,128)(2,1)}, bf16[256,512]{1,0:T(8,128)(2,1)}, bf16[512,512]{1,0:T(8,128)(2,1)}, bf16[512,512]{1,0:T(8,128)(2,1)}, bf16[512,512]{1,0:T(8,128)(2,1)}) custom-call(s32[4]{0:T(128)} %pad_add_fusion.place, bf16[512,512]{1,0:T(8,128)(2,1)} %bitcast.27, bf16[512,512]{1,0:T(8,128)(2,1)} %copy-done.2, bf16[512,512]{1,0:T(8,128)(2,1)} %copy-done.3, ...), custom_call_target="tpu_custom_call" | custom-call | tf_op jit(solution)/shard_map/experts/pallas_call | solution.py:388
  68.5 3.1 %collective-permute-start.28 = (bf16[256,512]{1,0:T(8,128)(2,1)}, bf16[256,512]{1,0:T(8,128)(2,1)S(1)}, u32[]{:S(2)}, u32[]{:S(2)}) collective-permute-start(bf16[256,512]{1,0:T(8,128)(2,1)} %get-tuple-element.25), channel_id=1, source_target_pairs={{0,6},{2,0},{4,2},{6,4},{1,7},{3,1},{5,3},{7,5},{8,14},{10,8},{12,... | collective-permute-start | bytes 786440 | tf_op jit(solution)/shard_map/ppermute | solution.py:403
  72.6 2.5 %collective-permute-done.26 = bf16[256,512]{1,0:T(8,128)(2,1)S(1)} collective-permute-done((bf16[256,512]{1,0:T(8,128)(2,1)}, bf16[256,512]{1,0:T(8,128)(2,1)S(1)}, u32[]{:S(2)}, u32[]{:S(2)}) %collective-permute-start.26) | collective-permute-done | bytes 262176 | tf_op jit(solution)/shard_map/ppermute | solution.py:403
  77.4 3.3 %collective-permute-start.29 = (bf16[512,512]{1,0:T(8,128)(2,1)S(1)}, bf16[512,512]{1,0:T(8,128)(2,1)S(1)}, u32[]{:S(2)}, u32[]{:S(2)}) collective-permute-start(bf16[512,512]{1,0:T(8,128)(2,1)S(1)} %pad_maximum_fusion.1), channel_id=1, source_target_pairs={{0,6},{2,0},{4,2},{6,4},{1,7},{3,1},{5,3},{7,5},{8,14},{10,8},{12,... | collective-permute-start | bytes 1572872 | tf_op jit(solution)/shard_map/ppermute | solution.py:403
  85.7 2.7 %collective-permute-start.5 = (bf16[512,128]{1,0:T(8,128)(2,1)S(1)}, bf16[512,128]{1,0:T(8,128)(2,1)S(1)}, u32[]{:S(2)}, u32[]{:S(2)}) collective-permute-start(bf16[512,128]{1,0:T(8,128)(2,1)S(1)} %collective-permute-done.3.refs_4_), channel_id=1, source_target_pairs={{0,224},{32,0},{64,32},{96,64},{128,96},{160,128},{192,160},{224,1... | collective-permute-start | bytes 393224 | tf_op jit(solution)/shard_map/ppermute | solution.py:403
  89.4 9.7 %all-to-all-start.1 = ((bf16[32,16,512]{2,1,0:T(8,128)(2,1)}), bf16[32,16,512]{2,1,0:T(8,128)(2,1)S(1)}, u32[]{:S(2)}, u32[]{:S(2)}) async-start(bf16[32,16,512]{2,1,0:T(8,128)(2,1)} %bitcast.18), calls=%async_computation.1 | async-start | bytes 1048576 | tf_op jit(solution)/shard_map/all_to_all | solution.py:463
  99.2 2.8 %collective-permute-start.7 = (bf16[512,128]{1,0:T(8,128)(2,1)S(1)}, bf16[512,128]{1,0:T(8,128)(2,1)S(1)}, u32[]{:S(2)}, u32[]{:S(2)}) collective-permute-start(bf16[512,128]{1,0:T(8,128)(2,1)S(1)} %collective-permute-done.5.refs_6_), channel_id=1, source_target_pairs={{0,224},{32,0},{64,32},{96,64},{128,96},{160,128},{192,160},{224,1... | collective-permute-start | bytes 393224 | tf_op jit(solution)/shard_map/ppermute | solution.py:403
  102.0 2.2 %collective-permute-start.10 = (bf16[512,128]{1,0:T(8,128)(2,1)S(1)}, bf16[512,128]{1,0:T(8,128)(2,1)S(1)}, u32[]{:S(2)}, u32[]{:S(2)}) collective-permute-start(bf16[512,128]{1,0:T(8,128)(2,1)S(1)} %pad_maximum_fusion.2.refs_0_), channel_id=1, source_target_pairs={{0,16},{8,24},{16,0},{24,8},{1,17},{9,25},{17,1},{25,9},{2,18},{10... | collective-permute-start | bytes 393224 | tf_op jit(solution)/shard_map/ppermute | solution.py:403
  105.6 5.0 %collective-permute-done.7.refs_8_ = bf16[512,128]{1,0:T(8,128)(2,1)S(1)} collective-permute-done((bf16[512,128]{1,0:T(8,128)(2,1)S(1)}, bf16[512,128]{1,0:T(8,128)(2,1)S(1)}, u32[]{:S(2)}, u32[]{:S(2)}) %collective-permute-start.7) | collective-permute-done | bytes 131104 | tf_op jit(solution)/shard_map/ppermute | solution.py:403
  116.3 22.1 %attend.3 = (bf16[2,80,512]{2,1,0:T(8,128)(2,1)}, bf16[2,80,512]{2,1,0:T(8,128)(2,1)}) custom-call(s32[4]{0:T(128)} %pad_add_fusion.place, bf16[512,128]{1,0:T(8,128)(2,1)} %copy-done.23, bf16[512,128]{1,0:T(8,128)(2,1)} %copy-done.24, bf16[512,128]{1,0:T(8,128)(2,1)} %refs_2_.3, bf16[512,128]{1,0:T(8,128)(2,1)} %copy-done.9, bf16[512,128]{1,0:T(8,128)(2,1)} %copy-done.8, ...), custom_call_target="tpu_custom_call" | custom-call | tf_op jit(solution)/shard_map/attend/pallas_call | solution.py:182
  141.2 20.2 %attend.2 = (bf16[2,80,512]{2,1,0:T(8,128)(2,1)}, bf16[2,80,512]{2,1,0:T(8,128)(2,1)}) custom-call(s32[4]{0:T(128)} %pad_add_fusion.place, bf16[512,128]{1,0:T(8,128)(2,1)} %copy-done.6, bf16[512,128]{1,0:T(8,128)(2,1)} %copy-done.22, bf16[512,128]{1,0:T(8,128)(2,1)} %refs_2_.3, bf16[512,128]{1,0:T(8,128)(2,1)} %copy-done.9, bf16[512,128]{1,0:T(8,128)(2,1)} %copy-done.8, ...), custom_call_target="tpu_custom_call" | custom-call | tf_op jit(solution)/shard_map/attend/pallas_call | solution.py:182
  161.3 2.3 %collective-permute-start.9 = (bf16[2,80,512]{2,1,0:T(8,128)(2,1)}, bf16[2,80,512]{2,1,0:T(8,128)(2,1)S(1)}, u32[]{:S(2)}, u32[]{:S(2)}) collective-permute-start(bf16[2,80,512]{2,1,0:T(8,128)(2,1)} %get-tuple-element.16), channel_id=1, source_target_pairs={{0,24},{8,0},{16,8},{24,16},{1,25},{9,1},{17,9},{25,17},{2,26},{10... | collective-permute-start | bytes 491528 | tf_op jit(solution)/shard_map/ppermute | solution.py:403
  163.6 3.3 %collective-permute-done.9.refs_1_ = bf16[2,80,512]{2,1,0:T(8,128)(2,1)S(1)} collective-permute-done((bf16[2,80,512]{2,1,0:T(8,128)(2,1)}, bf16[2,80,512]{2,1,0:T(8,128)(2,1)S(1)}, u32[]{:S(2)}, u32[]{:S(2)}) %collective-permute-start.9) | collective-permute-done | bytes 163872 | tf_op jit(solution)/shard_map/ppermute | solution.py:403
  170.5 3.1 %collective-permute-start.14 = (bf16[256,128]{1,0:T(8,128)(2,1)S(1)}, bf16[256,128]{1,0:T(8,128)(2,1)S(1)}, u32[]{:S(2)}, u32[]{:S(2)}) collective-permute-start(bf16[256,128]{1,0:T(8,128)(2,1)S(1)} %get-tuple-element.35), channel_id=1, source_target_pairs={{0,224},{32,192},{64,160},{96,128},{128,96},{160,64},{192,32},{224... | collective-permute-start | bytes 196616 | tf_op jit(solution)/shard_map/ppermute | solution.py:408
  173.5 2.5 %collective-permute-done.14 = bf16[256,128]{1,0:T(8,128)(2,1)S(1)} collective-permute-done((bf16[256,128]{1,0:T(8,128)(2,1)S(1)}, bf16[256,128]{1,0:T(8,128)(2,1)S(1)}, u32[]{:S(2)}, u32[]{:S(2)}) %collective-permute-start.14) | collective-permute-done | bytes 65568 | tf_op jit(solution)/shard_map/ppermute | solution.py:408
  177.0 2.1 %combine.1 = (f32[128,256]{1,0:T(8,128)}, f32[128,256]{1,0:T(8,128)}) custom-call(s32[4]{0:T(128)} %pad_add_fusion.place, bf16[2,128,512]{2,1,0:T(8,128)(2,1)} %get-tuple-element.19.table_ref, bf16[512,512]{1,0:T(8,128)(2,1)} %bitcast.28), custom_call_target="tpu_custom_call" | custom-call | tf_op jit(solution)/shard_map/combine/pallas_call | solution.py:330
  180.3 3.7 %collective-permute-start.17 = (bf16[2,64,128]{2,1,0:T(8,128)(2,1)S(1)}, bf16[2,64,128]{2,1,0:T(8,128)(2,1)S(1)}, u32[]{:S(2)}, u32[]{:S(2)}) collective-permute-start(bf16[2,64,128]{2,1,0:T(8,128)(2,1)S(1)} %get-tuple-element.31), channel_id=1, source_target_pairs={{0,4},{2,6},{4,0},{6,2},{1,5},{3,7},{5,1},{7,3},{8,12},{10,14},{12... | collective-permute-start | bytes 98312 | tf_op jit(solution)/shard_map/ppermute | solution.py:403
  188.5 3.8 %project.1 = bf16[64,2048]{1,0:T(8,128)(2,1)} custom-call(s32[4]{0:T(128)} %pad_add_fusion.place, bf16[2,64,128]{2,1,0:T(8,128)(2,1)} %get-tuple-element.29.refs_0_, bf16[2,64,128]{2,1,0:T(8,128)(2,1)} %copy-done.25, bf16[2,64,128]{2,1,0:T(8,128)(2,1)} %copy-done.26, bf16[2,64,128]{2,1,0:T(8,128)(2,1)} %copy-done.27, f32[8,128]{1,0:T(8,128)} %bitcast.39, ...), custom_call_target="tpu_custom_call" | custom-call | tf_op jit(solution)/shard_map/project/pallas_call | solution.py:251
  (124 shorter events, 40.2 us)
Async XLA Ops:
  6.9 28.5 %all-to-all-start = ((bf16[32,16,512]{2,1,0:T(8,128)(2,1)}), bf16[32,16,512]{2,1,0:T(8,128)(2,1)S(1)}, u32[]{:S(2)}, u32[]{:S(2)}) async-start(bf16[32,16,512]{2,1,0:T(8,128)(2,1)} %bitcast.35), calls=%async_computation | async-start | bytes 1048576 | tf_op jit(solution)/shard_map/all_to_all | solution.py:440
  18.5 33.9 %collective-permute-start.23 = (bf16[2048,256]{1,0:T(8,128)(2,1)}, bf16[2048,256]{1,0:T(8,128)(2,1)S(1)}, u32[]{:S(2)}, u32[]{:S(2)}) collective-permute-start(bf16[2048,256]{1,0:T(8,128)(2,1)} %bitcast.29), channel_id=1, source_target_pairs={{0,1},{1,0},{2,3},{3,2},{4,5},{5,4},{6,7},{7,6},{8,9},{9,8},{10,11... | collective-permute-start | bytes 3145736 | tf_op jit(solution)/shard_map/ppermute | solution.py:403
  18.6 33.8 %collective-permute-start.24 = (bf16[2048,256]{1,0:T(8,128)(2,1)}, bf16[2048,256]{1,0:T(8,128)(2,1)}, u32[]{:S(2)}, u32[]{:S(2)}) collective-permute-start(bf16[2048,256]{1,0:T(8,128)(2,1)} %bitcast.31), channel_id=1, source_target_pairs={{0,1},{1,0},{2,3},{3,2},{4,5},{5,4},{6,7},{7,6},{8,9},{9,8},{10,11... | collective-permute-start | bytes 3145736 | tf_op jit(solution)/shard_map/ppermute | solution.py:403
  19.1 33.3 %collective-permute-start.25 = (bf16[256,2048]{1,0:T(8,128)(2,1)}, bf16[256,2048]{1,0:T(8,128)(2,1)}, u32[]{:S(2)}, u32[]{:S(2)}) collective-permute-start(bf16[256,2048]{1,0:T(8,128)(2,1)} %bitcast.33), channel_id=1, source_target_pairs={{0,1},{1,0},{2,3},{3,2},{4,5},{5,4},{6,7},{7,6},{8,9},{9,8},{10,11... | collective-permute-start | bytes 3145736 | tf_op jit(solution)/shard_map/ppermute | solution.py:403
  35.3 13.6 %collective-permute-start.19 = (bf16[512,512]{1,0:T(8,128)(2,1)S(1)}, bf16[512,512]{1,0:T(8,128)(2,1)S(1)}, u32[]{:S(2)}, u32[]{:S(2)}) collective-permute-start(bf16[512,512]{1,0:T(8,128)(2,1)S(1)} %bitcast.25), channel_id=1, source_target_pairs={{0,2},{2,4},{4,6},{6,0},{1,3},{3,5},{5,7},{7,1},{8,10},{10,12},{12... | collective-permute-start | bytes 1572872 | tf_op jit(solution)/shard_map/ppermute | solution.py:403
  36.9 12.5 %collective-permute-start.20 = (bf16[512,512]{1,0:T(8,128)(2,1)S(1)}, bf16[512,512]{1,0:T(8,128)(2,1)S(1)}, u32[]{:S(2)}, u32[]{:S(2)}) collective-permute-start(bf16[512,512]{1,0:T(8,128)(2,1)S(1)} %bitcast.26), channel_id=1, source_target_pairs={{0,6},{2,0},{4,2},{6,4},{1,7},{3,1},{5,3},{7,5},{8,14},{10,8},{12,... | collective-permute-start | bytes 1572872 | tf_op jit(solution)/shard_map/ppermute | solution.py:403
  49.0 7.7 %collective-permute-start.21 = (bf16[256,512]{1,0:T(8,128)(2,1)S(1)}, bf16[256,512]{1,0:T(8,128)(2,1)S(1)}, u32[]{:S(2)}, u32[]{:S(2)}) collective-permute-start(bf16[256,512]{1,0:T(8,128)(2,1)S(1)} %slice.42), channel_id=1, source_target_pairs={{0,2},{2,4},{4,6},{6,0},{1,3},{3,5},{5,7},{7,1},{8,10},{10,12},{12... | collective-permute-start | bytes 786440 | tf_op jit(solution)/shard_map/ppermute | solution.py:403
  67.3 7.9 %collective-permute-start.26 = (bf16[256,512]{1,0:T(8,128)(2,1)}, bf16[256,512]{1,0:T(8,128)(2,1)S(1)}, u32[]{:S(2)}, u32[]{:S(2)}) collective-permute-start(bf16[256,512]{1,0:T(8,128)(2,1)} %get-tuple-element.23), channel_id=1, source_target_pairs={{0,2},{2,4},{4,6},{6,0},{1,3},{3,5},{5,7},{7,1},{8,10},{10,12},{12... | collective-permute-start | bytes 786440 | tf_op jit(solution)/shard_map/ppermute | solution.py:403
  68.5 7.8 %collective-permute-start.28 = (bf16[256,512]{1,0:T(8,128)(2,1)}, bf16[256,512]{1,0:T(8,128)(2,1)S(1)}, u32[]{:S(2)}, u32[]{:S(2)}) collective-permute-start(bf16[256,512]{1,0:T(8,128)(2,1)} %get-tuple-element.25), channel_id=1, source_target_pairs={{0,6},{2,0},{4,2},{6,4},{1,7},{3,1},{5,3},{7,5},{8,14},{10,8},{12,... | collective-permute-start | bytes 786440 | tf_op jit(solution)/shard_map/ppermute | solution.py:403
  76.2 12.2 %collective-permute-start.27 = (bf16[512,512]{1,0:T(8,128)(2,1)S(1)}, bf16[512,512]{1,0:T(8,128)(2,1)S(1)}, u32[]{:S(2)}, u32[]{:S(2)}) collective-permute-start(bf16[512,512]{1,0:T(8,128)(2,1)S(1)} %pad_maximum_fusion), channel_id=1, source_target_pairs={{0,2},{2,4},{4,6},{6,0},{1,3},{3,5},{5,7},{7,1},{8,10},{10,12},{12... | collective-permute-start | bytes 1572872 | tf_op jit(solution)/shard_map/ppermute | solution.py:403
  77.4 11.0 %collective-permute-start.29 = (bf16[512,512]{1,0:T(8,128)(2,1)S(1)}, bf16[512,512]{1,0:T(8,128)(2,1)S(1)}, u32[]{:S(2)}, u32[]{:S(2)}) collective-permute-start(bf16[512,512]{1,0:T(8,128)(2,1)S(1)} %pad_maximum_fusion.1), channel_id=1, source_target_pairs={{0,6},{2,0},{4,2},{6,4},{1,7},{3,1},{5,3},{7,5},{8,14},{10,8},{12,... | collective-permute-start | bytes 1572872 | tf_op jit(solution)/shard_map/ppermute | solution.py:403
  80.7 7.7 %collective-permute-start.2 = (bf16[512,128]{1,0:T(8,128)(2,1)S(1)}, bf16[512,128]{1,0:T(8,128)(2,1)S(1)}, u32[]{:S(2)}, u32[]{:S(2)}) collective-permute-start(bf16[512,128]{1,0:T(8,128)(2,1)S(1)} %copy-done.7), channel_id=1, source_target_pairs={{0,32},{32,64},{64,96},{96,128},{128,160},{160,192},{192,224},{224... | collective-permute-start | bytes 393224 | tf_op jit(solution)/shard_map/ppermute | solution.py:403
  82.7 19.3 %collective-permute-start = (bf16[256,128]{1,0:T(8,128)(2,1)S(1)}, bf16[256,128]{1,0:T(8,128)(2,1)S(1)}, u32[]{:S(2)}, u32[]{:S(2)}) collective-permute-start(bf16[256,128]{1,0:T(8,128)(2,1)S(1)} %get-tuple-element.37), channel_id=1, source_target_pairs={{0,224},{32,192},{64,160},{96,128},{128,96},{160,64},{192,32},{224... | collective-permute-start | bytes 196616 | tf_op jit(solution)/shard_map/ppermute | solution.py:408
  85.7 13.5 %collective-permute-start.5 = (bf16[512,128]{1,0:T(8,128)(2,1)S(1)}, bf16[512,128]{1,0:T(8,128)(2,1)S(1)}, u32[]{:S(2)}, u32[]{:S(2)}) collective-permute-start(bf16[512,128]{1,0:T(8,128)(2,1)S(1)} %collective-permute-done.3.refs_4_), channel_id=1, source_target_pairs={{0,224},{32,0},{64,32},{96,64},{128,96},{160,128},{192,160},{224,1... | collective-permute-start | bytes 393224 | tf_op jit(solution)/shard_map/ppermute | solution.py:403
  88.3 17.3 %collective-permute-start.4 = (bf16[512,128]{1,0:T(8,128)(2,1)S(1)}, bf16[512,128]{1,0:T(8,128)(2,1)S(1)}, u32[]{:S(2)}, u32[]{:S(2)}) collective-permute-start(bf16[512,128]{1,0:T(8,128)(2,1)S(1)} %collective-permute-done.2.refs_3_), channel_id=1, source_target_pairs={{0,32},{32,64},{64,96},{96,128},{128,160},{160,192},{192,224},{224... | collective-permute-start | bytes 393224 | tf_op jit(solution)/shard_map/ppermute | solution.py:403
  89.4 86.8 %all-to-all-start.1 = ((bf16[32,16,512]{2,1,0:T(8,128)(2,1)}), bf16[32,16,512]{2,1,0:T(8,128)(2,1)S(1)}, u32[]{:S(2)}, u32[]{:S(2)}) async-start(bf16[32,16,512]{2,1,0:T(8,128)(2,1)} %bitcast.18), calls=%async_computation.1 | async-start | bytes 1048576 | tf_op jit(solution)/shard_map/all_to_all | solution.py:463
  99.2 11.5 %collective-permute-start.7 = (bf16[512,128]{1,0:T(8,128)(2,1)S(1)}, bf16[512,128]{1,0:T(8,128)(2,1)S(1)}, u32[]{:S(2)}, u32[]{:S(2)}) collective-permute-start(bf16[512,128]{1,0:T(8,128)(2,1)S(1)} %collective-permute-done.5.refs_6_), channel_id=1, source_target_pairs={{0,224},{32,0},{64,32},{96,64},{128,96},{160,128},{192,160},{224,1... | collective-permute-start | bytes 393224 | tf_op jit(solution)/shard_map/ppermute | solution.py:403
  102.0 11.9 %collective-permute-start.10 = (bf16[512,128]{1,0:T(8,128)(2,1)S(1)}, bf16[512,128]{1,0:T(8,128)(2,1)S(1)}, u32[]{:S(2)}, u32[]{:S(2)}) collective-permute-start(bf16[512,128]{1,0:T(8,128)(2,1)S(1)} %pad_maximum_fusion.2.refs_0_), channel_id=1, source_target_pairs={{0,16},{8,24},{16,0},{24,8},{1,17},{9,25},{17,1},{25,9},{2,18},{10... | collective-permute-start | bytes 393224 | tf_op jit(solution)/shard_map/ppermute | solution.py:403
  104.2 9.7 %collective-permute-start.11 = (bf16[512,128]{1,0:T(8,128)(2,1)S(1)}, bf16[512,128]{1,0:T(8,128)(2,1)S(1)}, u32[]{:S(2)}, u32[]{:S(2)}) collective-permute-start(bf16[512,128]{1,0:T(8,128)(2,1)S(1)} %pad_maximum_fusion.2.refs_0_), channel_id=1, source_target_pairs={{0,24},{8,0},{16,8},{24,16},{1,25},{9,1},{17,9},{25,17},{2,26},{10... | collective-permute-start | bytes 393224 | tf_op jit(solution)/shard_map/ppermute | solution.py:403
  105.6 8.3 %collective-permute-start.6 = (bf16[512,128]{1,0:T(8,128)(2,1)S(1)}, bf16[512,128]{1,0:T(8,128)(2,1)S(1)}, u32[]{:S(2)}, u32[]{:S(2)}) collective-permute-start(bf16[512,128]{1,0:T(8,128)(2,1)S(1)} %collective-permute-done.4.refs_5_), channel_id=1, source_target_pairs={{0,32},{32,64},{64,96},{96,128},{128,160},{160,192},{192,224},{224... | collective-permute-start | bytes 393224 | tf_op jit(solution)/shard_map/ppermute | solution.py:403
  112.4 28.1 %collective-permute-start.1 = (bf16[512,128]{1,0:T(8,128)(2,1)S(1)}, bf16[512,128]{1,0:T(8,128)(2,1)S(1)}, u32[]{:S(2)}, u32[]{:S(2)}) collective-permute-start(bf16[512,128]{1,0:T(8,128)(2,1)S(1)} %pad_maximum_fusion.2.refs_0_), channel_id=1, source_target_pairs={{0,8},{8,16},{16,24},{24,0},{1,9},{9,17},{17,25},{25,1},{2,10},{10... | collective-permute-start | bytes 393224 | tf_op jit(solution)/shard_map/ppermute | solution.py:403
  138.5 25.1 %collective-permute-start.12 = (bf16[2,80,512]{2,1,0:T(8,128)(2,1)}, bf16[2,80,512]{2,1,0:T(8,128)(2,1)S(1)}, u32[]{:S(2)}, u32[]{:S(2)}) collective-permute-start(bf16[2,80,512]{2,1,0:T(8,128)(2,1)} %get-tuple-element.17), channel_id=1, source_target_pairs={{0,16},{8,24},{16,0},{24,8},{1,17},{9,25},{17,1},{25,9},{2,18},{10... | collective-permute-start | bytes 491528 | tf_op jit(solution)/shard_map/ppermute | solution.py:403
  138.5 25.1 %collective-permute-start.13 = (bf16[2,80,512]{2,1,0:T(8,128)(2,1)}, bf16[2,80,512]{2,1,0:T(8,128)(2,1)S(1)}, u32[]{:S(2)}, u32[]{:S(2)}) collective-permute-start(bf16[2,80,512]{2,1,0:T(8,128)(2,1)} %get-tuple-element.18), channel_id=1, source_target_pairs={{0,8},{8,16},{16,24},{24,0},{1,9},{9,17},{17,25},{25,1},{2,10},{10... | collective-permute-start | bytes 491528 | tf_op jit(solution)/shard_map/ppermute | solution.py:403
  179.1 13.2 %collective-permute-start.30 = (f32[128,256]{1,0:T(8,128)}, f32[128,256]{1,0:T(8,128)S(1)}, u32[]{:S(2)}, u32[]{:S(2)}) collective-permute-start(f32[128,256]{1,0:T(8,128)} %get-tuple-element.27), channel_id=1, source_target_pairs={{0,1},{1,0},{2,3},{3,2},{4,5},{5,4},{6,7},{7,6},{8,9},{9,8},{10,11... | collective-permute-start | bytes 393224 | tf_op jit(solution)/shard_map/ppermute | solution.py:403
  (37 other events, 298.8 us)
